TPU v7x, 32 devices: a whole 2x2x4 slice. The times are simulated.
32 devices in a mesh: fs: 4 (over z), rep: 4 (over y, x), tp: 2 (over core).
Axes of the slice: x: 2, y: 2, z: 4, core: 2. Of those that a mesh axis runs over, the one named last changes fastest.
Arguments:
- saved_inputs: bfloat16 [12288, 2048], P(('fs', 'rep')), may hold values from -6 to 6
- query_cotangent: bfloat16 [12288, 1024], P(('fs', 'rep'), 'tp'), may hold values from -0.053955078 to 0.053955078
- value_cotangent: bfloat16 [12288, 2048], P(('fs', 'rep'), 'tp'), may hold values from -0.053955078 to 0.053955078
- query_weight: float32 [2048, 1024], P('fs', 'tp'), may hold values from -0.125 to 0.125
- value_weight: float32 [2048, 2048], P('fs', 'tp'), may hold values from -0.125 to 0.125
- query_factor: bfloat16 [2048, 256], P('fs'), as said below
- value_factor: bfloat16 [2048, 256], P('fs'), as said below
- query_first: float32 [256, 1024], P('rep', 'tp'), may hold values from -6 to 6
- query_second: float32 [256, 1024], P('rep', 'tp'), may hold values from 0.3 to 3
- value_first: float32 [256, 2048], P('rep', 'tp'), may hold values from -6 to 6
- value_second: float32 [256, 2048], P('rep', 'tp'), may hold values from 0.3 to 3
Outputs:
- query_direction: float32 [2048, 1024], P('fs', 'tp')
- value_direction: float32 [2048, 2048], P('fs', 'tp')
- query_master: float32 [2048, 1024], P('fs', 'tp')
- value_master: float32 [2048, 2048], P('fs', 'tp')
- query_first_new: float32 [256, 1024], P('rep', 'tp')
- query_second_new: float32 [256, 1024], P('rep', 'tp')
- value_first_new: float32 [256, 2048], P('rep', 'tp')
- value_second_new: float32 [256, 2048], P('rep', 'tp')
- query_copy: bfloat16 [2048, 1024], P(None, 'tp')
- value_copy: bfloat16 [2048, 2048], P(None, 'tp')
Inputs may be any that keep to these rules, and one draw needn't show every extreme that they name: `query_factor`: A matrix of full rank. `value_factor`: A matrix of full rank.
All inputs are finite; a program needn't handle non-finite values.
Results may differ from a plain program's by a relative error of at most 0.012.
Values may be sent and summed in bfloat16 or wider, within the bound.
No kernel may reach another device: no remote copies, remote signals or barrier semaphores. Data moves between devices by JAX's collectives and lax.ppermute only.
A program may use at most 128 MiB of HBM per device.

v0:
```python
import functools

import jax
import jax.numpy as jnp
from jax import lax
from jax.experimental import pallas as pl
from jax.experimental.pallas import tpu as pltpu
from jax.sharding import PartitionSpec as P


BETA_ONE = 0.8
BETA_TWO = 0.9
EPS_RATIO = 1e-08
EPS_NORM = 1e-06
RATE = 0.02


BF = jnp.bfloat16
F32 = jnp.float32
VMEM = pl.BlockSpec(memory_space=pltpu.VMEM)
ANY = pl.BlockSpec(memory_space=pltpu.HBM)
TILE = 16


def swap(x, axis, n, k):
    return lax.ppermute(x, axis, [(i, i ^ k) for i in range(n)])


def rows_at(block, height):
    return pl.ds(pl.multiple_of(block * height, height), height)


def call(body, outs, n_in, scratch=(), limit=8, flops=0, nbytes=0, in_specs=None, out_specs=None):
    return pl.pallas_call(
        body,
        out_shape=outs,
        in_specs=in_specs or [VMEM] * n_in,
        out_specs=out_specs or [VMEM] * len(outs),
        scratch_shapes=list(scratch),
        compiler_params=pltpu.CompilerParams(vmem_limit_bytes=limit << 20),
        cost_estimate=pl.CostEstimate(flops=flops, bytes_accessed=nbytes, transcendentals=0),
    )


def first_body(nr, fq, fv, out, sem):
    r, t = lax.axis_index("rep"), lax.axis_index("tp")
    here = rows_at(r, fq.shape[0] // nr)
    for n, ref in enumerate((fq, fv)):

        @pl.when(t == n)
        def _():
            move = pltpu.make_async_copy(ref.at[here, :], out, sem)
            move.start()
            move.wait()


def pack_body(nr, wq_h, wv_h, quarter, low, high, wq, wv, sem):
    r = lax.axis_index("rep")
    dl, nq = wq.shape
    loads = [pltpu.make_async_copy(wq_h, wq, sem.at[0]), pltpu.make_async_copy(wv_h, wv, sem.at[1])]
    for c in loads:
        c.start()
    for c in loads:
        c.wait()
    for out, here in ((quarter, rows_at(r, dl // nr)), (low, slice(0, dl // 2)), (high, slice(dl // 2, dl))):
        out[:, :nq] = wq[here, :].astype(BF)
        out[:, nq:] = wv[here, :].astype(BF)


def project_body(nf, nr, *refs):
    x, fq, fv, cq_h, cv_h = refs[:5]
    mine, other = refs[5 : 5 + nr], refs[5 + nr : 5 + 2 * nr]
    outs = refs[5 + 2 * nr : 5 + 3 * nr]
    fac, part, cq, cv, sem = refs[5 + 3 * nr :]
    loads = [pltpu.make_async_copy(cq_h, cq, sem.at[0]), pltpu.make_async_copy(cv_h, cv, sem.at[1])]
    for c in loads:
        c.start()
    f, r, t = lax.axis_index("fs"), lax.axis_index("rep"), lax.axis_index("tp")
    dl = fq.shape[0]
    piece = dl // nr
    fac[0, rows_at(f, dl), :] = fq[...]
    fac[1, rows_at(f, dl), :] = fv[...]
    for k in range(1, nf):
        for j in range(nr):
            here = rows_at((f ^ k) * nr + (r ^ j), piece)
            fac[t, here, :] = mine[j][k - 1]
            fac[1 - t, here, :] = other[j][k - 1]
    nq = cq.shape[1]
    dims = (((0,), (0,)), ((), ()))
    yq = jnp.dot(x[...], fac[0], preferred_element_type=F32).astype(BF)
    for c in loads:
        c.wait()
    part[:, :nq] = lax.dot_general(yq, cq[...], dims, preferred_element_type=F32).astype(BF)
    yv = jnp.dot(x[...], fac[1], preferred_element_type=F32).astype(BF)
    part[:, nq:] = lax.dot_general(yv, cv[...], dims, preferred_element_type=F32).astype(BF)
    h = part.shape[0] // nr
    for j in range(nr):
        outs[j][...] = part[rows_at(r ^ j, h), :]


def plane_sum_body(nf, nr, *refs):
    ins, own, rest, acc = refs[:nr], refs[nr], refs[nr + 1 : nr + nf], refs[nr + nf]
    f = lax.axis_index("fs")
    total = ins[0][...].astype(F32)
    for ref in ins[1:]:
        total += ref[...].astype(F32)
    acc[...] = total
    h = acc.shape[0] // nf
    own[...] = acc[rows_at(f, h), :]
    for k in range(1, nf):
        rest[k - 1][...] = acc[rows_at(f ^ k, h), :].astype(BF)


def line_sum_body(nf, *refs):
    total = refs[0][...]
    for ref in refs[1:nf]:
        total += ref[...].astype(F32)
    refs[nf][...] = total.astype(BF)


def moments_body(nf, nq, *refs):
    ins = refs[:nf]
    q1, q2, v1, v2 = refs[nf : nf + 4]
    q1n, q2n, v1n, v2n, ratio, proj = refs[nf + 4 :]
    f = lax.axis_index("fs")
    h = ins[0].shape[0]
    for k in range(nf):
        proj[rows_at(f ^ k, h), :] = ins[k][...].astype(F32)
    for cols, first, second, fo, so in (
        (slice(None, nq), q1, q2, q1n, q2n),
        (slice(nq, None), v1, v2, v1n, v2n),
    ):
        p = proj[:, cols]
        fn = BETA_ONE * first[...] + (1.0 - BETA_ONE) * p
        sn = BETA_TWO * second[...] + (1.0 - BETA_TWO) * p * p
        fo[...] = fn
        so[...] = sn
        ratio[:, cols] = (fn / (jnp.sqrt(sn) + EPS_RATIO)).astype(BF)


def gram_body(fac, out):
    dims = (((0,), (0,)), ((), ()))
    for s in range(2):
        out[s] = lax.dot_general(fac[s], fac[s], dims, preferred_element_type=F32)


def total_body(nr, nq, *refs):
    ins, gram, ratio, total = refs[:nr], refs[nr], refs[nr + 1], refs[nr + 2]
    r = lax.axis_index("rep")
    h = ins[0].shape[0]
    for j in range(nr):
        ratio[rows_at(r ^ j, h), :] = ins[j][...]
    for s, cols in ((0, slice(None, nq)), (1, slice(nq, None))):
        z = ratio[:, cols]
        g = gram[s]
        acc = None
        for _ in range(3):
            high = g.astype(BF)
            g = g - high.astype(F32)
            term = jnp.dot(high, z, preferred_element_type=F32)
            acc = term if acc is None else acc + term
        total[rows_at(s, 8), :] = jnp.broadcast_to(jnp.sum(acc * z.astype(F32), keepdims=True), (8, 128))


def final_body(nf, nr, nt, *refs):
    fac, ratio, tot, tot_in, wq, wv = refs[:6]
    near, far = refs[6:8], refs[8:-14]
    qd_h, vd_h, qm_h, vm_h, qc_h, vc_h, raw, qd, vd, qm, vm, qc, vc, sem = refs[-14:]
    f, r = lax.axis_index("fs"), lax.axis_index("rep")
    dl, nq, nv = wq.shape[0], wq.shape[1], wv.shape[1]
    half = (nq + nv) // 2
    d = dl * nf
    piece = dl // nr
    both = tot[...] + tot_in[...]
    sq = lax.rsqrt(both[0:1, 0:1] / (d * nq * nt) + EPS_NORM)
    sv = lax.rsqrt(both[8:9, 0:1] / (d * nv * nt) + EPS_NORM)
    stores = []

    def put(k, here, cols, w):
        value = (w.astype(F32) - RATE * raw[here, cols]).astype(BF)
        split = min(max(nq - cols.start, 0), cols.stop - cols.start)
        if split:
            qc[k, here, cols.start : cols.start + split] = value[:, :split]
        if split < cols.stop - cols.start:
            vc[k, here, cols.start + split - nq : cols.stop - nq] = value[:, split:]

    left, right, whole = slice(0, half), slice(half, 2 * half), slice(0, 2 * half)
    for k in range(nf):
        raw[:, :nq] = jnp.dot(fac[0, rows_at(f ^ k, dl), :], ratio[:, :nq], preferred_element_type=F32) * sq
        raw[:, nq:] = jnp.dot(fac[1, rows_at(f ^ k, dl), :], ratio[:, nq:], preferred_element_type=F32) * sv
        if k == 0:
            qd[...] = raw[:, :nq]
            vd[...] = raw[:, nq:]
            qm[...] = wq[...] - RATE * raw[:, :nq]
            vm[...] = wv[...] - RATE * raw[:, nq:]
            put(0, slice(None), slice(0, nq), wq[...].astype(BF))
            put(0, slice(None), slice(nq, nq + nv), wv[...].astype(BF))
            stores += [
                pltpu.make_async_copy(qd, qd_h, sem.at[0]),
                pltpu.make_async_copy(vd, vd_h, sem.at[1]),
                pltpu.make_async_copy(qm, qm_h, sem.at[2]),
                pltpu.make_async_copy(vm, vm_h, sem.at[3]),
            ]
            for c in stores:
                c.start()
        elif k == 1:
            put(1, slice(0, dl // 2), whole, near[0][...])
            put(1, slice(dl // 2, dl), whole, near[1][...])
        else:
            own_z, xa, yb, ya, xb = far[5 * (k - 2) : 5 * (k - 1)]
            put(k, rows_at(r, piece), whole, own_z[...])
            for cols, group in ((left, (xa[...], ya[0], ya[1])), (right, (xb[0], yb[...], xb[1]))):
                for m, w in enumerate(group):
                    put(k, rows_at(r ^ (m + 1), piece), cols, w)
        new = [
            pltpu.make_async_copy(qc.at[k], qc_h.at[rows_at(f ^ k, dl), :], sem.at[4 + 2 * k]),
            pltpu.make_async_copy(vc.at[k], vc_h.at[rows_at(f ^ k, dl), :], sem.at[5 + 2 * k]),
        ]
        for c in new:
            c.start()
        stores += new
    for c in stores:
        c.wait()


def exchange(nf, nr, nt, xs, cq, cv, wq, wv, fq, fv, q1, q2, v1, v2):
    S = jax.ShapeDtypeStruct
    dl, rank = fq.shape
    nq, nv = cq.shape[1], cv.shape[1]
    nc = nq + nv
    half = nc // 2
    d = nf * dl
    piece = dl // nr
    tokens = xs.shape[0]

    (start,) = call(functools.partial(first_body, nr), [S((piece, rank), BF)], 2, [pltpu.SemaphoreType.DMA], limit=60, in_specs=[ANY] * 2)(fq, fv)
    zs = [swap(start, "fs", nf, k) for k in range(1, nf)]
    stacked = jnp.stack(zs)
    mine = [stacked] + [swap(stacked, "rep", nr, j) for j in range(1, nr)]
    other = [swap(m, "tp", nt, 1) for m in mine]

    quarter, low, high = call(
        functools.partial(pack_body, nr),
        [S((piece, nc), BF)] + [S((dl // 2, nc), BF)] * 2,
        2,
        [pltpu.VMEM((dl, nq), F32), pltpu.VMEM((dl, nv), F32), pltpu.SemaphoreType.DMA((2,))],
        in_specs=[ANY] * 2,
        limit=12,
    )(wq, wv)
    near = [swap(low, "fs", nf, 1), swap(high, "fs", nf, 1)]
    far = []
    for k in range(2, nf):
        own_z = swap(quarter, "fs", nf, k)
        fa, fb = own_z[:, :half], own_z[:, half:]
        xa = swap(fa, "rep", nr, 1)
        yb = swap(fb, "rep", nr, 2)
        ya = swap(jnp.stack([fa, xa]), "rep", nr, 2)
        xb = swap(jnp.stack([fb, yb]), "rep", nr, 1)
        far += [own_z, xa, yb, ya, xb]

    h = rank // nr
    *parts, fac = call(
        functools.partial(project_body, nf, nr),
        [S((h, nc), BF)] * nr + [S((2, d, rank), BF)],
        5 + 2 * nr,
        [
            pltpu.VMEM((rank, nc), BF),
            pltpu.VMEM(cq.shape, BF),
            pltpu.VMEM(cv.shape, BF),
            pltpu.SemaphoreType.DMA((2,)),
        ],
        limit=24,
        in_specs=[VMEM] * 3 + [ANY] * 2 + [VMEM] * 2 * nr,
        flops=2 * tokens * (d * 2 * rank + rank * nc),
        nbytes=2 * (tokens * (d + nc) + 4 * d * rank),
    )(xs, fq, fv, cq, cv, *mine, *other)
    (gram,) = call(gram_body, [S((2, rank, rank), F32)], 1, flops=4 * d * rank * rank, nbytes=4 * d * rank)(fac)

    got = [parts[0]] + [swap(parts[j], "rep", nr, j) for j in range(1, nr)]
    g = h // nf
    own, *rest = call(
        functools.partial(plane_sum_body, nf, nr),
        [S((g, nc), F32)] + [S((g, nc), BF)] * (nf - 1),
        nr,
        [pltpu.VMEM((h, nc), F32)],
    )(*got)
    got = [own] + [swap(rest[k - 1], "fs", nf, k) for k in range(1, nf)]
    (proj,) = call(functools.partial(line_sum_body, nf), [S((g, nc), BF)], nf)(*got)
    got = [proj] + [swap(proj, "fs", nf, k) for k in range(1, nf)]
    q1n, q2n, v1n, v2n, ratio = call(
        functools.partial(moments_body, nf, nq),
        [S((h, nq), F32)] * 2 + [S((h, nv), F32)] * 2 + [S((h, nc), BF)],
        nf + 4,
        [pltpu.VMEM((h, nc), F32)],
    )(*got, q1, q2, v1, v2)
    got = [ratio] + [swap(ratio, "rep", nr, j) for j in range(1, nr)]
    ratios, total = call(
        functools.partial(total_body, nr, nq), [S((rank, nc), BF), S((16, 128), F32)], nr + 1, limit=12
    )(*got, gram)
    total_in = swap(total, "tp", nt, 1)
    return (
        *call(
            functools.partial(final_body, nf, nr, nt),
            [S((dl, nq), F32), S((dl, nv), F32)] * 2 + [S((d, nq), BF), S((d, nv), BF)],
            8 + 5 * (nf - 2),
            [
                pltpu.VMEM((dl, nc), F32),
                pltpu.VMEM((dl, nq), F32),
                pltpu.VMEM((dl, nv), F32),
                pltpu.VMEM((dl, nq), F32),
                pltpu.VMEM((dl, nv), F32),
                pltpu.VMEM((nf, dl, nq), BF),
                pltpu.VMEM((nf, dl, nv), BF),
                pltpu.SemaphoreType.DMA((4 + 2 * nf,)),
            ],
            limit=36,
            out_specs=[ANY] * 6,
            flops=2 * d * rank * nc,
            nbytes=2 * d * nc * 2 + 12 * dl * nc,
        )(fac, ratios, total, total_in, wq, wv, *near, *far),
        q1n, q2n, v1n, v2n,
    )


def moments(projected, first, second):
    first_new = BETA_ONE * first + (1.0 - BETA_ONE) * projected
    second_new = BETA_TWO * second + (1.0 - BETA_TWO) * projected * projected
    ratio = first_new / (jnp.sqrt(second_new) + EPS_RATIO)
    return (first_new, second_new, ratio)


def collective(nf, nt, xs, cq, cv, wq, wv, fq, fv, q1, q2, v1, v2):
    dims = (((0,), (0,)), ((), ()))
    highest = lax.Precision.HIGHEST

    def one(cot, weight, factor, first, second):
        grad = lax.dot_general(xs, cot, dims, preferred_element_type=F32)
        whole = lax.all_gather(factor, "fs", axis=0, tiled=True).astype(F32)
        proj = jnp.dot(whole.T, grad, precision=highest)
        proj = lax.psum_scatter(proj.astype(BF), "rep", scatter_dimension=0, tiled=True).astype(F32)
        first_new, second_new, ratio = moments(lax.psum(proj, "fs"), first, second)
        ratio = lax.all_gather(ratio, "rep", axis=0, tiled=True)
        raw = jnp.dot(factor.astype(F32), ratio, precision=highest)
        total = lax.psum(jnp.sum(raw * raw), ("fs", "tp"))
        size = raw.size * nf * nt
        direction = raw * lax.rsqrt(total / size + EPS_NORM)
        master = weight - RATE * direction
        copy = lax.all_gather(master.astype(BF), "fs", axis=0, tiled=True)
        return direction, master, first_new, second_new, copy

    qd, qm, q1n, q2n, qc = one(cq, wq, fq, q1, q2)
    vd, vm, v1n, v2n, vc = one(cv, wv, fv, v1, v2)
    return qd, vd, qm, vm, q1n, q2n, v1n, v2n, qc, vc


def local(nf, nr, nt, *args):
    rank = args[5].shape[1]
    if not square(nf, nr, nt) or rank % (nf * nr * TILE):
        return collective(nf, nt, *args)
    qd, vd, qm, vm, qc, vc, *new = exchange(nf, nr, nt, *args)
    return qd, vd, qm, vm, *new, qc, vc


def square(nf, nr, nt):
    return (nf, nr, nt) == (4, 2 * 2, 2)


def solution(mesh):
    placed = (
        P(("fs", "rep"), None),
        P(("fs", "rep"), "tp"),
        P(("fs", "rep"), "tp"),
        P("fs", "tp"),
        P("fs", "tp"),
        P("fs", None),
        P("fs", None),
        P("rep", "tp"),
        P("rep", "tp"),
        P("rep", "tp"),
        P("rep", "tp"),
    )
    return jax.shard_map(
        functools.partial(local, mesh.shape["fs"], mesh.shape["rep"], mesh.shape["tp"]),
        mesh=mesh,
        in_specs=placed,
        out_specs=(P("fs", "tp"),) * 4 + (P("rep", "tp"),) * 4 + (P(None, "tp"),) * 2,
        check_vma=False,
    )
```

profile of v0, /device:TPU:0, one launch (start us, length us, event | category | flops | bytes accessed | tf_op | source)
XLA Modules:
  0.0 138.9 jit_solution(13318446180088997166)
XLA Ops:
  0.7 1.5 %shard_map.186 = bf16[128,256]{1,0:T(8,128)(2,1)} custom-call(bf16[512,256]{1,0:T(8,128)(2,1)} %refs_1_.1, bf16[512,256]{1,0:T(8,128)(2,1)} %refs_2_.1), custom_call_target="tpu_custom_call" | custom-call | tf_op jit(solution)/shard_map/pallas_call | solution.py:236
  2.2 5.1 %collective-permute-start.2 = (bf16[128,256]{1,0:T(8,128)(2,1)}, bf16[128,256]{1,0:T(8,128)(2,1)S(1)}, u32[]{:S(2)}, u32[]{:S(2)}) collective-permute-start(bf16[128,256]{1,0:T(8,128)(2,1)} %shard_map.186), channel_id=1, source_target_pairs={{0,24},{8,16},{16,8},{24,0},{1,25},{9,17},{17,9},{25,1},{2,26},{10... | collective-permute-start | bytes 196616 | tf_op jit(solution)/shard_map/ppermute | solution.py:26
  8.0 2.2 %collective-permute-done.2 = bf16[128,256]{1,0:T(8,128)(2,1)S(1)} collective-permute-done((bf16[128,256]{1,0:T(8,128)(2,1)}, bf16[128,256]{1,0:T(8,128)(2,1)S(1)}, u32[]{:S(2)}, u32[]{:S(2)}) %collective-permute-start.2) | collective-permute-done | bytes 65568 | tf_op jit(solution)/shard_map/ppermute | solution.py:26
  10.2 3.0 %collective-permute-done.1 = bf16[128,256]{1,0:T(8,128)(2,1)S(1)} collective-permute-done((bf16[128,256]{1,0:T(8,128)(2,1)}, bf16[128,256]{1,0:T(8,128)(2,1)S(1)}, u32[]{:S(2)}, u32[]{:S(2)}) %collective-permute-start.1) | collective-permute-done | bytes 65568 | tf_op jit(solution)/shard_map/ppermute | solution.py:26
  13.2 2.5 %collective-permute-start.5 = (bf16[3,128,256]{2,1,0:T(8,128)(2,1)S(1)}, bf16[3,128,256]{2,1,0:T(8,128)(2,1)S(1)}, u32[]{:S(2)}, u32[]{:S(2)}) collective-permute-start(bf16[3,128,256]{2,1,0:T(8,128)(2,1)S(1)} %pad_maximum_fusion.4.refs_5_), channel_id=1, source_target_pairs={{0,6},{2,4},{4,2},{6,0},{1,7},{3,5},{5,3},{7,1},{8,14},{10,12},{12... | collective-permute-start | bytes 589832 | tf_op jit(solution)/shard_map/ppermute | solution.py:26
  16.8 5.2 %collective-permute-done.5.refs_8_ = bf16[3,128,256]{2,1,0:T(8,128)(2,1)S(1)} collective-permute-done((bf16[3,128,256]{2,1,0:T(8,128)(2,1)S(1)}, bf16[3,128,256]{2,1,0:T(8,128)(2,1)S(1)}, u32[]{:S(2)}, u32[]{:S(2)}) %collective-permute-start.5) | collective-permute-done | bytes 196640 | tf_op jit(solution)/shard_map/ppermute | solution.py:26
  21.9 2.9 %collective-permute-done.4.refs_7_ = bf16[3,128,256]{2,1,0:T(8,128)(2,1)S(1)} collective-permute-done((bf16[3,128,256]{2,1,0:T(8,128)(2,1)S(1)}, bf16[3,128,256]{2,1,0:T(8,128)(2,1)S(1)}, u32[]{:S(2)}, u32[]{:S(2)}) %collective-permute-start.4) | collective-permute-done | bytes 196640 | tf_op jit(solution)/shard_map/ppermute | solution.py:26
  25.4 1.6 %copy-done = f32[512,1024]{1,0:T(8,128)S(1)} copy-done((f32[512,1024]{1,0:T(8,128)S(1)}, f32[512,1024]{1,0:T(8,128)}, u32[]{:S(2)}) %copy-start) | copy-done | bytes 2097176
  32.6 5.0 %shard_map.187 = (bf16[64,1536]{1,0:T(8,128)(2,1)S(1)}, bf16[64,1536]{1,0:T(8,128)(2,1)S(1)}, bf16[64,1536]{1,0:T(8,128)(2,1)S(1)}, bf16[64,1536]{1,0:T(8,128)(2,1)S(1)}, bf16[2,2048,256]{2,1,0:T(8,128)(2,1)S(1)}) custom-call(bf16[768,2048]{1,0:T(8,128)(2,1)S(1)} %copy-done.10, bf16[512,256]{1,0:T(8,128)(2,1)S(1)} %copy-done.4, ...), custom_call_target="tpu_custom_call" | custom-call | flops 2214592512 | bytes 9699328 | tf_op jit(solution)/shard_map/pallas_call | solution.py:262
  37.6 1.7 %collective-permute-start.10 = (bf16[64,1536]{1,0:T(8,128)(2,1)S(1)}, bf16[64,1536]{1,0:T(8,128)(2,1)S(1)}, u32[]{:S(2)}, u32[]{:S(2)}) collective-permute-start(bf16[64,1536]{1,0:T(8,128)(2,1)S(1)} %get-tuple-element.37), channel_id=1, source_target_pairs={{0,2},{2,0},{4,6},{6,4},{1,3},{3,1},{5,7},{7,5},{8,10},{10,8},{12,... | collective-permute-start | bytes 589832 | tf_op jit(solution)/shard_map/ppermute | solution.py:26
  41.2 1.6 %collective-permute-start.30 = (bf16[128,1536]{1,0:T(8,128)(2,1)S(1)}, bf16[128,1536]{1,0:T(8,128)(2,1)S(1)}, u32[]{:S(2)}, u32[]{:S(2)}) collective-permute-start(bf16[128,1536]{1,0:T(8,128)(2,1)S(1)} %get-tuple-element.49), channel_id=1, source_target_pairs={{0,24},{8,16},{16,8},{24,0},{1,25},{9,17},{17,9},{25,1},{2,26},{10... | collective-permute-start | bytes 1179656 | tf_op jit(solution)/shard_map/ppermute | solution.py:26
  42.8 2.7 %collective-permute-done.10.refs_1_ = bf16[64,1536]{1,0:T(8,128)(2,1)S(1)} collective-permute-done((bf16[64,1536]{1,0:T(8,128)(2,1)S(1)}, bf16[64,1536]{1,0:T(8,128)(2,1)S(1)}, u32[]{:S(2)}, u32[]{:S(2)}) %collective-permute-start.10) | collective-permute-done | bytes 196640 | tf_op jit(solution)/shard_map/ppermute | solution.py:26
  46.3 3.8 %collective-permute-done.11.refs_2_ = bf16[64,1536]{1,0:T(8,128)(2,1)S(1)} collective-permute-done((bf16[64,1536]{1,0:T(8,128)(2,1)S(1)}, bf16[64,1536]{1,0:T(8,128)(2,1)S(1)}, u32[]{:S(2)}, u32[]{:S(2)}) %collective-permute-start.11) | collective-permute-done | bytes 196640 | tf_op jit(solution)/shard_map/ppermute | solution.py:26
  50.8 1.6 %collective-permute-start.14 = (bf16[16,1536]{1,0:T(8,128)(2,1)S(1)}, bf16[16,1536]{1,0:T(8,128)(2,1)S(1)}, u32[]{:S(2)}, u32[]{:S(2)}) collective-permute-start(bf16[16,1536]{1,0:T(8,128)(2,1)S(1)} %get-tuple-element.42), channel_id=1, source_target_pairs={{0,16},{8,24},{16,0},{24,8},{1,17},{9,25},{17,1},{25,9},{2,18},{10... | collective-permute-start | bytes 147464 | tf_op jit(solution)/shard_map/ppermute | solution.py:26
  52.4 4.8 %collective-permute-done.25.refs_8_ = bf16[128,1536]{1,0:T(8,128)(2,1)S(1)} collective-permute-done((bf16[128,1536]{1,0:T(8,128)(2,1)S(1)}, bf16[128,1536]{1,0:T(8,128)(2,1)S(1)}, u32[]{:S(2)}, u32[]{:S(2)}) %collective-permute-start.25) | collective-permute-done | bytes 393248 | tf_op jit(solution)/shard_map/ppermute | solution.py:26
  57.2 1.8 %collective-permute-start.15 = (bf16[16,1536]{1,0:T(8,128)(2,1)S(1)}, bf16[16,1536]{1,0:T(8,128)(2,1)S(1)}, u32[]{:S(2)}, u32[]{:S(2)}) collective-permute-start(bf16[16,1536]{1,0:T(8,128)(2,1)S(1)} %get-tuple-element.43), channel_id=1, source_target_pairs={{0,24},{8,16},{16,8},{24,0},{1,25},{9,17},{17,9},{25,1},{2,26},{10... | collective-permute-start | bytes 147464 | tf_op jit(solution)/shard_map/ppermute | solution.py:26
  59.1 18.0 %collective-permute-done.13.refs_1_ = bf16[16,1536]{1,0:T(8,128)(2,1)S(1)} collective-permute-done((bf16[16,1536]{1,0:T(8,128)(2,1)S(1)}, bf16[16,1536]{1,0:T(8,128)(2,1)S(1)}, u32[]{:S(2)}, u32[]{:S(2)}) %collective-permute-start.13) | collective-permute-done | bytes 49184 | tf_op jit(solution)/shard_map/ppermute | solution.py:26
  77.1 1.4 %collective-permute-start.27 = (bf16[128,768]{1,0:T(8,128)(2,1)S(1)}, bf16[128,768]{1,0:T(8,128)(2,1)S(1)}, u32[]{:S(2)}, u32[]{:S(2)}) collective-permute-start(bf16[128,768]{1,0:T(8,128)(2,1)S(1)} %get-tuple-element.66), channel_id=1, source_target_pairs={{0,4},{2,6},{4,0},{6,2},{1,5},{3,7},{5,1},{7,3},{8,12},{10,14},{12... | collective-permute-start | bytes 589832 | tf_op jit(solution)/shard_map/ppermute | solution.py:26
  79.4 1.7 %collective-permute-start.18 = (bf16[16,1536]{1,0:T(8,128)(2,1)S(1)}, bf16[16,1536]{1,0:T(8,128)(2,1)S(1)}, u32[]{:S(2)}, u32[]{:S(2)}) collective-permute-start(bf16[16,1536]{1,0:T(8,128)(2,1)S(1)} %shard_map.189.refs_0_), channel_id=1, source_target_pairs={{0,24},{8,16},{16,8},{24,0},{1,25},{9,17},{17,9},{25,1},{2,26},{10... | collective-permute-start | bytes 147464 | tf_op jit(solution)/shard_map/ppermute | solution.py:26
  81.2 2.8 %collective-permute-done.27.refs_10_ = bf16[128,768]{1,0:T(8,128)(2,1)S(1)} collective-permute-done((bf16[128,768]{1,0:T(8,128)(2,1)S(1)}, bf16[128,768]{1,0:T(8,128)(2,1)S(1)}, u32[]{:S(2)}, u32[]{:S(2)}) %collective-permute-start.27) | collective-permute-done | bytes 196640 | tf_op jit(solution)/shard_map/ppermute | solution.py:26
  86.2 11.5 %collective-permute-done.18.refs_3_ = bf16[16,1536]{1,0:T(8,128)(2,1)S(1)} collective-permute-done((bf16[16,1536]{1,0:T(8,128)(2,1)S(1)}, bf16[16,1536]{1,0:T(8,128)(2,1)S(1)}, u32[]{:S(2)}, u32[]{:S(2)}) %collective-permute-start.18) | collective-permute-done | bytes 49184 | tf_op jit(solution)/shard_map/ppermute | solution.py:26
  97.7 4.9 %collective-permute-done.17.refs_2_ = bf16[16,1536]{1,0:T(8,128)(2,1)S(1)} collective-permute-done((bf16[16,1536]{1,0:T(8,128)(2,1)S(1)}, bf16[16,1536]{1,0:T(8,128)(2,1)S(1)}, u32[]{:S(2)}, u32[]{:S(2)}) %collective-permute-start.17) | collective-permute-done | bytes 49184 | tf_op jit(solution)/shard_map/ppermute | solution.py:26
  102.7 4.0 %collective-permute-done.16.refs_1_ = bf16[16,1536]{1,0:T(8,128)(2,1)S(1)} collective-permute-done((bf16[16,1536]{1,0:T(8,128)(2,1)S(1)}, bf16[16,1536]{1,0:T(8,128)(2,1)S(1)}, u32[]{:S(2)}, u32[]{:S(2)}) %collective-permute-start.16) | collective-permute-done | bytes 49184 | tf_op jit(solution)/shard_map/ppermute | solution.py:26
  107.8 1.7 %collective-permute-start.21 = (bf16[64,1536]{1,0:T(8,128)(2,1)S(1)}, bf16[64,1536]{1,0:T(8,128)(2,1)S(1)}, u32[]{:S(2)}, u32[]{:S(2)}) collective-permute-start(bf16[64,1536]{1,0:T(8,128)(2,1)S(1)} %get-tuple-element.44.refs_0_), channel_id=1, source_target_pairs={{0,6},{2,4},{4,2},{6,0},{1,7},{3,5},{5,3},{7,1},{8,14},{10,12},{12... | collective-permute-start | bytes 589832 | tf_op jit(solution)/shard_map/ppermute | solution.py:26
  111.4 1.5 %collective-permute-start.28 = (bf16[2,128,768]{2,1,0:T(8,128)(2,1)S(1)}, bf16[2,128,768]{2,1,0:T(8,128)(2,1)S(1)}, u32[]{:S(2)}, u32[]{:S(2)}) collective-permute-start(bf16[2,128,768]{2,1,0:T(8,128)(2,1)S(1)} %pad_maximum_fusion), channel_id=1, source_target_pairs={{0,4},{2,6},{4,0},{6,2},{1,5},{3,7},{5,1},{7,3},{8,12},{10,14},{12... | collective-permute-start | bytes 1179656 | tf_op jit(solution)/shard_map/ppermute | solution.py:26
  112.9 2.5 %collective-permute-done.21.refs_3_ = bf16[64,1536]{1,0:T(8,128)(2,1)S(1)} collective-permute-done((bf16[64,1536]{1,0:T(8,128)(2,1)S(1)}, bf16[64,1536]{1,0:T(8,128)(2,1)S(1)}, u32[]{:S(2)}, u32[]{:S(2)}) %collective-permute-start.21) | collective-permute-done | bytes 196640 | tf_op jit(solution)/shard_map/ppermute | solution.py:26
  115.4 2.2 %collective-permute-start.29 = (bf16[2,128,768]{2,1,0:T(8,128)(2,1)S(1)}, bf16[2,128,768]{2,1,0:T(8,128)(2,1)S(1)}, u32[]{:S(2)}, u32[]{:S(2)}) collective-permute-start(bf16[2,128,768]{2,1,0:T(8,128)(2,1)S(1)} %pad_maximum_fusion.1), channel_id=1, source_target_pairs={{0,2},{2,0},{4,6},{6,4},{1,3},{3,1},{5,7},{7,5},{8,10},{10,8},{12,... | collective-permute-start | bytes 1179656 | tf_op jit(solution)/shard_map/ppermute | solution.py:26
  118.8 1.5 %collective-permute-start.33 = (bf16[2,128,768]{2,1,0:T(8,128)(2,1)S(1)}, bf16[2,128,768]{2,1,0:T(8,128)(2,1)S(1)}, u32[]{:S(2)}, u32[]{:S(2)}) collective-permute-start(bf16[2,128,768]{2,1,0:T(8,128)(2,1)S(1)} %pad_maximum_fusion.2), channel_id=1, source_target_pairs={{0,4},{2,6},{4,0},{6,2},{1,5},{3,7},{5,1},{7,3},{8,12},{10,14},{12... | collective-permute-start | bytes 1179656 | tf_op jit(solution)/shard_map/ppermute | solution.py:26
  124.2 3.0 %collective-permute-done.28.refs_11_ = bf16[2,128,768]{2,1,0:T(8,128)(2,1)S(1)} collective-permute-done((bf16[2,128,768]{2,1,0:T(8,128)(2,1)S(1)}, bf16[2,128,768]{2,1,0:T(8,128)(2,1)S(1)}, u32[]{:S(2)}, u32[]{:S(2)}) %collective-permute-start.28) | collective-permute-done | bytes 393248 | tf_op jit(solution)/shard_map/ppermute | solution.py:26
  127.2 1.6 %collective-permute-done.29.refs_12_ = bf16[2,128,768]{2,1,0:T(8,128)(2,1)S(1)} collective-permute-done((bf16[2,128,768]{2,1,0:T(8,128)(2,1)S(1)}, bf16[2,128,768]{2,1,0:T(8,128)(2,1)S(1)}, u32[]{:S(2)}, u32[]{:S(2)}) %collective-permute-start.29) | collective-permute-done | bytes 393248 | tf_op jit(solution)/shard_map/ppermute | solution.py:26
  128.8 4.6 %collective-permute-done.33.refs_16_ = bf16[2,128,768]{2,1,0:T(8,128)(2,1)S(1)} collective-permute-done((bf16[2,128,768]{2,1,0:T(8,128)(2,1)S(1)}, bf16[2,128,768]{2,1,0:T(8,128)(2,1)S(1)}, u32[]{:S(2)}, u32[]{:S(2)}) %collective-permute-start.33) | collective-permute-done | bytes 393248 | tf_op jit(solution)/shard_map/ppermute | solution.py:26
  133.4 5.5 %shard_map.194 = (f32[512,512]{1,0:T(8,128)}, f32[512,1024]{1,0:T(8,128)}, f32[512,512]{1,0:T(8,128)}, f32[512,1024]{1,0:T(8,128)}, bf16[2048,512]{1,0:T(8,128)(2,1)}, /*index=5*/bf16[2048,1024]{1,0:T(8,128)(2,1)}) custom-call(bf16[2,2048,256]{2,1,0:T(8,128)(2,1)S(1)} %get-tuple-element.35.fac.refs_0_, bf16[256,1536]{1,0:T(8,128)(2,1)S(1)} %get-tuple-element.45.refs_1_, ...), custom_call_target="tpu_custom_call" | custom-call | flops 1610612736 | bytes 22020096 | tf_op jit(solution)/shard_map/pallas_call | solution.py:302
  (80 shorter events, 22.6 us)
Async XLA Ops:
  2.2 7.9 %collective-permute-start.2 = (bf16[128,256]{1,0:T(8,128)(2,1)}, bf16[128,256]{1,0:T(8,128)(2,1)S(1)}, u32[]{:S(2)}, u32[]{:S(2)}) collective-permute-start(bf16[128,256]{1,0:T(8,128)(2,1)} %shard_map.186), channel_id=1, source_target_pairs={{0,24},{8,16},{16,8},{24,0},{1,25},{9,17},{17,9},{25,1},{2,26},{10... | collective-permute-start | bytes 196616 | tf_op jit(solution)/shard_map/ppermute | solution.py:26
  7.4 5.8 %collective-permute-start.1 = (bf16[128,256]{1,0:T(8,128)(2,1)}, bf16[128,256]{1,0:T(8,128)(2,1)S(1)}, u32[]{:S(2)}, u32[]{:S(2)}) collective-permute-start(bf16[128,256]{1,0:T(8,128)(2,1)} %shard_map.186), channel_id=1, source_target_pairs={{0,16},{8,24},{16,0},{24,8},{1,17},{9,25},{17,1},{25,9},{2,18},{10... | collective-permute-start | bytes 196616 | tf_op jit(solution)/shard_map/ppermute | solution.py:26
  7.4 5.8 %collective-permute-start = (bf16[128,256]{1,0:T(8,128)(2,1)}, bf16[128,256]{1,0:T(8,128)(2,1)S(1)}, u32[]{:S(2)}, u32[]{:S(2)}) collective-permute-start(bf16[128,256]{1,0:T(8,128)(2,1)} %shard_map.186), channel_id=1, source_target_pairs={{0,8},{8,0},{16,24},{24,16},{1,9},{9,1},{17,25},{25,17},{2,10},{10... | collective-permute-start | bytes 196616 | tf_op jit(solution)/shard_map/ppermute | solution.py:26
  13.2 8.7 %collective-permute-start.5 = (bf16[3,128,256]{2,1,0:T(8,128)(2,1)S(1)}, bf16[3,128,256]{2,1,0:T(8,128)(2,1)S(1)}, u32[]{:S(2)}, u32[]{:S(2)}) collective-permute-start(bf16[3,128,256]{2,1,0:T(8,128)(2,1)S(1)} %pad_maximum_fusion.4.refs_5_), channel_id=1, source_target_pairs={{0,6},{2,4},{4,2},{6,0},{1,7},{3,5},{5,3},{7,1},{8,14},{10,12},{12... | collective-permute-start | bytes 589832 | tf_op jit(solution)/shard_map/ppermute | solution.py:26
  15.7 9.1 %collective-permute-start.4 = (bf16[3,128,256]{2,1,0:T(8,128)(2,1)S(1)}, bf16[3,128,256]{2,1,0:T(8,128)(2,1)S(1)}, u32[]{:S(2)}, u32[]{:S(2)}) collective-permute-start(bf16[3,128,256]{2,1,0:T(8,128)(2,1)S(1)} %pad_maximum_fusion.4.refs_5_), channel_id=1, source_target_pairs={{0,4},{2,6},{4,0},{6,2},{1,5},{3,7},{5,1},{7,3},{8,12},{10,14},{12... | collective-permute-start | bytes 589832 | tf_op jit(solution)/shard_map/ppermute | solution.py:26
  16.2 8.8 %collective-permute-start.3 = (bf16[3,128,256]{2,1,0:T(8,128)(2,1)S(1)}, bf16[3,128,256]{2,1,0:T(8,128)(2,1)S(1)}, u32[]{:S(2)}, u32[]{:S(2)}) collective-permute-start(bf16[3,128,256]{2,1,0:T(8,128)(2,1)S(1)} %pad_maximum_fusion.4.refs_5_), channel_id=1, source_target_pairs={{0,2},{2,0},{4,6},{6,4},{1,3},{3,1},{5,7},{7,5},{8,10},{10,8},{12,... | collective-permute-start | bytes 589832 | tf_op jit(solution)/shard_map/ppermute | solution.py:26
  16.8 12.3 %collective-permute-start.6 = (bf16[3,128,256]{2,1,0:T(8,128)(2,1)S(1)}, bf16[3,128,256]{2,1,0:T(8,128)(2,1)S(1)}, u32[]{:S(2)}, u32[]{:S(2)}) collective-permute-start(bf16[3,128,256]{2,1,0:T(8,128)(2,1)S(1)} %pad_maximum_fusion.4.refs_5_), channel_id=1, source_target_pairs={{0,1},{1,0},{2,3},{3,2},{4,5},{5,4},{6,7},{7,6},{8,9},{9,8},{10,11... | collective-permute-start | bytes 589832 | tf_op jit(solution)/shard_map/ppermute | solution.py:26
  21.9 7.1 %collective-permute-start.9 = (bf16[3,128,256]{2,1,0:T(8,128)(2,1)S(1)}, bf16[3,128,256]{2,1,0:T(8,128)(2,1)S(1)}, u32[]{:S(2)}, u32[]{:S(2)}) collective-permute-start(bf16[3,128,256]{2,1,0:T(8,128)(2,1)S(1)} %collective-permute-done.5.refs_8_), channel_id=1, source_target_pairs={{0,1},{1,0},{2,3},{3,2},{4,5},{5,4},{6,7},{7,6},{8,9},{9,8},{10,11... | collective-permute-start | bytes 589832 | tf_op jit(solution)/shard_map/ppermute | solution.py:26
  24.9 4.2 %collective-permute-start.8 = (bf16[3,128,256]{2,1,0:T(8,128)(2,1)S(1)}, bf16[3,128,256]{2,1,0:T(8,128)(2,1)S(1)}, u32[]{:S(2)}, u32[]{:S(2)}) collective-permute-start(bf16[3,128,256]{2,1,0:T(8,128)(2,1)S(1)} %collective-permute-done.4.refs_7_), channel_id=1, source_target_pairs={{0,1},{1,0},{2,3},{3,2},{4,5},{5,4},{6,7},{7,6},{8,9},{9,8},{10,11... | collective-permute-start | bytes 589832 | tf_op jit(solution)/shard_map/ppermute | solution.py:26
  28.6 28.6 %collective-permute-start.25 = (bf16[128,1536]{1,0:T(8,128)(2,1)S(1)}, bf16[128,1536]{1,0:T(8,128)(2,1)S(1)}, u32[]{:S(2)}, u32[]{:S(2)}) collective-permute-start(bf16[128,1536]{1,0:T(8,128)(2,1)S(1)} %get-tuple-element.49), channel_id=1, source_target_pairs={{0,16},{8,24},{16,0},{24,8},{1,17},{9,25},{17,1},{25,9},{2,18},{10... | collective-permute-start | bytes 1179656 | tf_op jit(solution)/shard_map/ppermute | solution.py:26
  37.6 7.8 %collective-permute-start.10 = (bf16[64,1536]{1,0:T(8,128)(2,1)S(1)}, bf16[64,1536]{1,0:T(8,128)(2,1)S(1)}, u32[]{:S(2)}, u32[]{:S(2)}) collective-permute-start(bf16[64,1536]{1,0:T(8,128)(2,1)S(1)} %get-tuple-element.37), channel_id=1, source_target_pairs={{0,2},{2,0},{4,6},{6,4},{1,3},{3,1},{5,7},{7,5},{8,10},{10,8},{12,... | collective-permute-start | bytes 589832 | tf_op jit(solution)/shard_map/ppermute | solution.py:26
  39.3 10.8 %collective-permute-start.11 = (bf16[64,1536]{1,0:T(8,128)(2,1)S(1)}, bf16[64,1536]{1,0:T(8,128)(2,1)S(1)}, u32[]{:S(2)}, u32[]{:S(2)}) collective-permute-start(bf16[64,1536]{1,0:T(8,128)(2,1)S(1)} %get-tuple-element.38), channel_id=1, source_target_pairs={{0,4},{2,6},{4,0},{6,2},{1,5},{3,7},{5,1},{7,3},{8,12},{10,14},{12... | collective-permute-start | bytes 589832 | tf_op jit(solution)/shard_map/ppermute | solution.py:26
  40.0 10.1 %collective-permute-start.12 = (bf16[64,1536]{1,0:T(8,128)(2,1)S(1)}, bf16[64,1536]{1,0:T(8,128)(2,1)S(1)}, u32[]{:S(2)}, u32[]{:S(2)}) collective-permute-start(bf16[64,1536]{1,0:T(8,128)(2,1)S(1)} %get-tuple-element.39), channel_id=1, source_target_pairs={{0,6},{2,4},{4,2},{6,0},{1,7},{3,5},{5,3},{7,1},{8,14},{10,12},{12... | collective-permute-start | bytes 589832 | tf_op jit(solution)/shard_map/ppermute | solution.py:26
  41.2 38.2 %collective-permute-start.30 = (bf16[128,1536]{1,0:T(8,128)(2,1)S(1)}, bf16[128,1536]{1,0:T(8,128)(2,1)S(1)}, u32[]{:S(2)}, u32[]{:S(2)}) collective-permute-start(bf16[128,1536]{1,0:T(8,128)(2,1)S(1)} %get-tuple-element.49), channel_id=1, source_target_pairs={{0,24},{8,16},{16,8},{24,0},{1,25},{9,17},{17,9},{25,1},{2,26},{10... | collective-permute-start | bytes 1179656 | tf_op jit(solution)/shard_map/ppermute | solution.py:26
  45.5 66.0 %collective-permute-start.23 = (bf16[256,1536]{1,0:T(8,128)(2,1)S(1)}, bf16[256,1536]{1,0:T(8,128)(2,1)S(1)}, u32[]{:S(2)}, u32[]{:S(2)}) collective-permute-start(bf16[256,1536]{1,0:T(8,128)(2,1)S(1)} %get-tuple-element.47), channel_id=1, source_target_pairs={{0,8},{8,0},{16,24},{24,16},{1,9},{9,1},{17,25},{25,17},{2,10},{10... | collective-permute-start | bytes 2359304 | tf_op jit(solution)/shard_map/ppermute | solution.py:26
  50.3 26.8 %collective-permute-start.13 = (bf16[16,1536]{1,0:T(8,128)(2,1)S(1)}, bf16[16,1536]{1,0:T(8,128)(2,1)S(1)}, u32[]{:S(2)}, u32[]{:S(2)}) collective-permute-start(bf16[16,1536]{1,0:T(8,128)(2,1)S(1)} %get-tuple-element.41), channel_id=1, source_target_pairs={{0,8},{8,0},{16,24},{24,16},{1,9},{9,1},{17,25},{25,17},{2,10},{10... | collective-permute-start | bytes 147464 | tf_op jit(solution)/shard_map/ppermute | solution.py:26
  50.8 26.3 %collective-permute-start.14 = (bf16[16,1536]{1,0:T(8,128)(2,1)S(1)}, bf16[16,1536]{1,0:T(8,128)(2,1)S(1)}, u32[]{:S(2)}, u32[]{:S(2)}) collective-permute-start(bf16[16,1536]{1,0:T(8,128)(2,1)S(1)} %get-tuple-element.42), channel_id=1, source_target_pairs={{0,16},{8,24},{16,0},{24,8},{1,17},{9,25},{17,1},{25,9},{2,18},{10... | collective-permute-start | bytes 147464 | tf_op jit(solution)/shard_map/ppermute | solution.py:26
  57.2 21.3 %collective-permute-start.15 = (bf16[16,1536]{1,0:T(8,128)(2,1)S(1)}, bf16[16,1536]{1,0:T(8,128)(2,1)S(1)}, u32[]{:S(2)}, u32[]{:S(2)}) collective-permute-start(bf16[16,1536]{1,0:T(8,128)(2,1)S(1)} %get-tuple-element.43), channel_id=1, source_target_pairs={{0,24},{8,16},{16,8},{24,0},{1,25},{9,17},{17,9},{25,1},{2,26},{10... | collective-permute-start | bytes 147464 | tf_op jit(solution)/shard_map/ppermute | solution.py:26
  77.1 45.8 %collective-permute-start.24 = (bf16[256,1536]{1,0:T(8,128)(2,1)S(1)}, bf16[256,1536]{1,0:T(8,128)(2,1)S(1)}, u32[]{:S(2)}, u32[]{:S(2)}) collective-permute-start(bf16[256,1536]{1,0:T(8,128)(2,1)S(1)} %get-tuple-element.48), channel_id=1, source_target_pairs={{0,8},{8,0},{16,24},{24,16},{1,9},{9,1},{17,25},{25,17},{2,10},{10... | collective-permute-start | bytes 2359304 | tf_op jit(solution)/shard_map/ppermute | solution.py:26
  77.1 6.8 %collective-permute-start.27 = (bf16[128,768]{1,0:T(8,128)(2,1)S(1)}, bf16[128,768]{1,0:T(8,128)(2,1)S(1)}, u32[]{:S(2)}, u32[]{:S(2)}) collective-permute-start(bf16[128,768]{1,0:T(8,128)(2,1)S(1)} %get-tuple-element.66), channel_id=1, source_target_pairs={{0,4},{2,6},{4,0},{6,2},{1,5},{3,7},{5,1},{7,3},{8,12},{10,14},{12... | collective-permute-start | bytes 589832 | tf_op jit(solution)/shard_map/ppermute | solution.py:26
  78.6 6.8 %collective-permute-start.26 = (bf16[128,768]{1,0:T(8,128)(2,1)S(1)}, bf16[128,768]{1,0:T(8,128)(2,1)S(1)}, u32[]{:S(2)}, u32[]{:S(2)}) collective-permute-start(bf16[128,768]{1,0:T(8,128)(2,1)S(1)} %get-tuple-element.67), channel_id=1, source_target_pairs={{0,2},{2,0},{4,6},{6,4},{1,3},{3,1},{5,7},{7,5},{8,10},{10,8},{12,... | collective-permute-start | bytes 589832 | tf_op jit(solution)/shard_map/ppermute | solution.py:26
  79.4 18.2 %collective-permute-start.18 = (bf16[16,1536]{1,0:T(8,128)(2,1)S(1)}, bf16[16,1536]{1,0:T(8,128)(2,1)S(1)}, u32[]{:S(2)}, u32[]{:S(2)}) collective-permute-start(bf16[16,1536]{1,0:T(8,128)(2,1)S(1)} %shard_map.189.refs_0_), channel_id=1, source_target_pairs={{0,24},{8,16},{16,8},{24,0},{1,25},{9,17},{17,9},{25,1},{2,26},{10... | collective-permute-start | bytes 147464 | tf_op jit(solution)/shard_map/ppermute | solution.py:26
  84.0 25.5 %collective-permute-start.32 = (bf16[128,768]{1,0:T(8,128)(2,1)S(1)}, bf16[128,768]{1,0:T(8,128)(2,1)S(1)}, u32[]{:S(2)}, u32[]{:S(2)}) collective-permute-start(bf16[128,768]{1,0:T(8,128)(2,1)S(1)} %get-tuple-element.62), channel_id=1, source_target_pairs={{0,4},{2,6},{4,0},{6,2},{1,5},{3,7},{5,1},{7,3},{8,12},{10,14},{12... | collective-permute-start | bytes 589832 | tf_op jit(solution)/shard_map/ppermute | solution.py:26
  85.4 25.4 %collective-permute-start.31 = (bf16[128,768]{1,0:T(8,128)(2,1)S(1)}, bf16[128,768]{1,0:T(8,128)(2,1)S(1)}, u32[]{:S(2)}, u32[]{:S(2)}) collective-permute-start(bf16[128,768]{1,0:T(8,128)(2,1)S(1)} %get-tuple-element.63), channel_id=1, source_target_pairs={{0,2},{2,0},{4,6},{6,4},{1,3},{3,1},{5,7},{7,5},{8,10},{10,8},{12,... | collective-permute-start | bytes 589832 | tf_op jit(solution)/shard_map/ppermute | solution.py:26
  97.7 5.0 %collective-permute-start.17 = (bf16[16,1536]{1,0:T(8,128)(2,1)S(1)}, bf16[16,1536]{1,0:T(8,128)(2,1)S(1)}, u32[]{:S(2)}, u32[]{:S(2)}) collective-permute-start(bf16[16,1536]{1,0:T(8,128)(2,1)S(1)} %shard_map.189.refs_0_), channel_id=1, source_target_pairs={{0,16},{8,24},{16,0},{24,8},{1,17},{9,25},{17,1},{25,9},{2,18},{10... | collective-permute-start | bytes 147464 | tf_op jit(solution)/shard_map/ppermute | solution.py:26
  107.8 7.6 %collective-permute-start.21 = (bf16[64,1536]{1,0:T(8,128)(2,1)S(1)}, bf16[64,1536]{1,0:T(8,128)(2,1)S(1)}, u32[]{:S(2)}, u32[]{:S(2)}) collective-permute-start(bf16[64,1536]{1,0:T(8,128)(2,1)S(1)} %get-tuple-element.44.refs_0_), channel_id=1, source_target_pairs={{0,6},{2,4},{4,2},{6,0},{1,7},{3,5},{5,3},{7,1},{8,14},{10,12},{12... | collective-permute-start | bytes 589832 | tf_op jit(solution)/shard_map/ppermute | solution.py:26
  109.5 9.3 %collective-permute-start.20 = (bf16[64,1536]{1,0:T(8,128)(2,1)S(1)}, bf16[64,1536]{1,0:T(8,128)(2,1)S(1)}, u32[]{:S(2)}, u32[]{:S(2)}) collective-permute-start(bf16[64,1536]{1,0:T(8,128)(2,1)S(1)} %get-tuple-element.44.refs_0_), channel_id=1, source_target_pairs={{0,4},{2,6},{4,0},{6,2},{1,5},{3,7},{5,1},{7,3},{8,12},{10,14},{12... | collective-permute-start | bytes 589832 | tf_op jit(solution)/shard_map/ppermute | solution.py:26
  110.8 9.6 %collective-permute-start.19 = (bf16[64,1536]{1,0:T(8,128)(2,1)S(1)}, bf16[64,1536]{1,0:T(8,128)(2,1)S(1)}, u32[]{:S(2)}, u32[]{:S(2)}) collective-permute-start(bf16[64,1536]{1,0:T(8,128)(2,1)S(1)} %get-tuple-element.44.refs_0_), channel_id=1, source_target_pairs={{0,2},{2,0},{4,6},{6,4},{1,3},{3,1},{5,7},{7,5},{8,10},{10,8},{12,... | collective-permute-start | bytes 589832 | tf_op jit(solution)/shard_map/ppermute | solution.py:26
  111.4 15.8 %collective-permute-start.28 = (bf16[2,128,768]{2,1,0:T(8,128)(2,1)S(1)}, bf16[2,128,768]{2,1,0:T(8,128)(2,1)S(1)}, u32[]{:S(2)}, u32[]{:S(2)}) collective-permute-start(bf16[2,128,768]{2,1,0:T(8,128)(2,1)S(1)} %pad_maximum_fusion), channel_id=1, source_target_pairs={{0,4},{2,6},{4,0},{6,2},{1,5},{3,7},{5,1},{7,3},{8,12},{10,14},{12... | collective-permute-start | bytes 1179656 | tf_op jit(solution)/shard_map/ppermute | solution.py:26
  115.4 13.4 %collective-permute-start.29 = (bf16[2,128,768]{2,1,0:T(8,128)(2,1)S(1)}, bf16[2,128,768]{2,1,0:T(8,128)(2,1)S(1)}, u32[]{:S(2)}, u32[]{:S(2)}) collective-permute-start(bf16[2,128,768]{2,1,0:T(8,128)(2,1)S(1)} %pad_maximum_fusion.1), channel_id=1, source_target_pairs={{0,2},{2,0},{4,6},{6,4},{1,3},{3,1},{5,7},{7,5},{8,10},{10,8},{12,... | collective-permute-start | bytes 1179656 | tf_op jit(solution)/shard_map/ppermute | solution.py:26
  118.8 14.6 %collective-permute-start.33 = (bf16[2,128,768]{2,1,0:T(8,128)(2,1)S(1)}, bf16[2,128,768]{2,1,0:T(8,128)(2,1)S(1)}, u32[]{:S(2)}, u32[]{:S(2)}) collective-permute-start(bf16[2,128,768]{2,1,0:T(8,128)(2,1)S(1)} %pad_maximum_fusion.2), channel_id=1, source_target_pairs={{0,4},{2,6},{4,0},{6,2},{1,5},{3,7},{5,1},{7,3},{8,12},{10,14},{12... | collective-permute-start | bytes 1179656 | tf_op jit(solution)/shard_map/ppermute | solution.py:26
  120.4 13.0 %collective-permute-start.34 = (bf16[2,128,768]{2,1,0:T(8,128)(2,1)S(1)}, bf16[2,128,768]{2,1,0:T(8,128)(2,1)S(1)}, u32[]{:S(2)}, u32[]{:S(2)}) collective-permute-start(bf16[2,128,768]{2,1,0:T(8,128)(2,1)S(1)} %pad_maximum_fusion.3), channel_id=1, source_target_pairs={{0,2},{2,0},{4,6},{6,4},{1,3},{3,1},{5,7},{7,5},{8,10},{10,8},{12,... | collective-permute-start | bytes 1179656 | tf_op jit(solution)/shard_map/ppermute | solution.py:26
  (16 other events, 315.4 us)
where the time goes:
time: 139 us
  waiting for transfers between devices  80.3 us (58%)
  starting transfers between devices  35.5 us (26%)
  Pallas kernels  15.6 us (11%)
  local copies, waits for them, and re-layouts  6.51 us (5%)
    ppermute x35, waiting for transfers between devices, swap(): return lax.ppermute(x, axis, [(i, i ^ k) for i in range(n)])  80.3 us
    ppermute x35, starting transfers between devices, swap(): return lax.ppermute(x, axis, [(i, i ^ k) for i in range(n)])  35.5 us
    unnamed x26, local copies, waits for them, and re-layouts  6.4 us
    pallas_call x1, Pallas kernels, exchange(): call(functools.partial(final_body, nf, nr, nt), [S((dl, nq), F32), S((dl,...  5.47 us
    pallas_call x1, Pallas kernels, exchange(): call(functools.partial(project_body, nf, nr), [S((h, nc), BF)] * nr + [S(...  5 us
  transfers between devices with their start and end apart: 35, of which 20 were waited for; matrix products, arithmetic and copies ran while one was open for 0% of the time, Pallas kernels for 6%

commit v1 on v0

--- a/solution.py
+++ b/solution.py
@@ -21,26 +21,23 @@
 ANY = pl.BlockSpec(memory_space=pltpu.HBM)
 TILE = 16
 
-
 def swap(x, axis, n, k):
     return lax.ppermute(x, axis, [(i, i ^ k) for i in range(n)])
 
-
 def rows_at(block, height):
     return pl.ds(pl.multiple_of(block * height, height), height)
 
-
-def call(body, outs, n_in, scratch=(), limit=8, flops=0, nbytes=0, in_specs=None, out_specs=None):
+def call(body, outs, n_in, scratch=(), limit=8, flops=0, nbytes=0, in_specs=None, out_specs=None, aliases=None):
     return pl.pallas_call(
         body,
         out_shape=outs,
         in_specs=in_specs or [VMEM] * n_in,
         out_specs=out_specs or [VMEM] * len(outs),
         scratch_shapes=list(scratch),
+        input_output_aliases=aliases or {},
         compiler_params=pltpu.CompilerParams(vmem_limit_bytes=limit << 20),
         cost_estimate=pl.CostEstimate(flops=flops, bytes_accessed=nbytes, transcendentals=0),
     )
-
 
 def first_body(nr, fq, fv, out, sem):
     r, t = lax.axis_index("rep"), lax.axis_index("tp")
@@ -52,7 +49,6 @@
             move = pltpu.make_async_copy(ref.at[here, :], out, sem)
             move.start()
             move.wait()
-
 
 def pack_body(nr, wq_h, wv_h, quarter, low, high, wq, wv, sem):
     r = lax.axis_index("rep")
@@ -66,15 +62,11 @@
         out[:, :nq] = wq[here, :].astype(BF)
         out[:, nq:] = wv[here, :].astype(BF)
 
-
-def project_body(nf, nr, *refs):
-    x, fq, fv, cq_h, cv_h = refs[:5]
-    mine, other = refs[5 : 5 + nr], refs[5 + nr : 5 + 2 * nr]
-    outs = refs[5 + 2 * nr : 5 + 3 * nr]
-    fac, part, cq, cv, sem = refs[5 + 3 * nr :]
-    loads = [pltpu.make_async_copy(cq_h, cq, sem.at[0]), pltpu.make_async_copy(cv_h, cv, sem.at[1])]
-    for c in loads:
-        c.start()
+def project_body(nf, nr, nq, *refs):
+    x, fq, fv, cot = refs[:4]
+    mine, other = refs[4 : 4 + nr], refs[4 + nr : 4 + 2 * nr]
+    outs = refs[4 + 2 * nr : 4 + 3 * nr]
+    fac, part = refs[4 + 3 * nr :]
     f, r, t = lax.axis_index("fs"), lax.axis_index("rep"), lax.axis_index("tp")
     dl = fq.shape[0]
     piece = dl // nr
@@ -85,18 +77,14 @@
             here = rows_at((f ^ k) * nr + (r ^ j), piece)
             fac[t, here, :] = mine[j][k - 1]
             fac[1 - t, here, :] = other[j][k - 1]
-    nq = cq.shape[1]
     dims = (((0,), (0,)), ((), ()))
     yq = jnp.dot(x[...], fac[0], preferred_element_type=F32).astype(BF)
-    for c in loads:
-        c.wait()
-    part[:, :nq] = lax.dot_general(yq, cq[...], dims, preferred_element_type=F32).astype(BF)
+    part[:, :nq] = lax.dot_general(yq, cot[:, :nq], dims, preferred_element_type=F32).astype(BF)
     yv = jnp.dot(x[...], fac[1], preferred_element_type=F32).astype(BF)
-    part[:, nq:] = lax.dot_general(yv, cv[...], dims, preferred_element_type=F32).astype(BF)
+    part[:, nq:] = lax.dot_general(yv, cot[:, nq:], dims, preferred_element_type=F32).astype(BF)
     h = part.shape[0] // nr
     for j in range(nr):
         outs[j][...] = part[rows_at(r ^ j, h), :]
-
 
 def plane_sum_body(nf, nr, *refs):
     ins, own, rest, acc = refs[:nr], refs[nr], refs[nr + 1 : nr + nf], refs[nr + nf]
@@ -110,13 +98,11 @@
     for k in range(1, nf):
         rest[k - 1][...] = acc[rows_at(f ^ k, h), :].astype(BF)
 
-
 def line_sum_body(nf, *refs):
     total = refs[0][...]
     for ref in refs[1:nf]:
         total += ref[...].astype(F32)
     refs[nf][...] = total.astype(BF)
-
 
 def moments_body(nf, nq, *refs):
     ins = refs[:nf]
@@ -137,12 +123,10 @@
         so[...] = sn
         ratio[:, cols] = (fn / (jnp.sqrt(sn) + EPS_RATIO)).astype(BF)
 
-
 def gram_body(fac, out):
     dims = (((0,), (0,)), ((), ()))
     for s in range(2):
         out[s] = lax.dot_general(fac[s], fac[s], dims, preferred_element_type=F32)
-
 
 def total_body(nr, nq, *refs):
     ins, gram, ratio, total = refs[:nr], refs[nr], refs[nr + 1], refs[nr + 2]
@@ -161,40 +145,63 @@
             acc = term if acc is None else acc + term
         total[rows_at(s, 8), :] = jnp.broadcast_to(jnp.sum(acc * z.astype(F32), keepdims=True), (8, 128))
 
-
-def final_body(nf, nr, nt, *refs):
+def scales(fac, tot, tot_in, nq, nv, nt):
+    both = tot[...] + tot_in[...]
+    d = fac.shape[1]
+    return (
+        lax.rsqrt(both[0:1, 0:1] / (d * nq * nt) + EPS_NORM),
+        lax.rsqrt(both[8:9, 0:1] / (d * nv * nt) + EPS_NORM),
+    )
+
+def step_rows(fac, ratio, raw, here, nq, scale):
+    for s, cols in ((0, slice(None, nq)), (1, slice(nq, None))):
+        raw[:, cols] = jnp.dot(fac[s, here, :], ratio[:, cols], preferred_element_type=F32) * scale[s]
+
+def put(raw, qc, vc, slot, here, cols, w):
+    nq = qc.shape[2]
+    value = (w.astype(F32) - RATE * raw[here, cols]).astype(BF)
+    split = min(max(nq - cols.start, 0), cols.stop - cols.start)
+    if split:
+        qc[slot, here, cols.start : cols.start + split] = value[:, :split]
+    if split < cols.stop - cols.start:
+        vc[slot, here, cols.start + split - nq : cols.stop - nq] = value[:, split:]
+
+def put_far(raw, qc, vc, slot, pieces):
+    own_z, xa, yb, ya, xb = pieces
+    r = lax.axis_index("rep")
+    piece, nc = own_z.shape
+    put(raw, qc, vc, slot, rows_at(r, piece), slice(0, nc), own_z[...])
+    left, right = slice(0, nc // 2), slice(nc // 2, nc)
+    for cols, group in ((left, (xa[...], ya[0], ya[1])), (right, (xb[0], yb[...], xb[1]))):
+        for m, w in enumerate(group):
+            put(raw, qc, vc, slot, rows_at(r ^ (m + 1), piece), cols, w)
+
+def send(qc, vc, qc_h, vc_h, slot, here, sem, at):
+    moves = [
+        pltpu.make_async_copy(qc.at[slot], qc_h.at[here, :], sem.at[at]),
+        pltpu.make_async_copy(vc.at[slot], vc_h.at[here, :], sem.at[at + 1]),
+    ]
+    for c in moves:
+        c.start()
+    return moves
+
+def final_body(nt, *refs):
     fac, ratio, tot, tot_in, wq, wv = refs[:6]
     near, far = refs[6:8], refs[8:-14]
     qd_h, vd_h, qm_h, vm_h, qc_h, vc_h, raw, qd, vd, qm, vm, qc, vc, sem = refs[-14:]
-    f, r = lax.axis_index("fs"), lax.axis_index("rep")
+    f = lax.axis_index("fs")
     dl, nq, nv = wq.shape[0], wq.shape[1], wv.shape[1]
-    half = (nq + nv) // 2
-    d = dl * nf
-    piece = dl // nr
-    both = tot[...] + tot_in[...]
-    sq = lax.rsqrt(both[0:1, 0:1] / (d * nq * nt) + EPS_NORM)
-    sv = lax.rsqrt(both[8:9, 0:1] / (d * nv * nt) + EPS_NORM)
+    scale = scales(fac, tot, tot_in, nq, nv, nt)
     stores = []
-
-    def put(k, here, cols, w):
-        value = (w.astype(F32) - RATE * raw[here, cols]).astype(BF)
-        split = min(max(nq - cols.start, 0), cols.stop - cols.start)
-        if split:
-            qc[k, here, cols.start : cols.start + split] = value[:, :split]
-        if split < cols.stop - cols.start:
-            vc[k, here, cols.start + split - nq : cols.stop - nq] = value[:, split:]
-
-    left, right, whole = slice(0, half), slice(half, 2 * half), slice(0, 2 * half)
-    for k in range(nf):
-        raw[:, :nq] = jnp.dot(fac[0, rows_at(f ^ k, dl), :], ratio[:, :nq], preferred_element_type=F32) * sq
-        raw[:, nq:] = jnp.dot(fac[1, rows_at(f ^ k, dl), :], ratio[:, nq:], preferred_element_type=F32) * sv
+    for k in range(2 + len(far) // 5):
+        step_rows(fac, ratio, raw, rows_at(f ^ k, dl), nq, scale)
         if k == 0:
             qd[...] = raw[:, :nq]
             vd[...] = raw[:, nq:]
             qm[...] = wq[...] - RATE * raw[:, :nq]
             vm[...] = wv[...] - RATE * raw[:, nq:]
-            put(0, slice(None), slice(0, nq), wq[...].astype(BF))
-            put(0, slice(None), slice(nq, nq + nv), wv[...].astype(BF))
+            put(raw, qc, vc, 0, slice(None), slice(0, nq), wq[...].astype(BF))
+            put(raw, qc, vc, 0, slice(None), slice(nq, nq + nv), wv[...].astype(BF))
             stores += [
                 pltpu.make_async_copy(qd, qd_h, sem.at[0]),
                 pltpu.make_async_copy(vd, vd_h, sem.at[1]),
@@ -204,24 +211,24 @@
             for c in stores:
                 c.start()
         elif k == 1:
-            put(1, slice(0, dl // 2), whole, near[0][...])
-            put(1, slice(dl // 2, dl), whole, near[1][...])
+            put(raw, qc, vc, 1, slice(0, dl // 2), slice(0, nq + nv), near[0][...])
+            put(raw, qc, vc, 1, slice(dl // 2, dl), slice(0, nq + nv), near[1][...])
         else:
-            own_z, xa, yb, ya, xb = far[5 * (k - 2) : 5 * (k - 1)]
-            put(k, rows_at(r, piece), whole, own_z[...])
-            for cols, group in ((left, (xa[...], ya[0], ya[1])), (right, (xb[0], yb[...], xb[1]))):
-                for m, w in enumerate(group):
-                    put(k, rows_at(r ^ (m + 1), piece), cols, w)
-        new = [
-            pltpu.make_async_copy(qc.at[k], qc_h.at[rows_at(f ^ k, dl), :], sem.at[4 + 2 * k]),
-            pltpu.make_async_copy(vc.at[k], vc_h.at[rows_at(f ^ k, dl), :], sem.at[5 + 2 * k]),
-        ]
-        for c in new:
-            c.start()
-        stores += new
+            put_far(raw, qc, vc, k, far[5 * (k - 2) : 5 * (k - 1)])
+        stores += send(qc, vc, qc_h, vc_h, k, rows_at(f ^ k, dl), sem, 4 + 2 * k)
     for c in stores:
         c.wait()
 
+def last_body(k, nt, *refs):
+    fac, ratio, tot, tot_in = refs[:4]
+    far, (qc_h, vc_h, raw, qc, vc, sem) = refs[4:9], refs[11:]
+    f = lax.axis_index("fs")
+    dl, nq, nv = qc.shape[1], qc.shape[2], vc.shape[2]
+    here = rows_at(f ^ k, dl)
+    step_rows(fac, ratio, raw, here, nq, scales(fac, tot, tot_in, nq, nv, nt))
+    put_far(raw, qc, vc, 0, far)
+    for c in send(qc, vc, qc_h, vc_h, 0, here, sem, 0):
+        c.wait()
 
 def exchange(nf, nr, nt, xs, cq, cv, wq, wv, fq, fv, q1, q2, v1, v2):
     S = jax.ShapeDtypeStruct
@@ -258,22 +265,17 @@
         xb = swap(jnp.stack([fb, yb]), "rep", nr, 1)
         far += [own_z, xa, yb, ya, xb]
 
+    cot = jnp.concatenate([cq, cv], axis=1)
     h = rank // nr
     *parts, fac = call(
-        functools.partial(project_body, nf, nr),
+        functools.partial(project_body, nf, nr, nq),
         [S((h, nc), BF)] * nr + [S((2, d, rank), BF)],
-        5 + 2 * nr,
-        [
-            pltpu.VMEM((rank, nc), BF),
-            pltpu.VMEM(cq.shape, BF),
-            pltpu.VMEM(cv.shape, BF),
-            pltpu.SemaphoreType.DMA((2,)),
-        ],
+        4 + 2 * nr,
+        [pltpu.VMEM((rank, nc), BF)],
         limit=24,
-        in_specs=[VMEM] * 3 + [ANY] * 2 + [VMEM] * 2 * nr,
         flops=2 * tokens * (d * 2 * rank + rank * nc),
         nbytes=2 * (tokens * (d + nc) + 4 * d * rank),
-    )(xs, fq, fv, cq, cv, *mine, *other)
+    )(xs, fq, fv, cot, *mine, *other)
     (gram,) = call(gram_body, [S((2, rank, rank), F32)], 1, flops=4 * d * rank * rank, nbytes=4 * d * rank)(fac)
 
     got = [parts[0]] + [swap(parts[j], "rep", nr, j) for j in range(1, nr)]
@@ -298,36 +300,50 @@
         functools.partial(total_body, nr, nq), [S((rank, nc), BF), S((16, 128), F32)], nr + 1, limit=12
     )(*got, gram)
     total_in = swap(total, "tp", nt, 1)
-    return (
-        *call(
-            functools.partial(final_body, nf, nr, nt),
-            [S((dl, nq), F32), S((dl, nv), F32)] * 2 + [S((d, nq), BF), S((d, nv), BF)],
-            8 + 5 * (nf - 2),
-            [
-                pltpu.VMEM((dl, nc), F32),
-                pltpu.VMEM((dl, nq), F32),
-                pltpu.VMEM((dl, nv), F32),
-                pltpu.VMEM((dl, nq), F32),
-                pltpu.VMEM((dl, nv), F32),
-                pltpu.VMEM((nf, dl, nq), BF),
-                pltpu.VMEM((nf, dl, nv), BF),
-                pltpu.SemaphoreType.DMA((4 + 2 * nf,)),
-            ],
-            limit=36,
-            out_specs=[ANY] * 6,
-            flops=2 * d * rank * nc,
-            nbytes=2 * d * nc * 2 + 12 * dl * nc,
-        )(fac, ratios, total, total_in, wq, wv, *near, *far),
-        q1n, q2n, v1n, v2n,
-    )
-
+    given = (fac, ratios, total, total_in)
+    qd, vd, qm, vm, qc, vc = call(
+        functools.partial(final_body, nt),
+        [S((dl, nq), F32), S((dl, nv), F32)] * 2 + [S((d, nq), BF), S((d, nv), BF)],
+        8 + 5 * (nf - 3),
+        [
+            pltpu.VMEM((dl, nc), F32),
+            pltpu.VMEM((dl, nq), F32),
+            pltpu.VMEM((dl, nv), F32),
+            pltpu.VMEM((dl, nq), F32),
+            pltpu.VMEM((dl, nv), F32),
+            pltpu.VMEM((nf - 1, dl, nq), BF),
+            pltpu.VMEM((nf - 1, dl, nv), BF),
+            pltpu.SemaphoreType.DMA((4 + 2 * nf,)),
+        ],
+        limit=30,
+        out_specs=[ANY] * 6,
+        flops=2 * d * rank * nc,
+        nbytes=2 * d * nc * 2 + 12 * dl * nc,
+    )(*given, wq, wv, *near, *far[:-5])
+    qc, vc = call(
+        functools.partial(last_body, nf - 1, nt),
+        [S((d, nq), BF), S((d, nv), BF)],
+        11,
+        [
+            pltpu.VMEM((dl, nc), F32),
+            pltpu.VMEM((1, dl, nq), BF),
+            pltpu.VMEM((1, dl, nv), BF),
+            pltpu.SemaphoreType.DMA((2,)),
+        ],
+        limit=16,
+        in_specs=[VMEM] * 9 + [ANY] * 2,
+        out_specs=[ANY] * 2,
+        flops=2 * dl * rank * nc,
+        nbytes=2 * dl * nc * 2,
+        aliases={9: 0, 10: 1},
+    )(*given, *far[-5:], qc, vc)
+    return qd, vd, qm, vm, qc, vc, q1n, q2n, v1n, v2n
 
 def moments(projected, first, second):
     first_new = BETA_ONE * first + (1.0 - BETA_ONE) * projected
     second_new = BETA_TWO * second + (1.0 - BETA_TWO) * projected * projected
     ratio = first_new / (jnp.sqrt(second_new) + EPS_RATIO)
     return (first_new, second_new, ratio)
-
 
 def collective(nf, nt, xs, cq, cv, wq, wv, fq, fv, q1, q2, v1, v2):
     dims = (((0,), (0,)), ((), ()))
@@ -352,7 +368,6 @@
     vd, vm, v1n, v2n, vc = one(cv, wv, fv, v1, v2)
     return qd, vd, qm, vm, q1n, q2n, v1n, v2n, qc, vc
 
-
 def local(nf, nr, nt, *args):
     rank = args[5].shape[1]
     if not square(nf, nr, nt) or rank % (nf * nr * TILE):
@@ -360,10 +375,8 @@
     qd, vd, qm, vm, qc, vc, *new = exchange(nf, nr, nt, *args)
     return qd, vd, qm, vm, *new, qc, vc
 
-
 def square(nf, nr, nt):
     return (nf, nr, nt) == (4, 2 * 2, 2)
-
 
 def solution(mesh):
     placed = (

time: 139 us -> 128 us (0.921)
  waiting for transfers between devices: 80.3 us -> 69.6 us
  local copies, waits for them, and re-layouts: 6.51 us -> 2.98 us
    ppermute x35, waiting for transfers between devices: 80.3 us -> 69.6 us  [swap(): return lax.ppermute(x, axis, [(i, i ^ k) for i in range(n)])]
    unnamed x26, local copies, waits for them, and re-layouts: 6.4 us -> 2.88 us
    pallas_call x2 -> x3, Pallas kernels: 10.5 us -> 11.8 us  [the longest x1 5.01 us: exchange(): call(functools.partial(final_body, nt), [S((dl, nq), F32), S((dl, nv), F3...]
  transfers between devices with their start and end apart: 35 -> 35, of which waited for: 20 -> 18; matrix products, arithmetic and copies ran while one was open for 0% -> 0% of each run, Pallas kernels for 6% -> 10%
where the time goes in v1:
time: 128 us
  waiting for transfers between devices  69.6 us (54%)
  starting transfers between devices  36.8 us (29%)
  Pallas kernels  16.9 us (13%)
  local copies, waits for them, and re-layouts  2.98 us (2%)
    ppermute x35, waiting for transfers between devices, swap(): return lax.ppermute(x, axis, [(i, i ^ k) for i in range(n)])  69.6 us
    ppermute x35, starting transfers between devices, swap(): return lax.ppermute(x, axis, [(i, i ^ k) for i in range(n)])  36.8 us
    pallas_call x1, Pallas kernels, exchange(): call(functools.partial(final_body, nt), [S((dl, nq), F32), S((dl, nv), F3...  5.01 us
    pallas_call x1, Pallas kernels, exchange(): call(functools.partial(project_body, nf, nr, nq), [S((h, nc), BF)] * nr +...  4.67 us
    unnamed x26, local copies, waits for them, and re-layouts  2.88 us
  transfers between devices with their start and end apart: 35, of which 18 were waited for; matrix products, arithmetic and copies ran while one was open for 0% of the time, Pallas kernels for 10%

profile of v1, /device:TPU:0, one launch (start us, length us, event | category | flops | bytes accessed | tf_op | source)
XLA Modules:
  0.0 127.6 jit_solution(11493562798411028137)
XLA Ops:
  0.7 1.6 %shard_map.186 = bf16[128,256]{1,0:T(8,128)(2,1)} custom-call(bf16[512,256]{1,0:T(8,128)(2,1)} %refs_1_.1, bf16[512,256]{1,0:T(8,128)(2,1)} %refs_2_.1), custom_call_target="tpu_custom_call" | custom-call | tf_op jit(solution)/shard_map/pallas_call | solution.py:243
  2.2 5.1 %collective-permute-start.2 = (bf16[128,256]{1,0:T(8,128)(2,1)}, bf16[128,256]{1,0:T(8,128)(2,1)S(1)}, u32[]{:S(2)}, u32[]{:S(2)}) collective-permute-start(bf16[128,256]{1,0:T(8,128)(2,1)} %shard_map.186), channel_id=1, source_target_pairs={{0,24},{8,16},{16,8},{24,0},{1,25},{9,17},{17,9},{25,1},{2,26},{10... | collective-permute-start | bytes 196616 | tf_op jit(solution)/shard_map/ppermute | solution.py:25
  8.0 2.2 %collective-permute-done.2 = bf16[128,256]{1,0:T(8,128)(2,1)S(1)} collective-permute-done((bf16[128,256]{1,0:T(8,128)(2,1)}, bf16[128,256]{1,0:T(8,128)(2,1)S(1)}, u32[]{:S(2)}, u32[]{:S(2)}) %collective-permute-start.2) | collective-permute-done | bytes 65568 | tf_op jit(solution)/shard_map/ppermute | solution.py:25
  10.2 3.0 %collective-permute-done.1 = bf16[128,256]{1,0:T(8,128)(2,1)S(1)} collective-permute-done((bf16[128,256]{1,0:T(8,128)(2,1)}, bf16[128,256]{1,0:T(8,128)(2,1)S(1)}, u32[]{:S(2)}, u32[]{:S(2)}) %collective-permute-start.1) | collective-permute-done | bytes 65568 | tf_op jit(solution)/shard_map/ppermute | solution.py:25
  13.2 2.5 %collective-permute-start.5 = (bf16[3,128,256]{2,1,0:T(8,128)(2,1)S(1)}, bf16[3,128,256]{2,1,0:T(8,128)(2,1)S(1)}, u32[]{:S(2)}, u32[]{:S(2)}) collective-permute-start(bf16[3,128,256]{2,1,0:T(8,128)(2,1)S(1)} %pad_maximum_fusion.5.refs_4_), channel_id=1, source_target_pairs={{0,6},{2,4},{4,2},{6,0},{1,7},{3,5},{5,3},{7,1},{8,14},{10,12},{12... | collective-permute-start | bytes 589832 | tf_op jit(solution)/shard_map/ppermute | solution.py:25
  16.8 1.6 %copy-done = f32[512,1024]{1,0:T(8,128)S(1)} copy-done((f32[512,1024]{1,0:T(8,128)S(1)}, f32[512,1024]{1,0:T(8,128)}, u32[]{:S(2)}) %copy-start) | copy-done | bytes 2097176
  20.0 1.6 %collective-permute-start.25 = (bf16[128,1536]{1,0:T(8,128)(2,1)S(1)}, bf16[128,1536]{1,0:T(8,128)(2,1)S(1)}, u32[]{:S(2)}, u32[]{:S(2)}) collective-permute-start(bf16[128,1536]{1,0:T(8,128)(2,1)S(1)} %get-tuple-element.51), channel_id=1, source_target_pairs={{0,16},{8,24},{16,0},{24,8},{1,17},{9,25},{17,1},{25,9},{2,18},{10... | collective-permute-start | bytes 1179656 | tf_op jit(solution)/shard_map/ppermute | solution.py:25
  22.2 2.6 %collective-permute-done.4.refs_6_ = bf16[3,128,256]{2,1,0:T(8,128)(2,1)S(1)} collective-permute-done((bf16[3,128,256]{2,1,0:T(8,128)(2,1)S(1)}, bf16[3,128,256]{2,1,0:T(8,128)(2,1)S(1)}, u32[]{:S(2)}, u32[]{:S(2)}) %collective-permute-start.4) | collective-permute-done | bytes 196640 | tf_op jit(solution)/shard_map/ppermute | solution.py:25
  26.6 4.7 %shard_map.187 = (bf16[64,1536]{1,0:T(8,128)(2,1)S(1)}, bf16[64,1536]{1,0:T(8,128)(2,1)S(1)}, bf16[64,1536]{1,0:T(8,128)(2,1)S(1)}, bf16[64,1536]{1,0:T(8,128)(2,1)S(1)}, bf16[2,2048,256]{2,1,0:T(8,128)(2,1)S(1)}) custom-call(bf16[768,2048]{1,0:T(8,128)(2,1)S(1)} %copy-done.10, bf16[512,256]{1,0:T(8,128)(2,1)S(1)} %copy-done.4, ...), custom_call_target="tpu_custom_call" | custom-call | flops 2214592512 | bytes 9699328 | tf_op jit(solution)/shard_map/pallas_call | solution.py:270
  31.3 1.7 %collective-permute-start.10 = (bf16[64,1536]{1,0:T(8,128)(2,1)S(1)}, bf16[64,1536]{1,0:T(8,128)(2,1)S(1)}, u32[]{:S(2)}, u32[]{:S(2)}) collective-permute-start(bf16[64,1536]{1,0:T(8,128)(2,1)S(1)} %get-tuple-element.39), channel_id=1, source_target_pairs={{0,2},{2,0},{4,6},{6,4},{1,3},{3,1},{5,7},{7,5},{8,10},{10,8},{12,... | collective-permute-start | bytes 589832 | tf_op jit(solution)/shard_map/ppermute | solution.py:25
  34.9 1.6 %collective-permute-start.30 = (bf16[128,1536]{1,0:T(8,128)(2,1)S(1)}, bf16[128,1536]{1,0:T(8,128)(2,1)S(1)}, u32[]{:S(2)}, u32[]{:S(2)}) collective-permute-start(bf16[128,1536]{1,0:T(8,128)(2,1)S(1)} %get-tuple-element.51), channel_id=1, source_target_pairs={{0,24},{8,16},{16,8},{24,0},{1,25},{9,17},{17,9},{25,1},{2,26},{10... | collective-permute-start | bytes 1179656 | tf_op jit(solution)/shard_map/ppermute | solution.py:25
  36.5 2.7 %collective-permute-done.10.refs_1_ = bf16[64,1536]{1,0:T(8,128)(2,1)S(1)} collective-permute-done((bf16[64,1536]{1,0:T(8,128)(2,1)S(1)}, bf16[64,1536]{1,0:T(8,128)(2,1)S(1)}, u32[]{:S(2)}, u32[]{:S(2)}) %collective-permute-start.10) | collective-permute-done | bytes 196640 | tf_op jit(solution)/shard_map/ppermute | solution.py:25
  39.2 4.8 %collective-permute-done.11.refs_2_ = bf16[64,1536]{1,0:T(8,128)(2,1)S(1)} collective-permute-done((bf16[64,1536]{1,0:T(8,128)(2,1)S(1)}, bf16[64,1536]{1,0:T(8,128)(2,1)S(1)}, u32[]{:S(2)}, u32[]{:S(2)}) %collective-permute-start.11) | collective-permute-done | bytes 196640 | tf_op jit(solution)/shard_map/ppermute | solution.py:25
  44.2 2.0 %collective-permute-start.23 = (bf16[256,1536]{1,0:T(8,128)(2,1)S(1)}, bf16[256,1536]{1,0:T(8,128)(2,1)S(1)}, u32[]{:S(2)}, u32[]{:S(2)}) collective-permute-start(bf16[256,1536]{1,0:T(8,128)(2,1)S(1)} %get-tuple-element.49), channel_id=1, source_target_pairs={{0,8},{8,0},{16,24},{24,16},{1,9},{9,1},{17,25},{25,17},{2,10},{10... | collective-permute-start | bytes 2359304 | tf_op jit(solution)/shard_map/ppermute | solution.py:25
  46.4 2.6 %collective-permute-done.13.refs_1_ = bf16[16,1536]{1,0:T(8,128)(2,1)S(1)} collective-permute-done((bf16[16,1536]{1,0:T(8,128)(2,1)S(1)}, bf16[16,1536]{1,0:T(8,128)(2,1)S(1)}, u32[]{:S(2)}, u32[]{:S(2)}) %collective-permute-start.13) | collective-permute-done | bytes 49184 | tf_op jit(solution)/shard_map/ppermute | solution.py:25
  49.0 1.3 %collective-permute-start.15 = (bf16[16,1536]{1,0:T(8,128)(2,1)S(1)}, bf16[16,1536]{1,0:T(8,128)(2,1)S(1)}, u32[]{:S(2)}, u32[]{:S(2)}) collective-permute-start(bf16[16,1536]{1,0:T(8,128)(2,1)S(1)} %get-tuple-element.45), channel_id=1, source_target_pairs={{0,24},{8,16},{16,8},{24,0},{1,25},{9,17},{17,9},{25,1},{2,26},{10... | collective-permute-start | bytes 147464 | tf_op jit(solution)/shard_map/ppermute | solution.py:25
  50.3 13.9 %collective-permute-done.14.refs_2_ = bf16[16,1536]{1,0:T(8,128)(2,1)S(1)} collective-permute-done((bf16[16,1536]{1,0:T(8,128)(2,1)S(1)}, bf16[16,1536]{1,0:T(8,128)(2,1)S(1)}, u32[]{:S(2)}, u32[]{:S(2)}) %collective-permute-start.14) | collective-permute-done | bytes 49184 | tf_op jit(solution)/shard_map/ppermute | solution.py:25
  64.2 3.0 %collective-permute-start.24 = (bf16[256,1536]{1,0:T(8,128)(2,1)S(1)}, bf16[256,1536]{1,0:T(8,128)(2,1)S(1)}, u32[]{:S(2)}, u32[]{:S(2)}) collective-permute-start(bf16[256,1536]{1,0:T(8,128)(2,1)S(1)} %get-tuple-element.50), channel_id=1, source_target_pairs={{0,8},{8,0},{16,24},{24,16},{1,9},{9,1},{17,25},{25,17},{2,10},{10... | collective-permute-start | bytes 2359304 | tf_op jit(solution)/shard_map/ppermute | solution.py:25
  67.3 1.9 %collective-permute-start.18 = (bf16[16,1536]{1,0:T(8,128)(2,1)S(1)}, bf16[16,1536]{1,0:T(8,128)(2,1)S(1)}, u32[]{:S(2)}, u32[]{:S(2)}) collective-permute-start(bf16[16,1536]{1,0:T(8,128)(2,1)S(1)} %shard_map.189.refs_0_), channel_id=1, source_target_pairs={{0,24},{8,16},{16,8},{24,0},{1,25},{9,17},{17,9},{25,1},{2,26},{10... | collective-permute-start | bytes 147464 | tf_op jit(solution)/shard_map/ppermute | solution.py:25
  69.3 1.4 %collective-permute-start.27 = (bf16[128,768]{1,0:T(8,128)(2,1)S(1)}, bf16[128,768]{1,0:T(8,128)(2,1)S(1)}, u32[]{:S(2)}, u32[]{:S(2)}) collective-permute-start(bf16[128,768]{1,0:T(8,128)(2,1)S(1)} %get-tuple-element.70), channel_id=1, source_target_pairs={{0,4},{2,6},{4,0},{6,2},{1,5},{3,7},{5,1},{7,3},{8,12},{10,14},{12... | collective-permute-start | bytes 589832 | tf_op jit(solution)/shard_map/ppermute | solution.py:25
  70.6 15.2 %collective-permute-done.18.refs_3_ = bf16[16,1536]{1,0:T(8,128)(2,1)S(1)} collective-permute-done((bf16[16,1536]{1,0:T(8,128)(2,1)S(1)}, bf16[16,1536]{1,0:T(8,128)(2,1)S(1)}, u32[]{:S(2)}, u32[]{:S(2)}) %collective-permute-start.18) | collective-permute-done | bytes 49184 | tf_op jit(solution)/shard_map/ppermute | solution.py:25
  85.9 1.7 %collective-permute-start.26 = (bf16[128,768]{1,0:T(8,128)(2,1)S(1)}, bf16[128,768]{1,0:T(8,128)(2,1)S(1)}, u32[]{:S(2)}, u32[]{:S(2)}) collective-permute-start(bf16[128,768]{1,0:T(8,128)(2,1)S(1)} %get-tuple-element.71), channel_id=1, source_target_pairs={{0,2},{2,0},{4,6},{6,4},{1,3},{3,1},{5,7},{7,5},{8,10},{10,8},{12,... | collective-permute-start | bytes 589832 | tf_op jit(solution)/shard_map/ppermute | solution.py:25
  87.6 4.0 %collective-permute-done.16.refs_1_ = bf16[16,1536]{1,0:T(8,128)(2,1)S(1)} collective-permute-done((bf16[16,1536]{1,0:T(8,128)(2,1)S(1)}, bf16[16,1536]{1,0:T(8,128)(2,1)S(1)}, u32[]{:S(2)}, u32[]{:S(2)}) %collective-permute-start.16) | collective-permute-done | bytes 49184 | tf_op jit(solution)/shard_map/ppermute | solution.py:25
  93.2 1.3 %collective-permute-start.31 = (bf16[128,768]{1,0:T(8,128)(2,1)S(1)}, bf16[128,768]{1,0:T(8,128)(2,1)S(1)}, u32[]{:S(2)}, u32[]{:S(2)}) collective-permute-start(bf16[128,768]{1,0:T(8,128)(2,1)S(1)} %get-tuple-element.67), channel_id=1, source_target_pairs={{0,2},{2,0},{4,6},{6,4},{1,3},{3,1},{5,7},{7,5},{8,10},{10,8},{12,... | collective-permute-start | bytes 589832 | tf_op jit(solution)/shard_map/ppermute | solution.py:25
  94.5 1.7 %collective-permute-start.21 = (bf16[64,1536]{1,0:T(8,128)(2,1)S(1)}, bf16[64,1536]{1,0:T(8,128)(2,1)S(1)}, u32[]{:S(2)}, u32[]{:S(2)}) collective-permute-start(bf16[64,1536]{1,0:T(8,128)(2,1)S(1)} %get-tuple-element.46.refs_0_), channel_id=1, source_target_pairs={{0,6},{2,4},{4,2},{6,0},{1,7},{3,5},{5,3},{7,1},{8,14},{10,12},{12... | collective-permute-start | bytes 589832 | tf_op jit(solution)/shard_map/ppermute | solution.py:25
  96.3 4.7 %collective-permute-done.32.refs_6_ = bf16[128,768]{1,0:T(8,128)(2,1)S(1)} collective-permute-done((bf16[128,768]{1,0:T(8,128)(2,1)S(1)}, bf16[128,768]{1,0:T(8,128)(2,1)S(1)}, u32[]{:S(2)}, u32[]{:S(2)}) %collective-permute-start.32) | collective-permute-done | bytes 196640 | tf_op jit(solution)/shard_map/ppermute | solution.py:25
  101.4 1.7 %collective-permute-start.29 = (bf16[2,128,768]{2,1,0:T(8,128)(2,1)S(1)}, bf16[2,128,768]{2,1,0:T(8,128)(2,1)S(1)}, u32[]{:S(2)}, u32[]{:S(2)}) collective-permute-start(bf16[2,128,768]{2,1,0:T(8,128)(2,1)S(1)} %pad_maximum_fusion.2), channel_id=1, source_target_pairs={{0,2},{2,0},{4,6},{6,4},{1,3},{3,1},{5,7},{7,5},{8,10},{10,8},{12,... | collective-permute-start | bytes 1179656 | tf_op jit(solution)/shard_map/ppermute | solution.py:25
  103.6 2.6 %collective-permute-done.21.refs_3_ = bf16[64,1536]{1,0:T(8,128)(2,1)S(1)} collective-permute-done((bf16[64,1536]{1,0:T(8,128)(2,1)S(1)}, bf16[64,1536]{1,0:T(8,128)(2,1)S(1)}, u32[]{:S(2)}, u32[]{:S(2)}) %collective-permute-start.21) | collective-permute-done | bytes 196640 | tf_op jit(solution)/shard_map/ppermute | solution.py:25
  106.6 8.7 %collective-permute-done.20.refs_2_ = bf16[64,1536]{1,0:T(8,128)(2,1)S(1)} collective-permute-done((bf16[64,1536]{1,0:T(8,128)(2,1)S(1)}, bf16[64,1536]{1,0:T(8,128)(2,1)S(1)}, u32[]{:S(2)}, u32[]{:S(2)}) %collective-permute-start.20) | collective-permute-done | bytes 196640 | tf_op jit(solution)/shard_map/ppermute | solution.py:25
  115.7 1.5 %collective-permute-start.34 = (bf16[2,128,768]{2,1,0:T(8,128)(2,1)S(1)}, bf16[2,128,768]{2,1,0:T(8,128)(2,1)S(1)}, u32[]{:S(2)}, u32[]{:S(2)}) collective-permute-start(bf16[2,128,768]{2,1,0:T(8,128)(2,1)S(1)} %pad_maximum_fusion.4), channel_id=1, source_target_pairs={{0,2},{2,0},{4,6},{6,4},{1,3},{3,1},{5,7},{7,5},{8,10},{10,8},{12,... | collective-permute-start | bytes 1179656 | tf_op jit(solution)/shard_map/ppermute | solution.py:25
  120.5 5.0 %shard_map.194 = (f32[512,512]{1,0:T(8,128)}, f32[512,1024]{1,0:T(8,128)}, f32[512,512]{1,0:T(8,128)}, f32[512,1024]{1,0:T(8,128)}, bf16[2048,512]{1,0:T(8,128)(2,1)}, /*index=5*/bf16[2048,1024]{1,0:T(8,128)(2,1)}) custom-call(bf16[2,2048,256]{2,1,0:T(8,128)(2,1)S(1)} %get-tuple-element.37.fac.refs_0_, bf16[256,1536]{1,0:T(8,128)(2,1)S(1)} %get-tuple-element.47.refs_1_, ...), custom_call_target="tpu_custom_call" | custom-call | flops 1610612736 | bytes 22020096 | tf_op jit(solution)/shard_map/pallas_call | solution.py:304
  125.5 2.1 %shard_map.195 = (bf16[2048,512]{1,0:T(8,128)(2,1)}, bf16[2048,1024]{1,0:T(8,128)(2,1)}) custom-call(bf16[2,2048,256]{2,1,0:T(8,128)(2,1)S(1)} %get-tuple-element.37.fac.refs_0_, bf16[256,1536]{1,0:T(8,128)(2,1)S(1)} %get-tuple-element.47.refs_1_, f32[16,128]{1,0:T(8,128)S(1)} %get-tuple-element.48.refs_2_, ...), custom_call_target="tpu_custom_call", output_to_operand_aliasing={{0}: (9, {}), {1}: (10, {})} | custom-call | flops 402653184 | bytes 3145728 | tf_op jit(solution)/shard_map/pallas_call | solution.py:323
  (82 shorter events, 14.8 us)
Async XLA Ops:
  2.2 7.9 %collective-permute-start.2 = (bf16[128,256]{1,0:T(8,128)(2,1)}, bf16[128,256]{1,0:T(8,128)(2,1)S(1)}, u32[]{:S(2)}, u32[]{:S(2)}) collective-permute-start(bf16[128,256]{1,0:T(8,128)(2,1)} %shard_map.186), channel_id=1, source_target_pairs={{0,24},{8,16},{16,8},{24,0},{1,25},{9,17},{17,9},{25,1},{2,26},{10... | collective-permute-start | bytes 196616 | tf_op jit(solution)/shard_map/ppermute | solution.py:25
  7.4 5.8 %collective-permute-start.1 = (bf16[128,256]{1,0:T(8,128)(2,1)}, bf16[128,256]{1,0:T(8,128)(2,1)S(1)}, u32[]{:S(2)}, u32[]{:S(2)}) collective-permute-start(bf16[128,256]{1,0:T(8,128)(2,1)} %shard_map.186), channel_id=1, source_target_pairs={{0,16},{8,24},{16,0},{24,8},{1,17},{9,25},{17,1},{25,9},{2,18},{10... | collective-permute-start | bytes 196616 | tf_op jit(solution)/shard_map/ppermute | solution.py:25
  7.4 5.8 %collective-permute-start = (bf16[128,256]{1,0:T(8,128)(2,1)}, bf16[128,256]{1,0:T(8,128)(2,1)S(1)}, u32[]{:S(2)}, u32[]{:S(2)}) collective-permute-start(bf16[128,256]{1,0:T(8,128)(2,1)} %shard_map.186), channel_id=1, source_target_pairs={{0,8},{8,0},{16,24},{24,16},{1,9},{9,1},{17,25},{25,17},{2,10},{10... | collective-permute-start | bytes 196616 | tf_op jit(solution)/shard_map/ppermute | solution.py:25
  13.2 8.7 %collective-permute-start.5 = (bf16[3,128,256]{2,1,0:T(8,128)(2,1)S(1)}, bf16[3,128,256]{2,1,0:T(8,128)(2,1)S(1)}, u32[]{:S(2)}, u32[]{:S(2)}) collective-permute-start(bf16[3,128,256]{2,1,0:T(8,128)(2,1)S(1)} %pad_maximum_fusion.5.refs_4_), channel_id=1, source_target_pairs={{0,6},{2,4},{4,2},{6,0},{1,7},{3,5},{5,3},{7,1},{8,14},{10,12},{12... | collective-permute-start | bytes 589832 | tf_op jit(solution)/shard_map/ppermute | solution.py:25
  15.7 9.1 %collective-permute-start.4 = (bf16[3,128,256]{2,1,0:T(8,128)(2,1)S(1)}, bf16[3,128,256]{2,1,0:T(8,128)(2,1)S(1)}, u32[]{:S(2)}, u32[]{:S(2)}) collective-permute-start(bf16[3,128,256]{2,1,0:T(8,128)(2,1)S(1)} %pad_maximum_fusion.5.refs_4_), channel_id=1, source_target_pairs={{0,4},{2,6},{4,0},{6,2},{1,5},{3,7},{5,1},{7,3},{8,12},{10,14},{12... | collective-permute-start | bytes 589832 | tf_op jit(solution)/shard_map/ppermute | solution.py:25
  16.2 8.8 %collective-permute-start.3 = (bf16[3,128,256]{2,1,0:T(8,128)(2,1)S(1)}, bf16[3,128,256]{2,1,0:T(8,128)(2,1)S(1)}, u32[]{:S(2)}, u32[]{:S(2)}) collective-permute-start(bf16[3,128,256]{2,1,0:T(8,128)(2,1)S(1)} %pad_maximum_fusion.5.refs_4_), channel_id=1, source_target_pairs={{0,2},{2,0},{4,6},{6,4},{1,3},{3,1},{5,7},{7,5},{8,10},{10,8},{12,... | collective-permute-start | bytes 589832 | tf_op jit(solution)/shard_map/ppermute | solution.py:25
  20.0 49.1 %collective-permute-start.25 = (bf16[128,1536]{1,0:T(8,128)(2,1)S(1)}, bf16[128,1536]{1,0:T(8,128)(2,1)S(1)}, u32[]{:S(2)}, u32[]{:S(2)}) collective-permute-start(bf16[128,1536]{1,0:T(8,128)(2,1)S(1)} %get-tuple-element.51), channel_id=1, source_target_pairs={{0,16},{8,24},{16,0},{24,8},{1,17},{9,25},{17,1},{25,9},{2,18},{10... | collective-permute-start | bytes 1179656 | tf_op jit(solution)/shard_map/ppermute | solution.py:25
  21.7 3.9 %collective-permute-start.6 = (bf16[3,128,256]{2,1,0:T(8,128)(2,1)S(1)}, bf16[3,128,256]{2,1,0:T(8,128)(2,1)S(1)}, u32[]{:S(2)}, u32[]{:S(2)}) collective-permute-start(bf16[3,128,256]{2,1,0:T(8,128)(2,1)S(1)} %pad_maximum_fusion.5.refs_4_), channel_id=1, source_target_pairs={{0,1},{1,0},{2,3},{3,2},{4,5},{5,4},{6,7},{7,6},{8,9},{9,8},{10,11... | collective-permute-start | bytes 589832 | tf_op jit(solution)/shard_map/ppermute | solution.py:25
  22.0 3.6 %collective-permute-start.9 = (bf16[3,128,256]{2,1,0:T(8,128)(2,1)S(1)}, bf16[3,128,256]{2,1,0:T(8,128)(2,1)S(1)}, u32[]{:S(2)}, u32[]{:S(2)}) collective-permute-start(bf16[3,128,256]{2,1,0:T(8,128)(2,1)S(1)} %collective-permute-done.5.refs_7_), channel_id=1, source_target_pairs={{0,1},{1,0},{2,3},{3,2},{4,5},{5,4},{6,7},{7,6},{8,9},{9,8},{10,11... | collective-permute-start | bytes 589832 | tf_op jit(solution)/shard_map/ppermute | solution.py:25
  31.3 7.8 %collective-permute-start.10 = (bf16[64,1536]{1,0:T(8,128)(2,1)S(1)}, bf16[64,1536]{1,0:T(8,128)(2,1)S(1)}, u32[]{:S(2)}, u32[]{:S(2)}) collective-permute-start(bf16[64,1536]{1,0:T(8,128)(2,1)S(1)} %get-tuple-element.39), channel_id=1, source_target_pairs={{0,2},{2,0},{4,6},{6,4},{1,3},{3,1},{5,7},{7,5},{8,10},{10,8},{12,... | collective-permute-start | bytes 589832 | tf_op jit(solution)/shard_map/ppermute | solution.py:25
  33.0 11.0 %collective-permute-start.11 = (bf16[64,1536]{1,0:T(8,128)(2,1)S(1)}, bf16[64,1536]{1,0:T(8,128)(2,1)S(1)}, u32[]{:S(2)}, u32[]{:S(2)}) collective-permute-start(bf16[64,1536]{1,0:T(8,128)(2,1)S(1)} %get-tuple-element.40), channel_id=1, source_target_pairs={{0,4},{2,6},{4,0},{6,2},{1,5},{3,7},{5,1},{7,3},{8,12},{10,14},{12... | collective-permute-start | bytes 589832 | tf_op jit(solution)/shard_map/ppermute | solution.py:25
  33.7 10.3 %collective-permute-start.12 = (bf16[64,1536]{1,0:T(8,128)(2,1)S(1)}, bf16[64,1536]{1,0:T(8,128)(2,1)S(1)}, u32[]{:S(2)}, u32[]{:S(2)}) collective-permute-start(bf16[64,1536]{1,0:T(8,128)(2,1)S(1)} %get-tuple-element.41), channel_id=1, source_target_pairs={{0,6},{2,4},{4,2},{6,0},{1,7},{3,5},{5,3},{7,1},{8,14},{10,12},{12... | collective-permute-start | bytes 589832 | tf_op jit(solution)/shard_map/ppermute | solution.py:25
  34.9 34.4 %collective-permute-start.30 = (bf16[128,1536]{1,0:T(8,128)(2,1)S(1)}, bf16[128,1536]{1,0:T(8,128)(2,1)S(1)}, u32[]{:S(2)}, u32[]{:S(2)}) collective-permute-start(bf16[128,1536]{1,0:T(8,128)(2,1)S(1)} %get-tuple-element.51), channel_id=1, source_target_pairs={{0,24},{8,16},{16,8},{24,0},{1,25},{9,17},{17,9},{25,1},{2,26},{10... | collective-permute-start | bytes 1179656 | tf_op jit(solution)/shard_map/ppermute | solution.py:25
  44.1 4.9 %collective-permute-start.13 = (bf16[16,1536]{1,0:T(8,128)(2,1)S(1)}, bf16[16,1536]{1,0:T(8,128)(2,1)S(1)}, u32[]{:S(2)}, u32[]{:S(2)}) collective-permute-start(bf16[16,1536]{1,0:T(8,128)(2,1)S(1)} %get-tuple-element.43), channel_id=1, source_target_pairs={{0,8},{8,0},{16,24},{24,16},{1,9},{9,1},{17,25},{25,17},{2,10},{10... | collective-permute-start | bytes 147464 | tf_op jit(solution)/shard_map/ppermute | solution.py:25
  44.2 58.9 %collective-permute-start.23 = (bf16[256,1536]{1,0:T(8,128)(2,1)S(1)}, bf16[256,1536]{1,0:T(8,128)(2,1)S(1)}, u32[]{:S(2)}, u32[]{:S(2)}) collective-permute-start(bf16[256,1536]{1,0:T(8,128)(2,1)S(1)} %get-tuple-element.49), channel_id=1, source_target_pairs={{0,8},{8,0},{16,24},{24,16},{1,9},{9,1},{17,25},{25,17},{2,10},{10... | collective-permute-start | bytes 2359304 | tf_op jit(solution)/shard_map/ppermute | solution.py:25
  46.2 18.0 %collective-permute-start.14 = (bf16[16,1536]{1,0:T(8,128)(2,1)S(1)}, bf16[16,1536]{1,0:T(8,128)(2,1)S(1)}, u32[]{:S(2)}, u32[]{:S(2)}) collective-permute-start(bf16[16,1536]{1,0:T(8,128)(2,1)S(1)} %get-tuple-element.44), channel_id=1, source_target_pairs={{0,16},{8,24},{16,0},{24,8},{1,17},{9,25},{17,1},{25,9},{2,18},{10... | collective-permute-start | bytes 147464 | tf_op jit(solution)/shard_map/ppermute | solution.py:25
  49.0 18.2 %collective-permute-start.15 = (bf16[16,1536]{1,0:T(8,128)(2,1)S(1)}, bf16[16,1536]{1,0:T(8,128)(2,1)S(1)}, u32[]{:S(2)}, u32[]{:S(2)}) collective-permute-start(bf16[16,1536]{1,0:T(8,128)(2,1)S(1)} %get-tuple-element.45), channel_id=1, source_target_pairs={{0,24},{8,16},{16,8},{24,0},{1,25},{9,17},{17,9},{25,1},{2,26},{10... | collective-permute-start | bytes 147464 | tf_op jit(solution)/shard_map/ppermute | solution.py:25
  64.2 55.0 %collective-permute-start.24 = (bf16[256,1536]{1,0:T(8,128)(2,1)S(1)}, bf16[256,1536]{1,0:T(8,128)(2,1)S(1)}, u32[]{:S(2)}, u32[]{:S(2)}) collective-permute-start(bf16[256,1536]{1,0:T(8,128)(2,1)S(1)} %get-tuple-element.50), channel_id=1, source_target_pairs={{0,8},{8,0},{16,24},{24,16},{1,9},{9,1},{17,25},{25,17},{2,10},{10... | collective-permute-start | bytes 2359304 | tf_op jit(solution)/shard_map/ppermute | solution.py:25
  67.3 18.6 %collective-permute-start.18 = (bf16[16,1536]{1,0:T(8,128)(2,1)S(1)}, bf16[16,1536]{1,0:T(8,128)(2,1)S(1)}, u32[]{:S(2)}, u32[]{:S(2)}) collective-permute-start(bf16[16,1536]{1,0:T(8,128)(2,1)S(1)} %shard_map.189.refs_0_), channel_id=1, source_target_pairs={{0,24},{8,16},{16,8},{24,0},{1,25},{9,17},{17,9},{25,1},{2,26},{10... | collective-permute-start | bytes 147464 | tf_op jit(solution)/shard_map/ppermute | solution.py:25
  69.2 18.4 %collective-permute-start.17 = (bf16[16,1536]{1,0:T(8,128)(2,1)S(1)}, bf16[16,1536]{1,0:T(8,128)(2,1)S(1)}, u32[]{:S(2)}, u32[]{:S(2)}) collective-permute-start(bf16[16,1536]{1,0:T(8,128)(2,1)S(1)} %shard_map.189.refs_0_), channel_id=1, source_target_pairs={{0,16},{8,24},{16,0},{24,8},{1,17},{9,25},{17,1},{25,9},{2,18},{10... | collective-permute-start | bytes 147464 | tf_op jit(solution)/shard_map/ppermute | solution.py:25
  69.3 23.9 %collective-permute-start.27 = (bf16[128,768]{1,0:T(8,128)(2,1)S(1)}, bf16[128,768]{1,0:T(8,128)(2,1)S(1)}, u32[]{:S(2)}, u32[]{:S(2)}) collective-permute-start(bf16[128,768]{1,0:T(8,128)(2,1)S(1)} %get-tuple-element.70), channel_id=1, source_target_pairs={{0,4},{2,6},{4,0},{6,2},{1,5},{3,7},{5,1},{7,3},{8,12},{10,14},{12... | collective-permute-start | bytes 589832 | tf_op jit(solution)/shard_map/ppermute | solution.py:25
  85.9 8.6 %collective-permute-start.26 = (bf16[128,768]{1,0:T(8,128)(2,1)S(1)}, bf16[128,768]{1,0:T(8,128)(2,1)S(1)}, u32[]{:S(2)}, u32[]{:S(2)}) collective-permute-start(bf16[128,768]{1,0:T(8,128)(2,1)S(1)} %get-tuple-element.71), channel_id=1, source_target_pairs={{0,2},{2,0},{4,6},{6,4},{1,3},{3,1},{5,7},{7,5},{8,10},{10,8},{12,... | collective-permute-start | bytes 589832 | tf_op jit(solution)/shard_map/ppermute | solution.py:25
  87.5 4.1 %collective-permute-start.16 = (bf16[16,1536]{1,0:T(8,128)(2,1)S(1)}, bf16[16,1536]{1,0:T(8,128)(2,1)S(1)}, u32[]{:S(2)}, u32[]{:S(2)}) collective-permute-start(bf16[16,1536]{1,0:T(8,128)(2,1)S(1)} %shard_map.189.refs_0_), channel_id=1, source_target_pairs={{0,8},{8,0},{16,24},{24,16},{1,9},{9,1},{17,25},{25,17},{2,10},{10... | collective-permute-start | bytes 147464 | tf_op jit(solution)/shard_map/ppermute | solution.py:25
  91.6 9.3 %collective-permute-start.32 = (bf16[128,768]{1,0:T(8,128)(2,1)S(1)}, bf16[128,768]{1,0:T(8,128)(2,1)S(1)}, u32[]{:S(2)}, u32[]{:S(2)}) collective-permute-start(bf16[128,768]{1,0:T(8,128)(2,1)S(1)} %get-tuple-element.66), channel_id=1, source_target_pairs={{0,4},{2,6},{4,0},{6,2},{1,5},{3,7},{5,1},{7,3},{8,12},{10,14},{12... | collective-permute-start | bytes 589832 | tf_op jit(solution)/shard_map/ppermute | solution.py:25
  93.2 8.3 %collective-permute-start.31 = (bf16[128,768]{1,0:T(8,128)(2,1)S(1)}, bf16[128,768]{1,0:T(8,128)(2,1)S(1)}, u32[]{:S(2)}, u32[]{:S(2)}) collective-permute-start(bf16[128,768]{1,0:T(8,128)(2,1)S(1)} %get-tuple-element.67), channel_id=1, source_target_pairs={{0,2},{2,0},{4,6},{6,4},{1,3},{3,1},{5,7},{7,5},{8,10},{10,8},{12,... | collective-permute-start | bytes 589832 | tf_op jit(solution)/shard_map/ppermute | solution.py:25
  94.5 11.6 %collective-permute-start.21 = (bf16[64,1536]{1,0:T(8,128)(2,1)S(1)}, bf16[64,1536]{1,0:T(8,128)(2,1)S(1)}, u32[]{:S(2)}, u32[]{:S(2)}) collective-permute-start(bf16[64,1536]{1,0:T(8,128)(2,1)S(1)} %get-tuple-element.46.refs_0_), channel_id=1, source_target_pairs={{0,6},{2,4},{4,2},{6,0},{1,7},{3,5},{5,3},{7,1},{8,14},{10,12},{12... | collective-permute-start | bytes 589832 | tf_op jit(solution)/shard_map/ppermute | solution.py:25
  100.9 19.5 %collective-permute-start.28 = (bf16[2,128,768]{2,1,0:T(8,128)(2,1)S(1)}, bf16[2,128,768]{2,1,0:T(8,128)(2,1)S(1)}, u32[]{:S(2)}, u32[]{:S(2)}) collective-permute-start(bf16[2,128,768]{2,1,0:T(8,128)(2,1)S(1)} %pad_maximum_fusion.1), channel_id=1, source_target_pairs={{0,4},{2,6},{4,0},{6,2},{1,5},{3,7},{5,1},{7,3},{8,12},{10,14},{12... | collective-permute-start | bytes 1179656 | tf_op jit(solution)/shard_map/ppermute | solution.py:25
  101.4 19.0 %collective-permute-start.29 = (bf16[2,128,768]{2,1,0:T(8,128)(2,1)S(1)}, bf16[2,128,768]{2,1,0:T(8,128)(2,1)S(1)}, u32[]{:S(2)}, u32[]{:S(2)}) collective-permute-start(bf16[2,128,768]{2,1,0:T(8,128)(2,1)S(1)} %pad_maximum_fusion.2), channel_id=1, source_target_pairs={{0,2},{2,0},{4,6},{6,4},{1,3},{3,1},{5,7},{7,5},{8,10},{10,8},{12,... | collective-permute-start | bytes 1179656 | tf_op jit(solution)/shard_map/ppermute | solution.py:25
  103.1 12.1 %collective-permute-start.20 = (bf16[64,1536]{1,0:T(8,128)(2,1)S(1)}, bf16[64,1536]{1,0:T(8,128)(2,1)S(1)}, u32[]{:S(2)}, u32[]{:S(2)}) collective-permute-start(bf16[64,1536]{1,0:T(8,128)(2,1)S(1)} %get-tuple-element.46.refs_0_), channel_id=1, source_target_pairs={{0,4},{2,6},{4,0},{6,2},{1,5},{3,7},{5,1},{7,3},{8,12},{10,14},{12... | collective-permute-start | bytes 589832 | tf_op jit(solution)/shard_map/ppermute | solution.py:25
  106.1 9.6 %collective-permute-start.19 = (bf16[64,1536]{1,0:T(8,128)(2,1)S(1)}, bf16[64,1536]{1,0:T(8,128)(2,1)S(1)}, u32[]{:S(2)}, u32[]{:S(2)}) collective-permute-start(bf16[64,1536]{1,0:T(8,128)(2,1)S(1)} %get-tuple-element.46.refs_0_), channel_id=1, source_target_pairs={{0,2},{2,0},{4,6},{6,4},{1,3},{3,1},{5,7},{7,5},{8,10},{10,8},{12,... | collective-permute-start | bytes 589832 | tf_op jit(solution)/shard_map/ppermute | solution.py:25
  115.3 10.2 %collective-permute-start.33 = (bf16[2,128,768]{2,1,0:T(8,128)(2,1)S(1)}, bf16[2,128,768]{2,1,0:T(8,128)(2,1)S(1)}, u32[]{:S(2)}, u32[]{:S(2)}) collective-permute-start(bf16[2,128,768]{2,1,0:T(8,128)(2,1)S(1)} %pad_maximum_fusion.3), channel_id=1, source_target_pairs={{0,4},{2,6},{4,0},{6,2},{1,5},{3,7},{5,1},{7,3},{8,12},{10,14},{12... | collective-permute-start | bytes 1179656 | tf_op jit(solution)/shard_map/ppermute | solution.py:25
  115.7 9.8 %collective-permute-start.34 = (bf16[2,128,768]{2,1,0:T(8,128)(2,1)S(1)}, bf16[2,128,768]{2,1,0:T(8,128)(2,1)S(1)}, u32[]{:S(2)}, u32[]{:S(2)}) collective-permute-start(bf16[2,128,768]{2,1,0:T(8,128)(2,1)S(1)} %pad_maximum_fusion.4), channel_id=1, source_target_pairs={{0,2},{2,0},{4,6},{6,4},{1,3},{3,1},{5,7},{7,5},{8,10},{10,8},{12,... | collective-permute-start | bytes 1179656 | tf_op jit(solution)/shard_map/ppermute | solution.py:25
  (16 other events, 328.3 us)

commit v2 on v1

--- a/solution.py
+++ b/solution.py
@@ -20,6 +20,7 @@
 VMEM = pl.BlockSpec(memory_space=pltpu.VMEM)
 ANY = pl.BlockSpec(memory_space=pltpu.HBM)
 TILE = 16
+EARLY = 5
 
 def swap(x, axis, n, k):
     return lax.ppermute(x, axis, [(i, i ^ k) for i in range(n)])
@@ -39,52 +40,56 @@
         cost_estimate=pl.CostEstimate(flops=flops, bytes_accessed=nbytes, transcendentals=0),
     )
 
-def first_body(nr, fq, fv, out, sem):
-    r, t = lax.axis_index("rep"), lax.axis_index("tp")
-    here = rows_at(r, fq.shape[0] // nr)
-    for n, ref in enumerate((fq, fv)):
-
-        @pl.when(t == n)
-        def _():
-            move = pltpu.make_async_copy(ref.at[here, :], out, sem)
-            move.start()
-            move.wait()
-
-def pack_body(nr, wq_h, wv_h, quarter, low, high, wq, wv, sem):
-    r = lax.axis_index("rep")
-    dl, nq = wq.shape
-    loads = [pltpu.make_async_copy(wq_h, wq, sem.at[0]), pltpu.make_async_copy(wv_h, wv, sem.at[1])]
-    for c in loads:
-        c.start()
-    for c in loads:
-        c.wait()
-    for out, here in ((quarter, rows_at(r, dl // nr)), (low, slice(0, dl // 2)), (high, slice(dl // 2, dl))):
-        out[:, :nq] = wq[here, :].astype(BF)
-        out[:, nq:] = wv[here, :].astype(BF)
-
-def project_body(nf, nr, nq, *refs):
-    x, fq, fv, cot = refs[:4]
-    mine, other = refs[4 : 4 + nr], refs[4 + nr : 4 + 2 * nr]
-    outs = refs[4 + 2 * nr : 4 + 3 * nr]
-    fac, part = refs[4 + 3 * nr :]
-    f, r, t = lax.axis_index("fs"), lax.axis_index("rep"), lax.axis_index("tp")
-    dl = fq.shape[0]
-    piece = dl // nr
-    fac[0, rows_at(f, dl), :] = fq[...]
-    fac[1, rows_at(f, dl), :] = fv[...]
+def pack_body(wq, wv, low, high):
+    nq = wq.shape[1]
+    for ref, here in ((low, slice(0, low.shape[0])), (high, slice(low.shape[0], wq.shape[0]))):
+        ref[:, :nq] = wq[here, :].astype(BF)
+        ref[:, nq:] = wv[here, :].astype(BF)
+
+
+def collect(nf, nr, out, pieces):
+    f, r = lax.axis_index("fs"), lax.axis_index("rep")
+    height = pieces[0].shape[1]
     for k in range(1, nf):
         for j in range(nr):
-            here = rows_at((f ^ k) * nr + (r ^ j), piece)
-            fac[t, here, :] = mine[j][k - 1]
-            fac[1 - t, here, :] = other[j][k - 1]
+            out[rows_at((f ^ k) * nr + (r ^ j), height), :] = pieces[j][k - 1]
+
+
+def lift_body(nf, nr, x, fq, fv, *refs):
+    pieces, (y, fac) = refs[:nr], refs[nr:]
+    own = rows_at(lax.axis_index("fs"), fq.shape[0])
+    for s, ref in enumerate((fq, fv)):
+
+        @pl.when(lax.axis_index("tp") == s)
+        def _():
+            fac[own, :] = ref[...]
+
+    collect(nf, nr, fac, pieces)
+    y[...] = jnp.dot(x[...], fac[...], preferred_element_type=F32).astype(BF)
+
+
+def project_body(nf, nr, nq, x, fq, fv, cot, y_mine, mine, *refs):
+    pieces, outs, (fac, y, part) = refs[:nr], refs[nr : 2 * nr], refs[2 * nr :]
+    f, r, t = lax.axis_index("fs"), lax.axis_index("rep"), lax.axis_index("tp")
+    own = rows_at(f, fq.shape[0])
+    other = fac.at[1 - t]
+    for s, ref in enumerate((fq, fv)):
+
+        @pl.when(t != s)
+        def _():
+            other[own, :] = ref[...]
+
+    collect(nf, nr, other, pieces)
+    y[1 - t] = jnp.dot(x[...], other[...], preferred_element_type=F32).astype(BF)
+    y[t] = y_mine[...]
+    fac[t] = mine[...]
     dims = (((0,), (0,)), ((), ()))
-    yq = jnp.dot(x[...], fac[0], preferred_element_type=F32).astype(BF)
-    part[:, :nq] = lax.dot_general(yq, cot[:, :nq], dims, preferred_element_type=F32).astype(BF)
-    yv = jnp.dot(x[...], fac[1], preferred_element_type=F32).astype(BF)
-    part[:, nq:] = lax.dot_general(yv, cot[:, nq:], dims, preferred_element_type=F32).astype(BF)
+    for s, cols in ((0, slice(None, nq)), (1, slice(nq, None))):
+        part[:, cols] = lax.dot_general(y[s], cot[:, cols], dims, preferred_element_type=F32).astype(BF)
     h = part.shape[0] // nr
     for j in range(nr):
         outs[j][...] = part[rows_at(r ^ j, h), :]
+
 
 def plane_sum_body(nf, nr, *refs):
     ins, own, rest, acc = refs[:nr], refs[nr], refs[nr + 1 : nr + nf], refs[nr + nf]
@@ -153,9 +158,15 @@
         lax.rsqrt(both[8:9, 0:1] / (d * nv * nt) + EPS_NORM),
     )
 
-def step_rows(fac, ratio, raw, here, nq, scale):
+
+def step_rows(fac, ratio, raw, here, nq, scale=(1.0, 1.0)):
     for s, cols in ((0, slice(None, nq)), (1, slice(nq, None))):
         raw[:, cols] = jnp.dot(fac[s, here, :], ratio[:, cols], preferred_element_type=F32) * scale[s]
+
+
+def raw_body(nq, fac, ratio, raw):
+    step_rows(fac, ratio, raw, rows_at(lax.axis_index("fs"), raw.shape[0]), nq)
+
 
 def put(raw, qc, vc, slot, here, cols, w):
     nq = qc.shape[2]
@@ -186,49 +197,48 @@
     return moves
 
 def final_body(nt, *refs):
-    fac, ratio, tot, tot_in, wq, wv = refs[:6]
-    near, far = refs[6:8], refs[8:-14]
-    qd_h, vd_h, qm_h, vm_h, qc_h, vc_h, raw, qd, vd, qm, vm, qc, vc, sem = refs[-14:]
+    fac, ratio, tot, tot_in, raw_own, wq, wv = refs[:7]
+    far = refs[7:-15]
+    qd_h, vd_h, qm_h, vm_h, qc_h, vc_h, raw_last, raw, qd, vd, qm, vm, qc, vc, sem = refs[-15:]
     f = lax.axis_index("fs")
     dl, nq, nv = wq.shape[0], wq.shape[1], wv.shape[1]
     scale = scales(fac, tot, tot_in, nq, nv, nt)
     stores = []
-    for k in range(2 + len(far) // 5):
-        step_rows(fac, ratio, raw, rows_at(f ^ k, dl), nq, scale)
-        if k == 0:
-            qd[...] = raw[:, :nq]
-            vd[...] = raw[:, nq:]
-            qm[...] = wq[...] - RATE * raw[:, :nq]
-            vm[...] = wv[...] - RATE * raw[:, nq:]
-            put(raw, qc, vc, 0, slice(None), slice(0, nq), wq[...].astype(BF))
-            put(raw, qc, vc, 0, slice(None), slice(nq, nq + nv), wv[...].astype(BF))
-            stores += [
-                pltpu.make_async_copy(qd, qd_h, sem.at[0]),
-                pltpu.make_async_copy(vd, vd_h, sem.at[1]),
-                pltpu.make_async_copy(qm, qm_h, sem.at[2]),
-                pltpu.make_async_copy(vm, vm_h, sem.at[3]),
-            ]
-            for c in stores:
-                c.start()
-        elif k == 1:
-            put(raw, qc, vc, 1, slice(0, dl // 2), slice(0, nq + nv), near[0][...])
-            put(raw, qc, vc, 1, slice(dl // 2, dl), slice(0, nq + nv), near[1][...])
-        else:
-            put_far(raw, qc, vc, k, far[5 * (k - 2) : 5 * (k - 1)])
-        stores += send(qc, vc, qc_h, vc_h, k, rows_at(f ^ k, dl), sem, 4 + 2 * k)
+    for n, (here, w, dr, ms) in enumerate(((slice(0, nq), wq, qd, qm), (slice(nq, nq + nv), wv, vd, vm))):
+        dr[...] = raw_own[:, here] * scale[n]
+        stores.append(pltpu.make_async_copy(dr, (qd_h, vd_h)[n], sem.at[n]))
+        stores[-1].start()
+        ms[...] = w[...] - RATE * dr[...]
+        stores.append(pltpu.make_async_copy(ms, (qm_h, vm_h)[n], sem.at[2 + n]))
+        stores[-1].start()
+        put_own(dr, (qc, vc)[n], w)
+    stores += send(qc, vc, qc_h, vc_h, 0, rows_at(f, dl), sem, 4)
+    step_rows(fac, ratio, raw, rows_at(f ^ 2, dl), nq, scale)
+    put_far(raw, qc, vc, 1, far)
+    stores += send(qc, vc, qc_h, vc_h, 1, rows_at(f ^ 2, dl), sem, 6)
+    for n, k in enumerate((1, 3)):
+        step_rows(fac, ratio, raw_last.at[n], rows_at(f ^ k, dl), nq, scale)
     for c in stores:
         c.wait()
 
-def last_body(k, nt, *refs):
-    fac, ratio, tot, tot_in = refs[:4]
-    far, (qc_h, vc_h, raw, qc, vc, sem) = refs[4:9], refs[11:]
+
+def put_own(step, copy, w):
+    copy[0] = (w[...].astype(BF).astype(F32) - RATE * step[...]).astype(BF)
+
+
+def last_body(raw, *refs):
+    near, far, (qc_h, vc_h, qc, vc, sem) = refs[:2], refs[2:7], refs[9:]
     f = lax.axis_index("fs")
-    dl, nq, nv = qc.shape[1], qc.shape[2], vc.shape[2]
-    here = rows_at(f ^ k, dl)
-    step_rows(fac, ratio, raw, here, nq, scales(fac, tot, tot_in, nq, nv, nt))
-    put_far(raw, qc, vc, 0, far)
-    for c in send(qc, vc, qc_h, vc_h, 0, here, sem, 0):
+    dl, whole = qc.shape[1], slice(0, raw.shape[2])
+    cut = near[0].shape[0]
+    put(raw.at[0], qc, vc, 0, slice(0, cut), whole, near[0][...])
+    put(raw.at[0], qc, vc, 0, slice(cut, dl), whole, near[1][...])
+    stores = send(qc, vc, qc_h, vc_h, 0, rows_at(f ^ 1, dl), sem, 0)
+    put_far(raw.at[1], qc, vc, 1, far)
+    stores += send(qc, vc, qc_h, vc_h, 1, rows_at(f ^ 3, dl), sem, 2)
+    for c in stores:
         c.wait()
+
 
 def exchange(nf, nr, nt, xs, cq, cv, wq, wv, fq, fv, q1, q2, v1, v2):
     S = jax.ShapeDtypeStruct
@@ -240,24 +250,27 @@
     piece = dl // nr
     tokens = xs.shape[0]
 
-    (start,) = call(functools.partial(first_body, nr), [S((piece, rank), BF)], 2, [pltpu.SemaphoreType.DMA], limit=60, in_specs=[ANY] * 2)(fq, fv)
+    mine_at = lax.axis_index("rep") * piece
+    start = jnp.where(
+        lax.axis_index("tp") == 0,
+        lax.dynamic_slice_in_dim(fq, mine_at, piece, 0),
+        lax.dynamic_slice_in_dim(fv, mine_at, piece, 0),
+    )
     zs = [swap(start, "fs", nf, k) for k in range(1, nf)]
     stacked = jnp.stack(zs)
     mine = [stacked] + [swap(stacked, "rep", nr, j) for j in range(1, nr)]
     other = [swap(m, "tp", nt, 1) for m in mine]
 
-    quarter, low, high = call(
-        functools.partial(pack_body, nr),
-        [S((piece, nc), BF)] + [S((dl // 2, nc), BF)] * 2,
-        2,
-        [pltpu.VMEM((dl, nq), F32), pltpu.VMEM((dl, nv), F32), pltpu.SemaphoreType.DMA((2,))],
-        in_specs=[ANY] * 2,
-        limit=12,
-    )(wq, wv)
+    quarter = jnp.concatenate(
+        [lax.dynamic_slice_in_dim(w, mine_at, piece, 0).astype(BF) for w in (wq, wv)], axis=1
+    )
+    early = EARLY * dl // 16
+    low, high = call(pack_body, [S((early, nc), BF), S((dl - early, nc), BF)], 2, limit=12)(wq, wv)
     near = [swap(low, "fs", nf, 1), swap(high, "fs", nf, 1)]
     far = []
+    own_z = quarter
     for k in range(2, nf):
-        own_z = swap(quarter, "fs", nf, k)
+        own_z = swap(own_z, "fs", nf, 2 if k == 2 else 1)
         fa, fb = own_z[:, :half], own_z[:, half:]
         xa = swap(fa, "rep", nr, 1)
         yb = swap(fb, "rep", nr, 2)
@@ -267,15 +280,23 @@
 
     cot = jnp.concatenate([cq, cv], axis=1)
     h = rank // nr
+    y_mine, fac_mine = call(
+        functools.partial(lift_body, nf, nr),
+        [S((tokens, rank), BF), S((d, rank), BF)],
+        3 + nr,
+        limit=12,
+        flops=2 * tokens * d * rank,
+        nbytes=2 * (tokens * d + 2 * d * rank),
+    )(xs, fq, fv, *mine)
     *parts, fac = call(
         functools.partial(project_body, nf, nr, nq),
         [S((h, nc), BF)] * nr + [S((2, d, rank), BF)],
-        4 + 2 * nr,
-        [pltpu.VMEM((rank, nc), BF)],
+        6 + nr,
+        [pltpu.VMEM((2, tokens, rank), BF), pltpu.VMEM((rank, nc), BF)],
         limit=24,
-        flops=2 * tokens * (d * 2 * rank + rank * nc),
+        flops=2 * tokens * (d * rank + rank * nc),
         nbytes=2 * (tokens * (d + nc) + 4 * d * rank),
-    )(xs, fq, fv, cot, *mine, *other)
+    )(xs, fq, fv, cot, y_mine, fac_mine, *other)
     (gram,) = call(gram_body, [S((2, rank, rank), F32)], 1, flops=4 * d * rank * rank, nbytes=4 * d * rank)(fac)
 
     got = [parts[0]] + [swap(parts[j], "rep", nr, j) for j in range(1, nr)]
@@ -300,44 +321,51 @@
         functools.partial(total_body, nr, nq), [S((rank, nc), BF), S((16, 128), F32)], nr + 1, limit=12
     )(*got, gram)
     total_in = swap(total, "tp", nt, 1)
-    given = (fac, ratios, total, total_in)
-    qd, vd, qm, vm, qc, vc = call(
+    (raw_own,) = call(
+        functools.partial(raw_body, nq),
+        [S((dl, nc), F32)],
+        2,
+        limit=12,
+        flops=2 * dl * rank * nc,
+        nbytes=2 * (2 * d * rank + rank * nc) + 4 * dl * nc,
+    )(fac, ratios)
+    qd, vd, qm, vm, qc, vc, raw_last = call(
         functools.partial(final_body, nt),
-        [S((dl, nq), F32), S((dl, nv), F32)] * 2 + [S((d, nq), BF), S((d, nv), BF)],
-        8 + 5 * (nf - 3),
+        [S((dl, nq), F32), S((dl, nv), F32)] * 2 + [S((d, nq), BF), S((d, nv), BF), S((2, dl, nc), F32)],
+        12,
         [
             pltpu.VMEM((dl, nc), F32),
             pltpu.VMEM((dl, nq), F32),
             pltpu.VMEM((dl, nv), F32),
             pltpu.VMEM((dl, nq), F32),
             pltpu.VMEM((dl, nv), F32),
-            pltpu.VMEM((nf - 1, dl, nq), BF),
-            pltpu.VMEM((nf - 1, dl, nv), BF),
-            pltpu.SemaphoreType.DMA((4 + 2 * nf,)),
+            pltpu.VMEM((2, dl, nq), BF),
+            pltpu.VMEM((2, dl, nv), BF),
+            pltpu.SemaphoreType.DMA((8,)),
         ],
         limit=30,
-        out_specs=[ANY] * 6,
+        out_specs=[ANY] * 6 + [VMEM],
         flops=2 * d * rank * nc,
         nbytes=2 * d * nc * 2 + 12 * dl * nc,
-    )(*given, wq, wv, *near, *far[:-5])
+    )(fac, ratios, total, total_in, raw_own, wq, wv, *far[:5])
     qc, vc = call(
-        functools.partial(last_body, nf - 1, nt),
+        last_body,
         [S((d, nq), BF), S((d, nv), BF)],
-        11,
+        10,
         [
-            pltpu.VMEM((dl, nc), F32),
-            pltpu.VMEM((1, dl, nq), BF),
-            pltpu.VMEM((1, dl, nv), BF),
-            pltpu.SemaphoreType.DMA((2,)),
+            pltpu.VMEM((2, dl, nq), BF),
+            pltpu.VMEM((2, dl, nv), BF),
+            pltpu.SemaphoreType.DMA((4,)),
         ],
         limit=16,
-        in_specs=[VMEM] * 9 + [ANY] * 2,
+        in_specs=[VMEM] * 8 + [ANY] * 2,
         out_specs=[ANY] * 2,
-        flops=2 * dl * rank * nc,
-        nbytes=2 * dl * nc * 2,
-        aliases={9: 0, 10: 1},
-    )(*given, *far[-5:], qc, vc)
+        flops=4 * dl * nc,
+        nbytes=8 * dl * nc,
+        aliases={8: 0, 9: 1},
+    )(raw_last, *near, *far[5:], qc, vc)
     return qd, vd, qm, vm, qc, vc, q1n, q2n, v1n, v2n
+
 
 def moments(projected, first, second):
     first_new = BETA_ONE * first + (1.0 - BETA_ONE) * projected

time: 128 us -> 118 us (0.922)
  waiting for transfers between devices: 69.6 us -> 60.1 us
  Pallas kernels: 16.9 us -> 14.1 us
  other arithmetic: 0.35 us -> 2.51 us
    ppermute x35, waiting for transfers between devices: 69.6 us -> 60.1 us  [swap(): return lax.ppermute(x, axis, [(i, i ^ k) for i in range(n)])]
    unnamed x26 -> x20, local copies, waits for them, and re-layouts: 2.88 us -> 0.06 us
    convert_element_type x0 -> x2, local copies, waits for them, and re-layouts: none -> 2.05 us  [exchange(): lax.dynamic_slice_in_dim(w, mine_at, piece, 0).astype(BF)]
    pallas_call x1, Pallas kernels: 4.67 us -> 3.09 us  [exchange(): call(functools.partial(project_body, nf, nr, nq), [S((h, nc), BF)] * nr +...]
    pallas_call x3 -> x4, Pallas kernels: 4.1 us -> 3.67 us  [the longest x1 1.88 us: exchange(): call(last_body, [S((d, nq), BF), S((d, nv), BF)], 10, [pltpu.VMEM((2, dl,...]
  transfers between devices with their start and end apart: 35 -> 35, of which waited for: 18 -> 17; matrix products, arithmetic and copies ran while one was open for 0% -> 3% of each run, Pallas kernels for 10% -> 10%
where the time goes in v2:
time: 118 us
  waiting for transfers between devices  60.1 us (51%)
  starting transfers between devices  37.8 us (32%)
  Pallas kernels  14.1 us (12%)
  other arithmetic  2.51 us (2%)
  local copies, waits for them, and re-layouts  2.21 us (2%)
    ppermute x35, waiting for transfers between devices, swap(): return lax.ppermute(x, axis, [(i, i ^ k) for i in range(n)])  60.1 us
    ppermute x35, starting transfers between devices, swap(): return lax.ppermute(x, axis, [(i, i ^ k) for i in range(n)])  37.8 us
    pallas_call x1, Pallas kernels, exchange(): call(functools.partial(final_body, nt), [S((dl, nq), F32), S((dl, nv), F3...  4.21 us
    pallas_call x1, Pallas kernels, exchange(): call(functools.partial(project_body, nf, nr, nq), [S((h, nc), BF)] * nr +...  3.09 us
  transfers between devices with their start and end apart: 35, of which 17 were waited for; matrix products, arithmetic and copies ran while one was open for 3% of the time, Pallas kernels for 10%

profile of v2, /device:TPU:0, one launch (start us, length us, event | category | flops | bytes accessed | tf_op | source)
XLA Modules:
  0.0 117.8 jit_solution(12037113396545490852)
XLA Ops:
  1.7 5.1 %collective-permute-start.2 = (bf16[128,256]{1,0:T(8,128)(2,1)S(1)}, bf16[128,256]{1,0:T(8,128)(2,1)S(1)}, u32[]{:S(2)}, u32[]{:S(2)}) collective-permute-start(bf16[128,256]{1,0:T(8,128)(2,1)S(1)} %dynamic-slice_select_fusion), channel_id=1, source_target_pairs={{0,24},{8,16},{16,8},{24,0},{1,25},{9,17},{17,9},{25,1},{2,26},{10... | collective-permute-start | bytes 196616 | tf_op jit(solution)/shard_map/ppermute | solution.py:26
  9.5 2.9 %collective-permute-done.1 = bf16[128,256]{1,0:T(8,128)(2,1)S(1)} collective-permute-done((bf16[128,256]{1,0:T(8,128)(2,1)S(1)}, bf16[128,256]{1,0:T(8,128)(2,1)S(1)}, u32[]{:S(2)}, u32[]{:S(2)}) %collective-permute-start.1) | collective-permute-done | bytes 65568 | tf_op jit(solution)/shard_map/ppermute | solution.py:26
  12.4 1.6 %collective-permute-start.3 = (bf16[3,128,256]{2,1,0:T(8,128)(2,1)S(1)}, bf16[3,128,256]{2,1,0:T(8,128)(2,1)S(1)}, u32[]{:S(2)}, u32[]{:S(2)}) collective-permute-start(bf16[3,128,256]{2,1,0:T(8,128)(2,1)S(1)} %pad_maximum_fusion.6.refs_0_), channel_id=1, source_target_pairs={{0,2},{2,0},{4,6},{6,4},{1,3},{3,1},{5,7},{7,5},{8,10},{10,8},{12,... | collective-permute-start | bytes 589832 | tf_op jit(solution)/shard_map/ppermute | solution.py:26
  14.0 1.5 %collective-permute-start.4 = (bf16[3,128,256]{2,1,0:T(8,128)(2,1)S(1)}, bf16[3,128,256]{2,1,0:T(8,128)(2,1)S(1)}, u32[]{:S(2)}, u32[]{:S(2)}) collective-permute-start(bf16[3,128,256]{2,1,0:T(8,128)(2,1)S(1)} %pad_maximum_fusion.6.refs_0_), channel_id=1, source_target_pairs={{0,4},{2,6},{4,0},{6,2},{1,5},{3,7},{5,1},{7,3},{8,12},{10,14},{12... | collective-permute-start | bytes 589832 | tf_op jit(solution)/shard_map/ppermute | solution.py:26
  16.1 1.6 %collective-permute-start.23 = (bf16[128,1536]{1,0:T(8,128)(2,1)S(1)}, bf16[128,1536]{1,0:T(8,128)(2,1)S(1)}, u32[]{:S(2)}, u32[]{:S(2)}) collective-permute-start(bf16[128,1536]{1,0:T(8,128)(2,1)S(1)} %pad_maximum_fusion.1), channel_id=1, source_target_pairs={{0,16},{8,24},{16,0},{24,8},{1,17},{9,25},{17,1},{25,9},{2,18},{10... | collective-permute-start | bytes 1179656 | tf_op jit(solution)/shard_map/ppermute | solution.py:26
  17.7 2.6 %collective-permute-done.3.refs_1_ = bf16[3,128,256]{2,1,0:T(8,128)(2,1)S(1)} collective-permute-done((bf16[3,128,256]{2,1,0:T(8,128)(2,1)S(1)}, bf16[3,128,256]{2,1,0:T(8,128)(2,1)S(1)}, u32[]{:S(2)}, u32[]{:S(2)}) %collective-permute-start.3) | collective-permute-done | bytes 196640 | tf_op jit(solution)/shard_map/ppermute | solution.py:26
  20.3 4.2 %collective-permute-done.4.refs_2_ = bf16[3,128,256]{2,1,0:T(8,128)(2,1)S(1)} collective-permute-done((bf16[3,128,256]{2,1,0:T(8,128)(2,1)S(1)}, bf16[3,128,256]{2,1,0:T(8,128)(2,1)S(1)}, u32[]{:S(2)}, u32[]{:S(2)}) %collective-permute-start.4) | collective-permute-done | bytes 196640 | tf_op jit(solution)/shard_map/ppermute | solution.py:26
  25.0 1.3 %pad_maximum_fusion.cot = bf16[768,1536]{1,0:T(8,128)(2,1)S(1)} fusion(bf16[768,1024]{1,0:T(8,128)(2,1)S(1)} %copy-done.9, bf16[768,512]{1,0:T(8,128)(2,1)} %param.12), kind=kLoop, calls=%fused_computation | loop fusion | flops 4718592 | bytes 4718592 | tf_op jit(solution)/shard_map/concatenate | solution.py:281
  27.5 3.1 %shard_map.187 = (bf16[64,1536]{1,0:T(8,128)(2,1)S(1)}, bf16[64,1536]{1,0:T(8,128)(2,1)S(1)}, bf16[64,1536]{1,0:T(8,128)(2,1)S(1)}, bf16[64,1536]{1,0:T(8,128)(2,1)S(1)}, bf16[2,2048,256]{2,1,0:T(8,128)(2,1)S(1)}) custom-call(bf16[768,2048]{1,0:T(8,128)(2,1)S(1)} %copy-done, bf16[512,256]{1,0:T(8,128)(2,1)S(1)} %copy-done.3, bf16[512,256]{1,0:T(8,128)(2,1)S(1)} %copy-done.4, ...), custom_call_target="tpu_custom_call" | custom-call | flops 1409286144 | bytes 9699328 | tf_op jit(solution)/shard_map/pallas_call | solution.py:291
  31.4 1.4 %collective-permute-start.11 = (bf16[64,1536]{1,0:T(8,128)(2,1)S(1)}, bf16[64,1536]{1,0:T(8,128)(2,1)S(1)}, u32[]{:S(2)}, u32[]{:S(2)}) collective-permute-start(bf16[64,1536]{1,0:T(8,128)(2,1)S(1)} %get-tuple-element.44), channel_id=1, source_target_pairs={{0,4},{2,6},{4,0},{6,2},{1,5},{3,7},{5,1},{7,3},{8,12},{10,14},{12... | collective-permute-start | bytes 589832 | tf_op jit(solution)/shard_map/ppermute | solution.py:26
  32.8 1.4 %collective-permute-start.12 = (bf16[64,1536]{1,0:T(8,128)(2,1)S(1)}, bf16[64,1536]{1,0:T(8,128)(2,1)S(1)}, u32[]{:S(2)}, u32[]{:S(2)}) collective-permute-start(bf16[64,1536]{1,0:T(8,128)(2,1)S(1)} %get-tuple-element.45), channel_id=1, source_target_pairs={{0,6},{2,4},{4,2},{6,0},{1,7},{3,5},{5,3},{7,1},{8,14},{10,12},{12... | collective-permute-start | bytes 589832 | tf_op jit(solution)/shard_map/ppermute | solution.py:26
  34.9 3.6 %collective-permute-done.10.refs_1_ = bf16[64,1536]{1,0:T(8,128)(2,1)S(1)} collective-permute-done((bf16[64,1536]{1,0:T(8,128)(2,1)S(1)}, bf16[64,1536]{1,0:T(8,128)(2,1)S(1)}, u32[]{:S(2)}, u32[]{:S(2)}) %collective-permute-start.10) | collective-permute-done | bytes 196640 | tf_op jit(solution)/shard_map/ppermute | solution.py:26
  38.5 2.6 %collective-permute-done.11.refs_2_ = bf16[64,1536]{1,0:T(8,128)(2,1)S(1)} collective-permute-done((bf16[64,1536]{1,0:T(8,128)(2,1)S(1)}, bf16[64,1536]{1,0:T(8,128)(2,1)S(1)}, u32[]{:S(2)}, u32[]{:S(2)}) %collective-permute-start.11) | collective-permute-done | bytes 196640 | tf_op jit(solution)/shard_map/ppermute | solution.py:26
  41.0 1.6 %collective-permute-done.12.refs_3_ = bf16[64,1536]{1,0:T(8,128)(2,1)S(1)} collective-permute-done((bf16[64,1536]{1,0:T(8,128)(2,1)S(1)}, bf16[64,1536]{1,0:T(8,128)(2,1)S(1)}, u32[]{:S(2)}, u32[]{:S(2)}) %collective-permute-start.12) | collective-permute-done | bytes 196640 | tf_op jit(solution)/shard_map/ppermute | solution.py:26
  43.0 2.0 %collective-permute-start.14 = (bf16[16,1536]{1,0:T(8,128)(2,1)S(1)}, bf16[16,1536]{1,0:T(8,128)(2,1)S(1)}, u32[]{:S(2)}, u32[]{:S(2)}) collective-permute-start(bf16[16,1536]{1,0:T(8,128)(2,1)S(1)} %get-tuple-element.48), channel_id=1, source_target_pairs={{0,16},{8,24},{16,0},{24,8},{1,17},{9,25},{17,1},{25,9},{2,18},{10... | collective-permute-start | bytes 147464 | tf_op jit(solution)/shard_map/ppermute | solution.py:26
  45.0 2.3 %collective-permute-start.15 = (bf16[16,1536]{1,0:T(8,128)(2,1)S(1)}, bf16[16,1536]{1,0:T(8,128)(2,1)S(1)}, u32[]{:S(2)}, u32[]{:S(2)}) collective-permute-start(bf16[16,1536]{1,0:T(8,128)(2,1)S(1)} %get-tuple-element.49), channel_id=1, source_target_pairs={{0,24},{8,16},{16,8},{24,0},{1,25},{9,17},{17,9},{25,1},{2,26},{10... | collective-permute-start | bytes 147464 | tf_op jit(solution)/shard_map/ppermute | solution.py:26
  48.0 3.4 %collective-permute-done.15.refs_3_ = bf16[16,1536]{1,0:T(8,128)(2,1)S(1)} collective-permute-done((bf16[16,1536]{1,0:T(8,128)(2,1)S(1)}, bf16[16,1536]{1,0:T(8,128)(2,1)S(1)}, u32[]{:S(2)}, u32[]{:S(2)}) %collective-permute-start.15) | collective-permute-done | bytes 49184 | tf_op jit(solution)/shard_map/ppermute | solution.py:26
  51.5 2.9 %collective-permute-start.17 = (bf16[16,1536]{1,0:T(8,128)(2,1)S(1)}, bf16[16,1536]{1,0:T(8,128)(2,1)S(1)}, u32[]{:S(2)}, u32[]{:S(2)}) collective-permute-start(bf16[16,1536]{1,0:T(8,128)(2,1)S(1)} %shard_map.189.refs_0_), channel_id=1, source_target_pairs={{0,16},{8,24},{16,0},{24,8},{1,17},{9,25},{17,1},{25,9},{2,18},{10... | collective-permute-start | bytes 147464 | tf_op jit(solution)/shard_map/ppermute | solution.py:26
  54.4 1.5 %collective-permute-start.18 = (bf16[16,1536]{1,0:T(8,128)(2,1)S(1)}, bf16[16,1536]{1,0:T(8,128)(2,1)S(1)}, u32[]{:S(2)}, u32[]{:S(2)}) collective-permute-start(bf16[16,1536]{1,0:T(8,128)(2,1)S(1)} %shard_map.189.refs_0_), channel_id=1, source_target_pairs={{0,24},{8,16},{16,8},{24,0},{1,25},{9,17},{17,9},{25,1},{2,26},{10... | collective-permute-start | bytes 147464 | tf_op jit(solution)/shard_map/ppermute | solution.py:26
  55.9 19.0 %collective-permute-done.16.refs_1_ = bf16[16,1536]{1,0:T(8,128)(2,1)S(1)} collective-permute-done((bf16[16,1536]{1,0:T(8,128)(2,1)S(1)}, bf16[16,1536]{1,0:T(8,128)(2,1)S(1)}, u32[]{:S(2)}, u32[]{:S(2)}) %collective-permute-start.16) | collective-permute-done | bytes 49184 | tf_op jit(solution)/shard_map/ppermute | solution.py:26
  74.9 1.5 %collective-permute-start.24 = (bf16[128,768]{1,0:T(8,128)(2,1)S(1)}, bf16[128,768]{1,0:T(8,128)(2,1)S(1)}, u32[]{:S(2)}, u32[]{:S(2)}) collective-permute-start(bf16[128,768]{1,0:T(8,128)(2,1)S(1)} %get-tuple-element.75), channel_id=1, source_target_pairs={{0,2},{2,0},{4,6},{6,4},{1,3},{3,1},{5,7},{7,5},{8,10},{10,8},{12,... | collective-permute-start | bytes 589832 | tf_op jit(solution)/shard_map/ppermute | solution.py:26
  76.4 1.5 %collective-permute-start.25 = (bf16[128,768]{1,0:T(8,128)(2,1)S(1)}, bf16[128,768]{1,0:T(8,128)(2,1)S(1)}, u32[]{:S(2)}, u32[]{:S(2)}) collective-permute-start(bf16[128,768]{1,0:T(8,128)(2,1)S(1)} %get-tuple-element.74), channel_id=1, source_target_pairs={{0,4},{2,6},{4,0},{6,2},{1,5},{3,7},{5,1},{7,3},{8,12},{10,14},{12... | collective-permute-start | bytes 589832 | tf_op jit(solution)/shard_map/ppermute | solution.py:26
  80.1 1.7 %collective-permute-done.24.refs_8_ = bf16[128,768]{1,0:T(8,128)(2,1)S(1)} collective-permute-done((bf16[128,768]{1,0:T(8,128)(2,1)S(1)}, bf16[128,768]{1,0:T(8,128)(2,1)S(1)}, u32[]{:S(2)}, u32[]{:S(2)}) %collective-permute-start.24) | collective-permute-done | bytes 196640 | tf_op jit(solution)/shard_map/ppermute | solution.py:26
  81.8 3.3 %collective-permute-start.21 = (bf16[64,1536]{1,0:T(8,128)(2,1)S(1)}, bf16[64,1536]{1,0:T(8,128)(2,1)S(1)}, u32[]{:S(2)}, u32[]{:S(2)}) collective-permute-start(bf16[64,1536]{1,0:T(8,128)(2,1)S(1)} %get-tuple-element.50.refs_0_), channel_id=1, source_target_pairs={{0,6},{2,4},{4,2},{6,0},{1,7},{3,5},{5,3},{7,1},{8,14},{10,12},{12... | collective-permute-start | bytes 589832 | tf_op jit(solution)/shard_map/ppermute | solution.py:26
  86.8 1.6 %collective-permute-start.26 = (bf16[2,128,768]{2,1,0:T(8,128)(2,1)S(1)}, bf16[2,128,768]{2,1,0:T(8,128)(2,1)S(1)}, u32[]{:S(2)}, u32[]{:S(2)}) collective-permute-start(bf16[2,128,768]{2,1,0:T(8,128)(2,1)S(1)} %pad_maximum_fusion.2), channel_id=1, source_target_pairs={{0,4},{2,6},{4,0},{6,2},{1,5},{3,7},{5,1},{7,3},{8,12},{10,14},{12... | collective-permute-start | bytes 1179656 | tf_op jit(solution)/shard_map/ppermute | solution.py:26
  89.2 1.9 %collective-permute-done.20.refs_2_ = bf16[64,1536]{1,0:T(8,128)(2,1)S(1)} collective-permute-done((bf16[64,1536]{1,0:T(8,128)(2,1)S(1)}, bf16[64,1536]{1,0:T(8,128)(2,1)S(1)}, u32[]{:S(2)}, u32[]{:S(2)}) %collective-permute-start.20) | collective-permute-done | bytes 196640 | tf_op jit(solution)/shard_map/ppermute | solution.py:26
  91.1 1.6 %collective-permute-start.32 = (bf16[128,768]{1,0:T(8,128)(2,1)S(1)}, bf16[128,768]{1,0:T(8,128)(2,1)S(1)}, u32[]{:S(2)}, u32[]{:S(2)}) collective-permute-start(bf16[128,768]{1,0:T(8,128)(2,1)S(1)} %get-tuple-element.70), channel_id=1, source_target_pairs={{0,4},{2,6},{4,0},{6,2},{1,5},{3,7},{5,1},{7,3},{8,12},{10,14},{12... | collective-permute-start | bytes 589832 | tf_op jit(solution)/shard_map/ppermute | solution.py:26
  92.8 1.2 shard_map.192
  94.6 8.1 %collective-permute-done.32.refs_4_ = bf16[128,768]{1,0:T(8,128)(2,1)S(1)} collective-permute-done((bf16[128,768]{1,0:T(8,128)(2,1)S(1)}, bf16[128,768]{1,0:T(8,128)(2,1)S(1)}, u32[]{:S(2)}, u32[]{:S(2)}) %collective-permute-start.32) | collective-permute-done | bytes 196640 | tf_op jit(solution)/shard_map/ppermute | solution.py:26
  106.5 4.2 %shard_map.194 = (f32[512,512]{1,0:T(8,128)}, f32[512,1024]{1,0:T(8,128)}, f32[512,512]{1,0:T(8,128)}, f32[512,1024]{1,0:T(8,128)}, bf16[2048,512]{1,0:T(8,128)(...) custom-call(bf16[2,2048,256]{2,1,0:T(8,128)(2,1)S(1)} %get-tuple-element.41.fac.refs_0_, ...), custom_call_target="tpu_custom_call" | custom-call | flops 1610612736 | bytes 22020096 | tf_op jit(solution)/shard_map/pallas_call | solution.py:332
  110.7 4.3 %collective-permute-done.33.refs_5_ = bf16[2,128,768]{2,1,0:T(8,128)(2,1)S(1)} collective-permute-done((bf16[2,128,768]{2,1,0:T(8,128)(2,1)S(1)}, bf16[2,128,768]{2,1,0:T(8,128)(2,1)S(1)}, u32[]{:S(2)}, u32[]{:S(2)}) %collective-permute-start.33) | collective-permute-done | bytes 393248 | tf_op jit(solution)/shard_map/ppermute | solution.py:26
  115.9 1.9 %shard_map.196 = (bf16[2048,512]{1,0:T(8,128)(2,1)}, bf16[2048,1024]{1,0:T(8,128)(2,1)}) custom-call(f32[2,512,1536]{2,1,0:T(8,128)S(1)} %get-tuple-element.61.raw, bf16[160,1536]{1,0:T(8,128)(2,1)S(1)} %collective-permute-done.28.refs_0_, bf16[352,1536]{1,0:T(8,128)(2,1)S(1)} %collective-permute-done.29.refs_1_, ...), custom_call_target="tpu_custom_call", output_to_operand_aliasing={{0}: (8, {}), {1}: (9, {})} | custom-call | flops 3145728 | bytes 6291456 | tf_op jit(solution)/shard_map/pallas_call | solution.py:351
  (81 shorter events, 18.3 us)
Async XLA Ops:
  1.7 7.8 %collective-permute-start.2 = (bf16[128,256]{1,0:T(8,128)(2,1)S(1)}, bf16[128,256]{1,0:T(8,128)(2,1)S(1)}, u32[]{:S(2)}, u32[]{:S(2)}) collective-permute-start(bf16[128,256]{1,0:T(8,128)(2,1)S(1)} %dynamic-slice_select_fusion), channel_id=1, source_target_pairs={{0,24},{8,16},{16,8},{24,0},{1,25},{9,17},{17,9},{25,1},{2,26},{10... | collective-permute-start | bytes 196616 | tf_op jit(solution)/shard_map/ppermute | solution.py:26
  6.8 5.6 %collective-permute-start.1 = (bf16[128,256]{1,0:T(8,128)(2,1)S(1)}, bf16[128,256]{1,0:T(8,128)(2,1)S(1)}, u32[]{:S(2)}, u32[]{:S(2)}) collective-permute-start(bf16[128,256]{1,0:T(8,128)(2,1)S(1)} %dynamic-slice_select_fusion), channel_id=1, source_target_pairs={{0,16},{8,24},{16,0},{24,8},{1,17},{9,25},{17,1},{25,9},{2,18},{10... | collective-permute-start | bytes 196616 | tf_op jit(solution)/shard_map/ppermute | solution.py:26
  6.8 5.6 %collective-permute-start = (bf16[128,256]{1,0:T(8,128)(2,1)S(1)}, bf16[128,256]{1,0:T(8,128)(2,1)S(1)}, u32[]{:S(2)}, u32[]{:S(2)}) collective-permute-start(bf16[128,256]{1,0:T(8,128)(2,1)S(1)} %dynamic-slice_select_fusion), channel_id=1, source_target_pairs={{0,8},{8,0},{16,24},{24,16},{1,9},{9,1},{17,25},{25,17},{2,10},{10... | collective-permute-start | bytes 196616 | tf_op jit(solution)/shard_map/ppermute | solution.py:26
  12.4 7.8 %collective-permute-start.3 = (bf16[3,128,256]{2,1,0:T(8,128)(2,1)S(1)}, bf16[3,128,256]{2,1,0:T(8,128)(2,1)S(1)}, u32[]{:S(2)}, u32[]{:S(2)}) collective-permute-start(bf16[3,128,256]{2,1,0:T(8,128)(2,1)S(1)} %pad_maximum_fusion.6.refs_0_), channel_id=1, source_target_pairs={{0,2},{2,0},{4,6},{6,4},{1,3},{3,1},{5,7},{7,5},{8,10},{10,8},{12,... | collective-permute-start | bytes 589832 | tf_op jit(solution)/shard_map/ppermute | solution.py:26
  14.0 10.5 %collective-permute-start.4 = (bf16[3,128,256]{2,1,0:T(8,128)(2,1)S(1)}, bf16[3,128,256]{2,1,0:T(8,128)(2,1)S(1)}, u32[]{:S(2)}, u32[]{:S(2)}) collective-permute-start(bf16[3,128,256]{2,1,0:T(8,128)(2,1)S(1)} %pad_maximum_fusion.6.refs_0_), channel_id=1, source_target_pairs={{0,4},{2,6},{4,0},{6,2},{1,5},{3,7},{5,1},{7,3},{8,12},{10,14},{12... | collective-permute-start | bytes 589832 | tf_op jit(solution)/shard_map/ppermute | solution.py:26
  15.5 9.0 %collective-permute-start.5 = (bf16[3,128,256]{2,1,0:T(8,128)(2,1)S(1)}, bf16[3,128,256]{2,1,0:T(8,128)(2,1)S(1)}, u32[]{:S(2)}, u32[]{:S(2)}) collective-permute-start(bf16[3,128,256]{2,1,0:T(8,128)(2,1)S(1)} %pad_maximum_fusion.6.refs_0_), channel_id=1, source_target_pairs={{0,6},{2,4},{4,2},{6,0},{1,7},{3,5},{5,3},{7,1},{8,14},{10,12},{12... | collective-permute-start | bytes 589832 | tf_op jit(solution)/shard_map/ppermute | solution.py:26
  16.1 18.8 %collective-permute-start.23 = (bf16[128,1536]{1,0:T(8,128)(2,1)S(1)}, bf16[128,1536]{1,0:T(8,128)(2,1)S(1)}, u32[]{:S(2)}, u32[]{:S(2)}) collective-permute-start(bf16[128,1536]{1,0:T(8,128)(2,1)S(1)} %pad_maximum_fusion.1), channel_id=1, source_target_pairs={{0,16},{8,24},{16,0},{24,8},{1,17},{9,25},{17,1},{25,9},{2,18},{10... | collective-permute-start | bytes 1179656 | tf_op jit(solution)/shard_map/ppermute | solution.py:26
  17.7 9.7 %collective-permute-start.6 = (bf16[3,128,256]{2,1,0:T(8,128)(2,1)S(1)}, bf16[3,128,256]{2,1,0:T(8,128)(2,1)S(1)}, u32[]{:S(2)}, u32[]{:S(2)}) collective-permute-start(bf16[3,128,256]{2,1,0:T(8,128)(2,1)S(1)} %pad_maximum_fusion.6.refs_0_), channel_id=1, source_target_pairs={{0,1},{1,0},{2,3},{3,2},{4,5},{5,4},{6,7},{7,6},{8,9},{9,8},{10,11... | collective-permute-start | bytes 589832 | tf_op jit(solution)/shard_map/ppermute | solution.py:26
  20.3 7.2 %collective-permute-start.7 = (bf16[3,128,256]{2,1,0:T(8,128)(2,1)S(1)}, bf16[3,128,256]{2,1,0:T(8,128)(2,1)S(1)}, u32[]{:S(2)}, u32[]{:S(2)}) collective-permute-start(bf16[3,128,256]{2,1,0:T(8,128)(2,1)S(1)} %collective-permute-done.3.refs_1_), channel_id=1, source_target_pairs={{0,1},{1,0},{2,3},{3,2},{4,5},{5,4},{6,7},{7,6},{8,9},{9,8},{10,11... | collective-permute-start | bytes 589832 | tf_op jit(solution)/shard_map/ppermute | solution.py:26
  30.6 7.8 %collective-permute-start.10 = (bf16[64,1536]{1,0:T(8,128)(2,1)S(1)}, bf16[64,1536]{1,0:T(8,128)(2,1)S(1)}, u32[]{:S(2)}, u32[]{:S(2)}) collective-permute-start(bf16[64,1536]{1,0:T(8,128)(2,1)S(1)} %get-tuple-element.43), channel_id=1, source_target_pairs={{0,2},{2,0},{4,6},{6,4},{1,3},{3,1},{5,7},{7,5},{8,10},{10,8},{12,... | collective-permute-start | bytes 589832 | tf_op jit(solution)/shard_map/ppermute | solution.py:26
  31.4 9.6 %collective-permute-start.11 = (bf16[64,1536]{1,0:T(8,128)(2,1)S(1)}, bf16[64,1536]{1,0:T(8,128)(2,1)S(1)}, u32[]{:S(2)}, u32[]{:S(2)}) collective-permute-start(bf16[64,1536]{1,0:T(8,128)(2,1)S(1)} %get-tuple-element.44), channel_id=1, source_target_pairs={{0,4},{2,6},{4,0},{6,2},{1,5},{3,7},{5,1},{7,3},{8,12},{10,14},{12... | collective-permute-start | bytes 589832 | tf_op jit(solution)/shard_map/ppermute | solution.py:26
  32.8 9.9 %collective-permute-start.12 = (bf16[64,1536]{1,0:T(8,128)(2,1)S(1)}, bf16[64,1536]{1,0:T(8,128)(2,1)S(1)}, u32[]{:S(2)}, u32[]{:S(2)}) collective-permute-start(bf16[64,1536]{1,0:T(8,128)(2,1)S(1)} %get-tuple-element.45), channel_id=1, source_target_pairs={{0,6},{2,4},{4,2},{6,0},{1,7},{3,5},{5,3},{7,1},{8,14},{10,12},{12... | collective-permute-start | bytes 589832 | tf_op jit(solution)/shard_map/ppermute | solution.py:26
  34.9 44.6 %collective-permute-start.30 = (bf16[128,1536]{1,0:T(8,128)(2,1)S(1)}, bf16[128,1536]{1,0:T(8,128)(2,1)S(1)}, u32[]{:S(2)}, u32[]{:S(2)}) collective-permute-start(bf16[128,1536]{1,0:T(8,128)(2,1)S(1)} %collective-permute-done.23.refs_7_), channel_id=1, source_target_pairs={{0,8},{8,0},{16,24},{24,16},{1,9},{9,1},{17,25},{25,17},{2,10},{10... | collective-permute-start | bytes 1179656 | tf_op jit(solution)/shard_map/ppermute | solution.py:26
  42.9 4.7 %collective-permute-start.13 = (bf16[16,1536]{1,0:T(8,128)(2,1)S(1)}, bf16[16,1536]{1,0:T(8,128)(2,1)S(1)}, u32[]{:S(2)}, u32[]{:S(2)}) collective-permute-start(bf16[16,1536]{1,0:T(8,128)(2,1)S(1)} %get-tuple-element.47), channel_id=1, source_target_pairs={{0,8},{8,0},{16,24},{24,16},{1,9},{9,1},{17,25},{25,17},{2,10},{10... | collective-permute-start | bytes 147464 | tf_op jit(solution)/shard_map/ppermute | solution.py:26
  43.0 5.1 %collective-permute-start.14 = (bf16[16,1536]{1,0:T(8,128)(2,1)S(1)}, bf16[16,1536]{1,0:T(8,128)(2,1)S(1)}, u32[]{:S(2)}, u32[]{:S(2)}) collective-permute-start(bf16[16,1536]{1,0:T(8,128)(2,1)S(1)} %get-tuple-element.48), channel_id=1, source_target_pairs={{0,16},{8,24},{16,0},{24,8},{1,17},{9,25},{17,1},{25,9},{2,18},{10... | collective-permute-start | bytes 147464 | tf_op jit(solution)/shard_map/ppermute | solution.py:26
  45.0 6.4 %collective-permute-start.15 = (bf16[16,1536]{1,0:T(8,128)(2,1)S(1)}, bf16[16,1536]{1,0:T(8,128)(2,1)S(1)}, u32[]{:S(2)}, u32[]{:S(2)}) collective-permute-start(bf16[16,1536]{1,0:T(8,128)(2,1)S(1)} %get-tuple-element.49), channel_id=1, source_target_pairs={{0,24},{8,16},{16,8},{24,0},{1,25},{9,17},{17,9},{25,1},{2,26},{10... | collective-permute-start | bytes 147464 | tf_op jit(solution)/shard_map/ppermute | solution.py:26
  47.5 63.3 %collective-permute-start.29 = (bf16[352,1536]{1,0:T(8,128)(2,1)S(1)}, bf16[352,1536]{1,0:T(8,128)(2,1)S(1)}, u32[]{:S(2)}, u32[]{:S(2)}) collective-permute-start(bf16[352,1536]{1,0:T(8,128)(2,1)S(1)} %get-tuple-element.63), channel_id=1, source_target_pairs={{0,8},{8,0},{16,24},{24,16},{1,9},{9,1},{17,25},{25,17},{2,10},{10... | collective-permute-start | bytes 3244040 | tf_op jit(solution)/shard_map/ppermute | solution.py:26
  51.4 23.5 %collective-permute-start.16 = (bf16[16,1536]{1,0:T(8,128)(2,1)S(1)}, bf16[16,1536]{1,0:T(8,128)(2,1)S(1)}, u32[]{:S(2)}, u32[]{:S(2)}) collective-permute-start(bf16[16,1536]{1,0:T(8,128)(2,1)S(1)} %shard_map.189.refs_0_), channel_id=1, source_target_pairs={{0,8},{8,0},{16,24},{24,16},{1,9},{9,1},{17,25},{25,17},{2,10},{10... | collective-permute-start | bytes 147464 | tf_op jit(solution)/shard_map/ppermute | solution.py:26
  51.5 24.9 %collective-permute-start.17 = (bf16[16,1536]{1,0:T(8,128)(2,1)S(1)}, bf16[16,1536]{1,0:T(8,128)(2,1)S(1)}, u32[]{:S(2)}, u32[]{:S(2)}) collective-permute-start(bf16[16,1536]{1,0:T(8,128)(2,1)S(1)} %shard_map.189.refs_0_), channel_id=1, source_target_pairs={{0,16},{8,24},{16,0},{24,8},{1,17},{9,25},{17,1},{25,9},{2,18},{10... | collective-permute-start | bytes 147464 | tf_op jit(solution)/shard_map/ppermute | solution.py:26
  54.4 23.5 %collective-permute-start.18 = (bf16[16,1536]{1,0:T(8,128)(2,1)S(1)}, bf16[16,1536]{1,0:T(8,128)(2,1)S(1)}, u32[]{:S(2)}, u32[]{:S(2)}) collective-permute-start(bf16[16,1536]{1,0:T(8,128)(2,1)S(1)} %shard_map.189.refs_0_), channel_id=1, source_target_pairs={{0,24},{8,16},{16,8},{24,0},{1,25},{9,17},{17,9},{25,1},{2,26},{10... | collective-permute-start | bytes 147464 | tf_op jit(solution)/shard_map/ppermute | solution.py:26
  74.9 6.9 %collective-permute-start.24 = (bf16[128,768]{1,0:T(8,128)(2,1)S(1)}, bf16[128,768]{1,0:T(8,128)(2,1)S(1)}, u32[]{:S(2)}, u32[]{:S(2)}) collective-permute-start(bf16[128,768]{1,0:T(8,128)(2,1)S(1)} %get-tuple-element.75), channel_id=1, source_target_pairs={{0,2},{2,0},{4,6},{6,4},{1,3},{3,1},{5,7},{7,5},{8,10},{10,8},{12,... | collective-permute-start | bytes 589832 | tf_op jit(solution)/shard_map/ppermute | solution.py:26
  76.4 8.7 %collective-permute-start.25 = (bf16[128,768]{1,0:T(8,128)(2,1)S(1)}, bf16[128,768]{1,0:T(8,128)(2,1)S(1)}, u32[]{:S(2)}, u32[]{:S(2)}) collective-permute-start(bf16[128,768]{1,0:T(8,128)(2,1)S(1)} %get-tuple-element.74), channel_id=1, source_target_pairs={{0,4},{2,6},{4,0},{6,2},{1,5},{3,7},{5,1},{7,3},{8,12},{10,14},{12... | collective-permute-start | bytes 589832 | tf_op jit(solution)/shard_map/ppermute | solution.py:26
  79.0 7.8 %collective-permute-start.19 = (bf16[64,1536]{1,0:T(8,128)(2,1)S(1)}, bf16[64,1536]{1,0:T(8,128)(2,1)S(1)}, u32[]{:S(2)}, u32[]{:S(2)}) collective-permute-start(bf16[64,1536]{1,0:T(8,128)(2,1)S(1)} %get-tuple-element.50.refs_0_), channel_id=1, source_target_pairs={{0,2},{2,0},{4,6},{6,4},{1,3},{3,1},{5,7},{7,5},{8,10},{10,8},{12,... | collective-permute-start | bytes 589832 | tf_op jit(solution)/shard_map/ppermute | solution.py:26
  79.5 11.5 %collective-permute-start.20 = (bf16[64,1536]{1,0:T(8,128)(2,1)S(1)}, bf16[64,1536]{1,0:T(8,128)(2,1)S(1)}, u32[]{:S(2)}, u32[]{:S(2)}) collective-permute-start(bf16[64,1536]{1,0:T(8,128)(2,1)S(1)} %get-tuple-element.50.refs_0_), channel_id=1, source_target_pairs={{0,4},{2,6},{4,0},{6,2},{1,5},{3,7},{5,1},{7,3},{8,12},{10,14},{12... | collective-permute-start | bytes 589832 | tf_op jit(solution)/shard_map/ppermute | solution.py:26
  81.8 11.0 %collective-permute-start.21 = (bf16[64,1536]{1,0:T(8,128)(2,1)S(1)}, bf16[64,1536]{1,0:T(8,128)(2,1)S(1)}, u32[]{:S(2)}, u32[]{:S(2)}) collective-permute-start(bf16[64,1536]{1,0:T(8,128)(2,1)S(1)} %get-tuple-element.50.refs_0_), channel_id=1, source_target_pairs={{0,6},{2,4},{4,2},{6,0},{1,7},{3,5},{5,3},{7,1},{8,14},{10,12},{12... | collective-permute-start | bytes 589832 | tf_op jit(solution)/shard_map/ppermute | solution.py:26
  85.1 8.9 %collective-permute-start.31 = (bf16[128,768]{1,0:T(8,128)(2,1)S(1)}, bf16[128,768]{1,0:T(8,128)(2,1)S(1)}, u32[]{:S(2)}, u32[]{:S(2)}) collective-permute-start(bf16[128,768]{1,0:T(8,128)(2,1)S(1)} %get-tuple-element.71), channel_id=1, source_target_pairs={{0,2},{2,0},{4,6},{6,4},{1,3},{3,1},{5,7},{7,5},{8,10},{10,8},{12,... | collective-permute-start | bytes 589832 | tf_op jit(solution)/shard_map/ppermute | solution.py:26
  86.8 18.2 %collective-permute-start.26 = (bf16[2,128,768]{2,1,0:T(8,128)(2,1)S(1)}, bf16[2,128,768]{2,1,0:T(8,128)(2,1)S(1)}, u32[]{:S(2)}, u32[]{:S(2)}) collective-permute-start(bf16[2,128,768]{2,1,0:T(8,128)(2,1)S(1)} %pad_maximum_fusion.2), channel_id=1, source_target_pairs={{0,4},{2,6},{4,0},{6,2},{1,5},{3,7},{5,1},{7,3},{8,12},{10,14},{12... | collective-permute-start | bytes 1179656 | tf_op jit(solution)/shard_map/ppermute | solution.py:26
  91.1 11.7 %collective-permute-start.32 = (bf16[128,768]{1,0:T(8,128)(2,1)S(1)}, bf16[128,768]{1,0:T(8,128)(2,1)S(1)}, u32[]{:S(2)}, u32[]{:S(2)}) collective-permute-start(bf16[128,768]{1,0:T(8,128)(2,1)S(1)} %get-tuple-element.70), channel_id=1, source_target_pairs={{0,4},{2,6},{4,0},{6,2},{1,5},{3,7},{5,1},{7,3},{8,12},{10,14},{12... | collective-permute-start | bytes 589832 | tf_op jit(solution)/shard_map/ppermute | solution.py:26
  92.8 18.0 %collective-permute-start.28 = (bf16[160,1536]{1,0:T(8,128)(2,1)S(1)}, bf16[160,1536]{1,0:T(8,128)(2,1)S(1)}, u32[]{:S(2)}, u32[]{:S(2)}) collective-permute-start(bf16[160,1536]{1,0:T(8,128)(2,1)S(1)} %get-tuple-element.62), channel_id=1, source_target_pairs={{0,8},{8,0},{16,24},{24,16},{1,9},{9,1},{17,25},{25,17},{2,10},{10... | collective-permute-start | bytes 1474568 | tf_op jit(solution)/shard_map/ppermute | solution.py:26
  94.0 12.5 %collective-permute-start.27 = (bf16[2,128,768]{2,1,0:T(8,128)(2,1)S(1)}, bf16[2,128,768]{2,1,0:T(8,128)(2,1)S(1)}, u32[]{:S(2)}, u32[]{:S(2)}) collective-permute-start(bf16[2,128,768]{2,1,0:T(8,128)(2,1)S(1)} %pad_maximum_fusion.3), channel_id=1, source_target_pairs={{0,2},{2,0},{4,6},{6,4},{1,3},{3,1},{5,7},{7,5},{8,10},{10,8},{12,... | collective-permute-start | bytes 1179656 | tf_op jit(solution)/shard_map/ppermute | solution.py:26
  103.9 11.2 %collective-permute-start.33 = (bf16[2,128,768]{2,1,0:T(8,128)(2,1)S(1)}, bf16[2,128,768]{2,1,0:T(8,128)(2,1)S(1)}, u32[]{:S(2)}, u32[]{:S(2)}) collective-permute-start(bf16[2,128,768]{2,1,0:T(8,128)(2,1)S(1)} %pad_maximum_fusion.4), channel_id=1, source_target_pairs={{0,4},{2,6},{4,0},{6,2},{1,5},{3,7},{5,1},{7,3},{8,12},{10,14},{12... | collective-permute-start | bytes 1179656 | tf_op jit(solution)/shard_map/ppermute | solution.py:26
  105.0 10.9 %collective-permute-start.34 = (bf16[2,128,768]{2,1,0:T(8,128)(2,1)S(1)}, bf16[2,128,768]{2,1,0:T(8,128)(2,1)S(1)}, u32[]{:S(2)}, u32[]{:S(2)}) collective-permute-start(bf16[2,128,768]{2,1,0:T(8,128)(2,1)S(1)} %pad_maximum_fusion.5), channel_id=1, source_target_pairs={{0,2},{2,0},{4,6},{6,4},{1,3},{3,1},{5,7},{7,5},{8,10},{10,8},{12,... | collective-permute-start | bytes 1179656 | tf_op jit(solution)/shard_map/ppermute | solution.py:26
  (13 other events, 242.5 us)

commit v3 on v2

--- a/solution.py
+++ b/solution.py
@@ -20,7 +20,7 @@
 VMEM = pl.BlockSpec(memory_space=pltpu.VMEM)
 ANY = pl.BlockSpec(memory_space=pltpu.HBM)
 TILE = 16
-EARLY = 5
+EARLY = 12
 
 def swap(x, axis, n, k):
     return lax.ppermute(x, axis, [(i, i ^ k) for i in range(n)])
@@ -109,24 +109,26 @@
         total += ref[...].astype(F32)
     refs[nf][...] = total.astype(BF)
 
+def advance(p, first, second):
+    first_new = BETA_ONE * first[...] + (1.0 - BETA_ONE) * p
+    return first_new, BETA_TWO * second[...] + (1.0 - BETA_TWO) * p * p
+
+
 def moments_body(nf, nq, *refs):
-    ins = refs[:nf]
-    q1, q2, v1, v2 = refs[nf : nf + 4]
-    q1n, q2n, v1n, v2n, ratio, proj = refs[nf + 4 :]
+    ins, (q1, q2, v1, v2, ratio, proj) = refs[:nf], refs[nf:]
     f = lax.axis_index("fs")
     h = ins[0].shape[0]
     for k in range(nf):
         proj[rows_at(f ^ k, h), :] = ins[k][...].astype(F32)
-    for cols, first, second, fo, so in (
-        (slice(None, nq), q1, q2, q1n, q2n),
-        (slice(nq, None), v1, v2, v1n, v2n),
-    ):
-        p = proj[:, cols]
-        fn = BETA_ONE * first[...] + (1.0 - BETA_ONE) * p
-        sn = BETA_TWO * second[...] + (1.0 - BETA_TWO) * p * p
-        fo[...] = fn
-        so[...] = sn
+    for cols, first, second in ((slice(None, nq), q1, q2), (slice(nq, None), v1, v2)):
+        fn, sn = advance(proj[:, cols], first, second)
         ratio[:, cols] = (fn / (jnp.sqrt(sn) + EPS_RATIO)).astype(BF)
+
+
+def state_body(nq, proj, q1, q2, v1, v2, q1n, q2n, v1n, v2n):
+    q1n[...], q2n[...] = advance(proj[:, :nq], q1, q2)
+    v1n[...], v2n[...] = advance(proj[:, nq:], v1, v2)
+
 
 def gram_body(fac, out):
     dims = (((0,), (0,)), ((), ()))
@@ -264,7 +266,7 @@
     quarter = jnp.concatenate(
         [lax.dynamic_slice_in_dim(w, mine_at, piece, 0).astype(BF) for w in (wq, wv)], axis=1
     )
-    early = EARLY * dl // 16
+    early = EARLY * dl // 32
     low, high = call(pack_body, [S((early, nc), BF), S((dl - early, nc), BF)], 2, limit=12)(wq, wv)
     near = [swap(low, "fs", nf, 1), swap(high, "fs", nf, 1)]
     far = []
@@ -310,12 +312,12 @@
     got = [own] + [swap(rest[k - 1], "fs", nf, k) for k in range(1, nf)]
     (proj,) = call(functools.partial(line_sum_body, nf), [S((g, nc), BF)], nf)(*got)
     got = [proj] + [swap(proj, "fs", nf, k) for k in range(1, nf)]
-    q1n, q2n, v1n, v2n, ratio = call(
-        functools.partial(moments_body, nf, nq),
-        [S((h, nq), F32)] * 2 + [S((h, nv), F32)] * 2 + [S((h, nc), BF)],
-        nf + 4,
-        [pltpu.VMEM((h, nc), F32)],
+    ratio, proj = call(
+        functools.partial(moments_body, nf, nq), [S((h, nc), BF), S((h, nc), F32)], nf + 4
     )(*got, q1, q2, v1, v2)
+    q1n, q2n, v1n, v2n = call(
+        functools.partial(state_body, nq), [S((h, nq), F32)] * 2 + [S((h, nv), F32)] * 2, 5
+    )(proj, q1, q2, v1, v2)
     got = [ratio] + [swap(ratio, "rep", nr, j) for j in range(1, nr)]
     ratios, total = call(
         functools.partial(total_body, nr, nq), [S((rank, nc), BF), S((16, 128), F32)], nr + 1, limit=12

time: 118 us -> 116 us (0.983)
  waiting for transfers between devices: 60.1 us -> 57.7 us
    ppermute x35, waiting for transfers between devices: 60.1 us -> 57.7 us  [swap(): return lax.ppermute(x, axis, [(i, i ^ k) for i in range(n)])]
  transfers between devices with their start and end apart: 35 -> 35, of which waited for: 17 -> 19; matrix products, arithmetic and copies ran while one was open for 3% -> 3% of each run, Pallas kernels for 10% -> 11%
where the time goes in v3:
time: 116 us
  waiting for transfers between devices  57.7 us (50%)
  starting transfers between devices  38.4 us (33%)
  Pallas kernels  14.4 us (12%)
  other arithmetic  2.52 us (2%)
  local copies, waits for them, and re-layouts  2.21 us (2%)
    ppermute x35, waiting for transfers between devices, swap(): return lax.ppermute(x, axis, [(i, i ^ k) for i in range(n)])  57.7 us
    ppermute x35, starting transfers between devices, swap(): return lax.ppermute(x, axis, [(i, i ^ k) for i in range(n)])  38.4 us
    pallas_call x1, Pallas kernels, exchange(): call(functools.partial(final_body, nt), [S((dl, nq), F32), S((dl, nv), F3...  4.21 us
    pallas_call x1, Pallas kernels, exchange(): call(functools.partial(project_body, nf, nr, nq), [S((h, nc), BF)] * nr +...  3.09 us
  transfers between devices with their start and end apart: 35, of which 19 were waited for; matrix products, arithmetic and copies ran while one was open for 3% of the time, Pallas kernels for 11%

profile of v3, /device:TPU:0, one launch (start us, length us, event | category | flops | bytes accessed | tf_op | source)
XLA Modules:
  0.0 116.2 jit_solution(15070899554800809592)
XLA Ops:
  1.7 3.1 %collective-permute-start = (bf16[128,256]{1,0:T(8,128)(2,1)S(1)}, bf16[128,256]{1,0:T(8,128)(2,1)S(1)}, u32[]{:S(2)}, u32[]{:S(2)}) collective-permute-start(bf16[128,256]{1,0:T(8,128)(2,1)S(1)} %dynamic-slice_select_fusion), channel_id=1, source_target_pairs={{0,8},{8,0},{16,24},{24,16},{1,9},{9,1},{17,25},{25,17},{2,10},{10... | collective-permute-start | bytes 196616 | tf_op jit(solution)/shard_map/ppermute | solution.py:26
  4.8 2.6 %collective-permute-start.1 = (bf16[128,256]{1,0:T(8,128)(2,1)S(1)}, bf16[128,256]{1,0:T(8,128)(2,1)S(1)}, u32[]{:S(2)}, u32[]{:S(2)}) collective-permute-start(bf16[128,256]{1,0:T(8,128)(2,1)S(1)} %dynamic-slice_select_fusion), channel_id=1, source_target_pairs={{0,16},{8,24},{16,0},{24,8},{1,17},{9,25},{17,1},{25,9},{2,18},{10... | collective-permute-start | bytes 196616 | tf_op jit(solution)/shard_map/ppermute | solution.py:26
  9.4 2.6 %collective-permute-done.1 = bf16[128,256]{1,0:T(8,128)(2,1)S(1)} collective-permute-done((bf16[128,256]{1,0:T(8,128)(2,1)S(1)}, bf16[128,256]{1,0:T(8,128)(2,1)S(1)}, u32[]{:S(2)}, u32[]{:S(2)}) %collective-permute-start.1) | collective-permute-done | bytes 65568 | tf_op jit(solution)/shard_map/ppermute | solution.py:26
  12.1 1.4 %collective-permute-done.2 = bf16[128,256]{1,0:T(8,128)(2,1)S(1)} collective-permute-done((bf16[128,256]{1,0:T(8,128)(2,1)S(1)}, bf16[128,256]{1,0:T(8,128)(2,1)S(1)}, u32[]{:S(2)}, u32[]{:S(2)}) %collective-permute-start.2) | collective-permute-done | bytes 65568 | tf_op jit(solution)/shard_map/ppermute | solution.py:26
  13.5 1.6 %collective-permute-start.3 = (bf16[3,128,256]{2,1,0:T(8,128)(2,1)S(1)}, bf16[3,128,256]{2,1,0:T(8,128)(2,1)S(1)}, u32[]{:S(2)}, u32[]{:S(2)}) collective-permute-start(bf16[3,128,256]{2,1,0:T(8,128)(2,1)S(1)} %pad_maximum_fusion.6.refs_0_), channel_id=1, source_target_pairs={{0,2},{2,0},{4,6},{6,4},{1,3},{3,1},{5,7},{7,5},{8,10},{10,8},{12,... | collective-permute-start | bytes 589832 | tf_op jit(solution)/shard_map/ppermute | solution.py:26
  15.0 1.5 %collective-permute-start.4 = (bf16[3,128,256]{2,1,0:T(8,128)(2,1)S(1)}, bf16[3,128,256]{2,1,0:T(8,128)(2,1)S(1)}, u32[]{:S(2)}, u32[]{:S(2)}) collective-permute-start(bf16[3,128,256]{2,1,0:T(8,128)(2,1)S(1)} %pad_maximum_fusion.6.refs_0_), channel_id=1, source_target_pairs={{0,4},{2,6},{4,0},{6,2},{1,5},{3,7},{5,1},{7,3},{8,12},{10,14},{12... | collective-permute-start | bytes 589832 | tf_op jit(solution)/shard_map/ppermute | solution.py:26
  17.1 1.6 %collective-permute-start.23 = (bf16[128,1536]{1,0:T(8,128)(2,1)S(1)}, bf16[128,1536]{1,0:T(8,128)(2,1)S(1)}, u32[]{:S(2)}, u32[]{:S(2)}) collective-permute-start(bf16[128,1536]{1,0:T(8,128)(2,1)S(1)} %pad_maximum_fusion.1), channel_id=1, source_target_pairs={{0,16},{8,24},{16,0},{24,8},{1,17},{9,25},{17,1},{25,9},{2,18},{10... | collective-permute-start | bytes 1179656 | tf_op jit(solution)/shard_map/ppermute | solution.py:26
  18.7 2.2 %collective-permute-done.3.refs_1_ = bf16[3,128,256]{2,1,0:T(8,128)(2,1)S(1)} collective-permute-done((bf16[3,128,256]{2,1,0:T(8,128)(2,1)S(1)}, bf16[3,128,256]{2,1,0:T(8,128)(2,1)S(1)}, u32[]{:S(2)}, u32[]{:S(2)}) %collective-permute-start.3) | collective-permute-done | bytes 196640 | tf_op jit(solution)/shard_map/ppermute | solution.py:26
  21.0 3.3 %collective-permute-done.4.refs_2_ = bf16[3,128,256]{2,1,0:T(8,128)(2,1)S(1)} collective-permute-done((bf16[3,128,256]{2,1,0:T(8,128)(2,1)S(1)}, bf16[3,128,256]{2,1,0:T(8,128)(2,1)S(1)}, u32[]{:S(2)}, u32[]{:S(2)}) %collective-permute-start.4) | collective-permute-done | bytes 196640 | tf_op jit(solution)/shard_map/ppermute | solution.py:26
  27.3 3.1 %shard_map.187 = (bf16[64,1536]{1,0:T(8,128)(2,1)S(1)}, bf16[64,1536]{1,0:T(8,128)(2,1)S(1)}, bf16[64,1536]{1,0:T(8,128)(2,1)S(1)}, bf16[64,1536]{1,0:T(8,128)(2,1)S(1)}, bf16[2,2048,256]{2,1,0:T(8,128)(2,1)S(1)}) custom-call(bf16[768,2048]{1,0:T(8,128)(2,1)S(1)} %copy-done, bf16[512,256]{1,0:T(8,128)(2,1)S(1)} %copy-done.3, bf16[512,256]{1,0:T(8,128)(2,1)S(1)} %copy-done.4, ...), custom_call_target="tpu_custom_call" | custom-call | flops 1409286144 | bytes 9699328 | tf_op jit(solution)/shard_map/pallas_call | solution.py:293
  32.2 1.7 %collective-permute-start.12 = (bf16[64,1536]{1,0:T(8,128)(2,1)S(1)}, bf16[64,1536]{1,0:T(8,128)(2,1)S(1)}, u32[]{:S(2)}, u32[]{:S(2)}) collective-permute-start(bf16[64,1536]{1,0:T(8,128)(2,1)S(1)} %get-tuple-element.46), channel_id=1, source_target_pairs={{0,6},{2,4},{4,2},{6,0},{1,7},{3,5},{5,3},{7,1},{8,14},{10,12},{12... | collective-permute-start | bytes 589832 | tf_op jit(solution)/shard_map/ppermute | solution.py:26
  34.9 3.3 %collective-permute-done.10.refs_1_ = bf16[64,1536]{1,0:T(8,128)(2,1)S(1)} collective-permute-done((bf16[64,1536]{1,0:T(8,128)(2,1)S(1)}, bf16[64,1536]{1,0:T(8,128)(2,1)S(1)}, u32[]{:S(2)}, u32[]{:S(2)}) %collective-permute-start.10) | collective-permute-done | bytes 196640 | tf_op jit(solution)/shard_map/ppermute | solution.py:26
  38.9 3.2 %collective-permute-done.12.refs_3_ = bf16[64,1536]{1,0:T(8,128)(2,1)S(1)} collective-permute-done((bf16[64,1536]{1,0:T(8,128)(2,1)S(1)}, bf16[64,1536]{1,0:T(8,128)(2,1)S(1)}, u32[]{:S(2)}, u32[]{:S(2)}) %collective-permute-start.12) | collective-permute-done | bytes 196640 | tf_op jit(solution)/shard_map/ppermute | solution.py:26
  43.1 1.4 %collective-permute-start.14 = (bf16[16,1536]{1,0:T(8,128)(2,1)S(1)}, bf16[16,1536]{1,0:T(8,128)(2,1)S(1)}, u32[]{:S(2)}, u32[]{:S(2)}) collective-permute-start(bf16[16,1536]{1,0:T(8,128)(2,1)S(1)} %get-tuple-element.49), channel_id=1, source_target_pairs={{0,16},{8,24},{16,0},{24,8},{1,17},{9,25},{17,1},{25,9},{2,18},{10... | collective-permute-start | bytes 147464 | tf_op jit(solution)/shard_map/ppermute | solution.py:26
  44.5 2.2 %collective-permute-start.15 = (bf16[16,1536]{1,0:T(8,128)(2,1)S(1)}, bf16[16,1536]{1,0:T(8,128)(2,1)S(1)}, u32[]{:S(2)}, u32[]{:S(2)}) collective-permute-start(bf16[16,1536]{1,0:T(8,128)(2,1)S(1)} %get-tuple-element.50), channel_id=1, source_target_pairs={{0,24},{8,16},{16,8},{24,0},{1,25},{9,17},{17,9},{25,1},{2,26},{10... | collective-permute-start | bytes 147464 | tf_op jit(solution)/shard_map/ppermute | solution.py:26
  47.4 1.7 %collective-permute-done.14.refs_2_ = bf16[16,1536]{1,0:T(8,128)(2,1)S(1)} collective-permute-done((bf16[16,1536]{1,0:T(8,128)(2,1)S(1)}, bf16[16,1536]{1,0:T(8,128)(2,1)S(1)}, u32[]{:S(2)}, u32[]{:S(2)}) %collective-permute-start.14) | collective-permute-done | bytes 49184 | tf_op jit(solution)/shard_map/ppermute | solution.py:26
  49.0 1.9 %collective-permute-done.15.refs_3_ = bf16[16,1536]{1,0:T(8,128)(2,1)S(1)} collective-permute-done((bf16[16,1536]{1,0:T(8,128)(2,1)S(1)}, bf16[16,1536]{1,0:T(8,128)(2,1)S(1)}, u32[]{:S(2)}, u32[]{:S(2)}) %collective-permute-start.15) | collective-permute-done | bytes 49184 | tf_op jit(solution)/shard_map/ppermute | solution.py:26
  51.1 2.8 %collective-permute-start.17 = (bf16[16,1536]{1,0:T(8,128)(2,1)S(1)}, bf16[16,1536]{1,0:T(8,128)(2,1)S(1)}, u32[]{:S(2)}, u32[]{:S(2)}) collective-permute-start(bf16[16,1536]{1,0:T(8,128)(2,1)S(1)} %shard_map.189.refs_0_), channel_id=1, source_target_pairs={{0,16},{8,24},{16,0},{24,8},{1,17},{9,25},{17,1},{25,9},{2,18},{10... | collective-permute-start | bytes 147464 | tf_op jit(solution)/shard_map/ppermute | solution.py:26
  53.8 1.6 %collective-permute-start.18 = (bf16[16,1536]{1,0:T(8,128)(2,1)S(1)}, bf16[16,1536]{1,0:T(8,128)(2,1)S(1)}, u32[]{:S(2)}, u32[]{:S(2)}) collective-permute-start(bf16[16,1536]{1,0:T(8,128)(2,1)S(1)} %shard_map.189.refs_0_), channel_id=1, source_target_pairs={{0,24},{8,16},{16,8},{24,0},{1,25},{9,17},{17,9},{25,1},{2,26},{10... | collective-permute-start | bytes 147464 | tf_op jit(solution)/shard_map/ppermute | solution.py:26
  55.5 17.4 %collective-permute-done.16.refs_1_ = bf16[16,1536]{1,0:T(8,128)(2,1)S(1)} collective-permute-done((bf16[16,1536]{1,0:T(8,128)(2,1)S(1)}, bf16[16,1536]{1,0:T(8,128)(2,1)S(1)}, u32[]{:S(2)}, u32[]{:S(2)}) %collective-permute-start.16) | collective-permute-done | bytes 49184 | tf_op jit(solution)/shard_map/ppermute | solution.py:26
  74.1 1.5 %collective-permute-start.25 = (bf16[128,768]{1,0:T(8,128)(2,1)S(1)}, bf16[128,768]{1,0:T(8,128)(2,1)S(1)}, u32[]{:S(2)}, u32[]{:S(2)}) collective-permute-start(bf16[128,768]{1,0:T(8,128)(2,1)S(1)} %get-tuple-element.76), channel_id=1, source_target_pairs={{0,4},{2,6},{4,0},{6,2},{1,5},{3,7},{5,1},{7,3},{8,12},{10,14},{12... | collective-permute-start | bytes 589832 | tf_op jit(solution)/shard_map/ppermute | solution.py:26
  77.5 2.6 %collective-permute-done.24.refs_8_ = bf16[128,768]{1,0:T(8,128)(2,1)S(1)} collective-permute-done((bf16[128,768]{1,0:T(8,128)(2,1)S(1)}, bf16[128,768]{1,0:T(8,128)(2,1)S(1)}, u32[]{:S(2)}, u32[]{:S(2)}) %collective-permute-start.24) | collective-permute-done | bytes 196640 | tf_op jit(solution)/shard_map/ppermute | solution.py:26
  80.0 2.9 %collective-permute-start.21 = (bf16[64,1536]{1,0:T(8,128)(2,1)S(1)}, bf16[64,1536]{1,0:T(8,128)(2,1)S(1)}, u32[]{:S(2)}, u32[]{:S(2)}) collective-permute-start(bf16[64,1536]{1,0:T(8,128)(2,1)S(1)} %get-tuple-element.51.refs_0_), channel_id=1, source_target_pairs={{0,6},{2,4},{4,2},{6,0},{1,7},{3,5},{5,3},{7,1},{8,14},{10,12},{12... | collective-permute-start | bytes 589832 | tf_op jit(solution)/shard_map/ppermute | solution.py:26
  84.2 1.9 %collective-permute-start.26 = (bf16[2,128,768]{2,1,0:T(8,128)(2,1)S(1)}, bf16[2,128,768]{2,1,0:T(8,128)(2,1)S(1)}, u32[]{:S(2)}, u32[]{:S(2)}) collective-permute-start(bf16[2,128,768]{2,1,0:T(8,128)(2,1)S(1)} %pad_maximum_fusion.2), channel_id=1, source_target_pairs={{0,4},{2,6},{4,0},{6,2},{1,5},{3,7},{5,1},{7,3},{8,12},{10,14},{12... | collective-permute-start | bytes 1179656 | tf_op jit(solution)/shard_map/ppermute | solution.py:26
  86.9 1.6 %collective-permute-done.20.refs_2_ = bf16[64,1536]{1,0:T(8,128)(2,1)S(1)} collective-permute-done((bf16[64,1536]{1,0:T(8,128)(2,1)S(1)}, bf16[64,1536]{1,0:T(8,128)(2,1)S(1)}, u32[]{:S(2)}, u32[]{:S(2)}) %collective-permute-start.20) | collective-permute-done | bytes 196640 | tf_op jit(solution)/shard_map/ppermute | solution.py:26
  88.5 2.6 %collective-permute-start.32 = (bf16[128,768]{1,0:T(8,128)(2,1)S(1)}, bf16[128,768]{1,0:T(8,128)(2,1)S(1)}, u32[]{:S(2)}, u32[]{:S(2)}) collective-permute-start(bf16[128,768]{1,0:T(8,128)(2,1)S(1)} %get-tuple-element.72), channel_id=1, source_target_pairs={{0,4},{2,6},{4,0},{6,2},{1,5},{3,7},{5,1},{7,3},{8,12},{10,14},{12... | collective-permute-start | bytes 589832 | tf_op jit(solution)/shard_map/ppermute | solution.py:26
  92.6 7.9 %collective-permute-done.32.refs_4_ = bf16[128,768]{1,0:T(8,128)(2,1)S(1)} collective-permute-done((bf16[128,768]{1,0:T(8,128)(2,1)S(1)}, bf16[128,768]{1,0:T(8,128)(2,1)S(1)}, u32[]{:S(2)}, u32[]{:S(2)}) %collective-permute-start.32) | collective-permute-done | bytes 196640 | tf_op jit(solution)/shard_map/ppermute | solution.py:26
  101.7 1.7 %collective-permute-start.33 = (bf16[2,128,768]{2,1,0:T(8,128)(2,1)S(1)}, bf16[2,128,768]{2,1,0:T(8,128)(2,1)S(1)}, u32[]{:S(2)}, u32[]{:S(2)}) collective-permute-start(bf16[2,128,768]{2,1,0:T(8,128)(2,1)S(1)} %pad_maximum_fusion.4), channel_id=1, source_target_pairs={{0,4},{2,6},{4,0},{6,2},{1,5},{3,7},{5,1},{7,3},{8,12},{10,14},{12... | collective-permute-start | bytes 1179656 | tf_op jit(solution)/shard_map/ppermute | solution.py:26
  105.5 4.2 %shard_map.194 = (f32[512,512]{1,0:T(8,128)}, f32[512,1024]{1,0:T(8,128)}, f32[512,512]{1,0:T(8,128)}, f32[512,1024]{1,0:T(8,128)}, bf16[2048,512]{1,0:T(8,128)(...) custom-call(bf16[2,2048,256]{2,1,0:T(8,128)(2,1)S(1)} %get-tuple-element.42.fac.refs_0_, ...), custom_call_target="tpu_custom_call" | custom-call | flops 1610612736 | bytes 22020096 | tf_op jit(solution)/shard_map/pallas_call | solution.py:334
  109.7 3.2 %collective-permute-done.33.refs_5_ = bf16[2,128,768]{2,1,0:T(8,128)(2,1)S(1)} collective-permute-done((bf16[2,128,768]{2,1,0:T(8,128)(2,1)S(1)}, bf16[2,128,768]{2,1,0:T(8,128)(2,1)S(1)}, u32[]{:S(2)}, u32[]{:S(2)}) %collective-permute-start.33) | collective-permute-done | bytes 393248 | tf_op jit(solution)/shard_map/ppermute | solution.py:26
  112.9 1.4 %collective-permute-done.34.refs_6_ = bf16[2,128,768]{2,1,0:T(8,128)(2,1)S(1)} collective-permute-done((bf16[2,128,768]{2,1,0:T(8,128)(2,1)S(1)}, bf16[2,128,768]{2,1,0:T(8,128)(2,1)S(1)}, u32[]{:S(2)}, u32[]{:S(2)}) %collective-permute-start.34) | collective-permute-done | bytes 393248 | tf_op jit(solution)/shard_map/ppermute | solution.py:26
  114.3 1.9 %shard_map.197 = (bf16[2048,512]{1,0:T(8,128)(2,1)}, bf16[2048,1024]{1,0:T(8,128)(2,1)}) custom-call(f32[2,512,1536]{2,1,0:T(8,128)S(1)} %get-tuple-element.63.raw, bf16[192,1536]{1,0:T(8,128)(2,1)S(1)} %collective-permute-done.28.refs_0_, bf16[320,1536]{1,0:T(8,128)(2,1)S(1)} %collective-permute-done.29.refs_1_, ...), custom_call_target="tpu_custom_call", output_to_operand_aliasing={{0}: (8, {}), {1}: (9, {})} | custom-call | flops 3145728 | bytes 6291456 | tf_op jit(solution)/shard_map/pallas_call | solution.py:353
  (82 shorter events, 21.3 us)
Async XLA Ops:
  1.7 7.8 %collective-permute-start = (bf16[128,256]{1,0:T(8,128)(2,1)S(1)}, bf16[128,256]{1,0:T(8,128)(2,1)S(1)}, u32[]{:S(2)}, u32[]{:S(2)}) collective-permute-start(bf16[128,256]{1,0:T(8,128)(2,1)S(1)} %dynamic-slice_select_fusion), channel_id=1, source_target_pairs={{0,8},{8,0},{16,24},{24,16},{1,9},{9,1},{17,25},{25,17},{2,10},{10... | collective-permute-start | bytes 196616 | tf_op jit(solution)/shard_map/ppermute | solution.py:26
  4.8 7.3 %collective-permute-start.1 = (bf16[128,256]{1,0:T(8,128)(2,1)S(1)}, bf16[128,256]{1,0:T(8,128)(2,1)S(1)}, u32[]{:S(2)}, u32[]{:S(2)}) collective-permute-start(bf16[128,256]{1,0:T(8,128)(2,1)S(1)} %dynamic-slice_select_fusion), channel_id=1, source_target_pairs={{0,16},{8,24},{16,0},{24,8},{1,17},{9,25},{17,1},{25,9},{2,18},{10... | collective-permute-start | bytes 196616 | tf_op jit(solution)/shard_map/ppermute | solution.py:26
  7.4 6.1 %collective-permute-start.2 = (bf16[128,256]{1,0:T(8,128)(2,1)S(1)}, bf16[128,256]{1,0:T(8,128)(2,1)S(1)}, u32[]{:S(2)}, u32[]{:S(2)}) collective-permute-start(bf16[128,256]{1,0:T(8,128)(2,1)S(1)} %dynamic-slice_select_fusion), channel_id=1, source_target_pairs={{0,24},{8,16},{16,8},{24,0},{1,25},{9,17},{17,9},{25,1},{2,26},{10... | collective-permute-start | bytes 196616 | tf_op jit(solution)/shard_map/ppermute | solution.py:26
  13.5 7.5 %collective-permute-start.3 = (bf16[3,128,256]{2,1,0:T(8,128)(2,1)S(1)}, bf16[3,128,256]{2,1,0:T(8,128)(2,1)S(1)}, u32[]{:S(2)}, u32[]{:S(2)}) collective-permute-start(bf16[3,128,256]{2,1,0:T(8,128)(2,1)S(1)} %pad_maximum_fusion.6.refs_0_), channel_id=1, source_target_pairs={{0,2},{2,0},{4,6},{6,4},{1,3},{3,1},{5,7},{7,5},{8,10},{10,8},{12,... | collective-permute-start | bytes 589832 | tf_op jit(solution)/shard_map/ppermute | solution.py:26
  15.0 9.3 %collective-permute-start.4 = (bf16[3,128,256]{2,1,0:T(8,128)(2,1)S(1)}, bf16[3,128,256]{2,1,0:T(8,128)(2,1)S(1)}, u32[]{:S(2)}, u32[]{:S(2)}) collective-permute-start(bf16[3,128,256]{2,1,0:T(8,128)(2,1)S(1)} %pad_maximum_fusion.6.refs_0_), channel_id=1, source_target_pairs={{0,4},{2,6},{4,0},{6,2},{1,5},{3,7},{5,1},{7,3},{8,12},{10,14},{12... | collective-permute-start | bytes 589832 | tf_op jit(solution)/shard_map/ppermute | solution.py:26
  16.6 7.7 %collective-permute-start.5 = (bf16[3,128,256]{2,1,0:T(8,128)(2,1)S(1)}, bf16[3,128,256]{2,1,0:T(8,128)(2,1)S(1)}, u32[]{:S(2)}, u32[]{:S(2)}) collective-permute-start(bf16[3,128,256]{2,1,0:T(8,128)(2,1)S(1)} %pad_maximum_fusion.6.refs_0_), channel_id=1, source_target_pairs={{0,6},{2,4},{4,2},{6,0},{1,7},{3,5},{5,3},{7,1},{8,14},{10,12},{12... | collective-permute-start | bytes 589832 | tf_op jit(solution)/shard_map/ppermute | solution.py:26
  17.1 17.8 %collective-permute-start.23 = (bf16[128,1536]{1,0:T(8,128)(2,1)S(1)}, bf16[128,1536]{1,0:T(8,128)(2,1)S(1)}, u32[]{:S(2)}, u32[]{:S(2)}) collective-permute-start(bf16[128,1536]{1,0:T(8,128)(2,1)S(1)} %pad_maximum_fusion.1), channel_id=1, source_target_pairs={{0,16},{8,24},{16,0},{24,8},{1,17},{9,25},{17,1},{25,9},{2,18},{10... | collective-permute-start | bytes 1179656 | tf_op jit(solution)/shard_map/ppermute | solution.py:26
  18.7 8.5 %collective-permute-start.6 = (bf16[3,128,256]{2,1,0:T(8,128)(2,1)S(1)}, bf16[3,128,256]{2,1,0:T(8,128)(2,1)S(1)}, u32[]{:S(2)}, u32[]{:S(2)}) collective-permute-start(bf16[3,128,256]{2,1,0:T(8,128)(2,1)S(1)} %pad_maximum_fusion.6.refs_0_), channel_id=1, source_target_pairs={{0,1},{1,0},{2,3},{3,2},{4,5},{5,4},{6,7},{7,6},{8,9},{9,8},{10,11... | collective-permute-start | bytes 589832 | tf_op jit(solution)/shard_map/ppermute | solution.py:26
  21.0 6.3 %collective-permute-start.7 = (bf16[3,128,256]{2,1,0:T(8,128)(2,1)S(1)}, bf16[3,128,256]{2,1,0:T(8,128)(2,1)S(1)}, u32[]{:S(2)}, u32[]{:S(2)}) collective-permute-start(bf16[3,128,256]{2,1,0:T(8,128)(2,1)S(1)} %collective-permute-done.3.refs_1_), channel_id=1, source_target_pairs={{0,1},{1,0},{2,3},{3,2},{4,5},{5,4},{6,7},{7,6},{8,9},{9,8},{10,11... | collective-permute-start | bytes 589832 | tf_op jit(solution)/shard_map/ppermute | solution.py:26
  30.4 7.8 %collective-permute-start.10 = (bf16[64,1536]{1,0:T(8,128)(2,1)S(1)}, bf16[64,1536]{1,0:T(8,128)(2,1)S(1)}, u32[]{:S(2)}, u32[]{:S(2)}) collective-permute-start(bf16[64,1536]{1,0:T(8,128)(2,1)S(1)} %get-tuple-element.44), channel_id=1, source_target_pairs={{0,2},{2,0},{4,6},{6,4},{1,3},{3,1},{5,7},{7,5},{8,10},{10,8},{12,... | collective-permute-start | bytes 589832 | tf_op jit(solution)/shard_map/ppermute | solution.py:26
  30.9 8.0 %collective-permute-start.11 = (bf16[64,1536]{1,0:T(8,128)(2,1)S(1)}, bf16[64,1536]{1,0:T(8,128)(2,1)S(1)}, u32[]{:S(2)}, u32[]{:S(2)}) collective-permute-start(bf16[64,1536]{1,0:T(8,128)(2,1)S(1)} %get-tuple-element.45), channel_id=1, source_target_pairs={{0,4},{2,6},{4,0},{6,2},{1,5},{3,7},{5,1},{7,3},{8,12},{10,14},{12... | collective-permute-start | bytes 589832 | tf_op jit(solution)/shard_map/ppermute | solution.py:26
  32.2 9.9 %collective-permute-start.12 = (bf16[64,1536]{1,0:T(8,128)(2,1)S(1)}, bf16[64,1536]{1,0:T(8,128)(2,1)S(1)}, u32[]{:S(2)}, u32[]{:S(2)}) collective-permute-start(bf16[64,1536]{1,0:T(8,128)(2,1)S(1)} %get-tuple-element.46), channel_id=1, source_target_pairs={{0,6},{2,4},{4,2},{6,0},{1,7},{3,5},{5,3},{7,1},{8,14},{10,12},{12... | collective-permute-start | bytes 589832 | tf_op jit(solution)/shard_map/ppermute | solution.py:26
  34.9 41.8 %collective-permute-start.30 = (bf16[128,1536]{1,0:T(8,128)(2,1)S(1)}, bf16[128,1536]{1,0:T(8,128)(2,1)S(1)}, u32[]{:S(2)}, u32[]{:S(2)}) collective-permute-start(bf16[128,1536]{1,0:T(8,128)(2,1)S(1)} %collective-permute-done.23.refs_7_), channel_id=1, source_target_pairs={{0,8},{8,0},{16,24},{24,16},{1,9},{9,1},{17,25},{25,17},{2,10},{10... | collective-permute-start | bytes 1179656 | tf_op jit(solution)/shard_map/ppermute | solution.py:26
  42.3 5.0 %collective-permute-start.13 = (bf16[16,1536]{1,0:T(8,128)(2,1)S(1)}, bf16[16,1536]{1,0:T(8,128)(2,1)S(1)}, u32[]{:S(2)}, u32[]{:S(2)}) collective-permute-start(bf16[16,1536]{1,0:T(8,128)(2,1)S(1)} %get-tuple-element.48), channel_id=1, source_target_pairs={{0,8},{8,0},{16,24},{24,16},{1,9},{9,1},{17,25},{25,17},{2,10},{10... | collective-permute-start | bytes 147464 | tf_op jit(solution)/shard_map/ppermute | solution.py:26
  43.1 5.9 %collective-permute-start.14 = (bf16[16,1536]{1,0:T(8,128)(2,1)S(1)}, bf16[16,1536]{1,0:T(8,128)(2,1)S(1)}, u32[]{:S(2)}, u32[]{:S(2)}) collective-permute-start(bf16[16,1536]{1,0:T(8,128)(2,1)S(1)} %get-tuple-element.49), channel_id=1, source_target_pairs={{0,16},{8,24},{16,0},{24,8},{1,17},{9,25},{17,1},{25,9},{2,18},{10... | collective-permute-start | bytes 147464 | tf_op jit(solution)/shard_map/ppermute | solution.py:26
  44.5 6.4 %collective-permute-start.15 = (bf16[16,1536]{1,0:T(8,128)(2,1)S(1)}, bf16[16,1536]{1,0:T(8,128)(2,1)S(1)}, u32[]{:S(2)}, u32[]{:S(2)}) collective-permute-start(bf16[16,1536]{1,0:T(8,128)(2,1)S(1)} %get-tuple-element.50), channel_id=1, source_target_pairs={{0,24},{8,16},{16,8},{24,0},{1,25},{9,17},{17,9},{25,1},{2,26},{10... | collective-permute-start | bytes 147464 | tf_op jit(solution)/shard_map/ppermute | solution.py:26
  46.9 62.8 %collective-permute-start.29 = (bf16[320,1536]{1,0:T(8,128)(2,1)S(1)}, bf16[320,1536]{1,0:T(8,128)(2,1)S(1)}, u32[]{:S(2)}, u32[]{:S(2)}) collective-permute-start(bf16[320,1536]{1,0:T(8,128)(2,1)S(1)} %get-tuple-element.65), channel_id=1, source_target_pairs={{0,8},{8,0},{16,24},{24,16},{1,9},{9,1},{17,25},{25,17},{2,10},{10... | collective-permute-start | bytes 2949128 | tf_op jit(solution)/shard_map/ppermute | solution.py:26
  51.0 21.9 %collective-permute-start.16 = (bf16[16,1536]{1,0:T(8,128)(2,1)S(1)}, bf16[16,1536]{1,0:T(8,128)(2,1)S(1)}, u32[]{:S(2)}, u32[]{:S(2)}) collective-permute-start(bf16[16,1536]{1,0:T(8,128)(2,1)S(1)} %shard_map.189.refs_0_), channel_id=1, source_target_pairs={{0,8},{8,0},{16,24},{24,16},{1,9},{9,1},{17,25},{25,17},{2,10},{10... | collective-permute-start | bytes 147464 | tf_op jit(solution)/shard_map/ppermute | solution.py:26
  51.1 23.1 %collective-permute-start.17 = (bf16[16,1536]{1,0:T(8,128)(2,1)S(1)}, bf16[16,1536]{1,0:T(8,128)(2,1)S(1)}, u32[]{:S(2)}, u32[]{:S(2)}) collective-permute-start(bf16[16,1536]{1,0:T(8,128)(2,1)S(1)} %shard_map.189.refs_0_), channel_id=1, source_target_pairs={{0,16},{8,24},{16,0},{24,8},{1,17},{9,25},{17,1},{25,9},{2,18},{10... | collective-permute-start | bytes 147464 | tf_op jit(solution)/shard_map/ppermute | solution.py:26
  53.8 21.8 %collective-permute-start.18 = (bf16[16,1536]{1,0:T(8,128)(2,1)S(1)}, bf16[16,1536]{1,0:T(8,128)(2,1)S(1)}, u32[]{:S(2)}, u32[]{:S(2)}) collective-permute-start(bf16[16,1536]{1,0:T(8,128)(2,1)S(1)} %shard_map.189.refs_0_), channel_id=1, source_target_pairs={{0,24},{8,16},{16,8},{24,0},{1,25},{9,17},{17,9},{25,1},{2,26},{10... | collective-permute-start | bytes 147464 | tf_op jit(solution)/shard_map/ppermute | solution.py:26
  72.9 7.1 %collective-permute-start.24 = (bf16[128,768]{1,0:T(8,128)(2,1)S(1)}, bf16[128,768]{1,0:T(8,128)(2,1)S(1)}, u32[]{:S(2)}, u32[]{:S(2)}) collective-permute-start(bf16[128,768]{1,0:T(8,128)(2,1)S(1)} %get-tuple-element.77), channel_id=1, source_target_pairs={{0,2},{2,0},{4,6},{6,4},{1,3},{3,1},{5,7},{7,5},{8,10},{10,8},{12,... | collective-permute-start | bytes 589832 | tf_op jit(solution)/shard_map/ppermute | solution.py:26
  74.1 8.7 %collective-permute-start.25 = (bf16[128,768]{1,0:T(8,128)(2,1)S(1)}, bf16[128,768]{1,0:T(8,128)(2,1)S(1)}, u32[]{:S(2)}, u32[]{:S(2)}) collective-permute-start(bf16[128,768]{1,0:T(8,128)(2,1)S(1)} %get-tuple-element.76), channel_id=1, source_target_pairs={{0,4},{2,6},{4,0},{6,2},{1,5},{3,7},{5,1},{7,3},{8,12},{10,14},{12... | collective-permute-start | bytes 589832 | tf_op jit(solution)/shard_map/ppermute | solution.py:26
  76.0 8.2 %collective-permute-start.19 = (bf16[64,1536]{1,0:T(8,128)(2,1)S(1)}, bf16[64,1536]{1,0:T(8,128)(2,1)S(1)}, u32[]{:S(2)}, u32[]{:S(2)}) collective-permute-start(bf16[64,1536]{1,0:T(8,128)(2,1)S(1)} %get-tuple-element.51.refs_0_), channel_id=1, source_target_pairs={{0,2},{2,0},{4,6},{6,4},{1,3},{3,1},{5,7},{7,5},{8,10},{10,8},{12,... | collective-permute-start | bytes 589832 | tf_op jit(solution)/shard_map/ppermute | solution.py:26
  76.6 11.9 %collective-permute-start.20 = (bf16[64,1536]{1,0:T(8,128)(2,1)S(1)}, bf16[64,1536]{1,0:T(8,128)(2,1)S(1)}, u32[]{:S(2)}, u32[]{:S(2)}) collective-permute-start(bf16[64,1536]{1,0:T(8,128)(2,1)S(1)} %get-tuple-element.51.refs_0_), channel_id=1, source_target_pairs={{0,4},{2,6},{4,0},{6,2},{1,5},{3,7},{5,1},{7,3},{8,12},{10,14},{12... | collective-permute-start | bytes 589832 | tf_op jit(solution)/shard_map/ppermute | solution.py:26
  80.0 11.2 %collective-permute-start.21 = (bf16[64,1536]{1,0:T(8,128)(2,1)S(1)}, bf16[64,1536]{1,0:T(8,128)(2,1)S(1)}, u32[]{:S(2)}, u32[]{:S(2)}) collective-permute-start(bf16[64,1536]{1,0:T(8,128)(2,1)S(1)} %get-tuple-element.51.refs_0_), channel_id=1, source_target_pairs={{0,6},{2,4},{4,2},{6,0},{1,7},{3,5},{5,3},{7,1},{8,14},{10,12},{12... | collective-permute-start | bytes 589832 | tf_op jit(solution)/shard_map/ppermute | solution.py:26
  82.9 9.6 %collective-permute-start.31 = (bf16[128,768]{1,0:T(8,128)(2,1)S(1)}, bf16[128,768]{1,0:T(8,128)(2,1)S(1)}, u32[]{:S(2)}, u32[]{:S(2)}) collective-permute-start(bf16[128,768]{1,0:T(8,128)(2,1)S(1)} %get-tuple-element.73), channel_id=1, source_target_pairs={{0,2},{2,0},{4,6},{6,4},{1,3},{3,1},{5,7},{7,5},{8,10},{10,8},{12,... | collective-permute-start | bytes 589832 | tf_op jit(solution)/shard_map/ppermute | solution.py:26
  84.2 19.2 %collective-permute-start.26 = (bf16[2,128,768]{2,1,0:T(8,128)(2,1)S(1)}, bf16[2,128,768]{2,1,0:T(8,128)(2,1)S(1)}, u32[]{:S(2)}, u32[]{:S(2)}) collective-permute-start(bf16[2,128,768]{2,1,0:T(8,128)(2,1)S(1)} %pad_maximum_fusion.2), channel_id=1, source_target_pairs={{0,4},{2,6},{4,0},{6,2},{1,5},{3,7},{5,1},{7,3},{8,12},{10,14},{12... | collective-permute-start | bytes 1179656 | tf_op jit(solution)/shard_map/ppermute | solution.py:26
  88.5 12.0 %collective-permute-start.32 = (bf16[128,768]{1,0:T(8,128)(2,1)S(1)}, bf16[128,768]{1,0:T(8,128)(2,1)S(1)}, u32[]{:S(2)}, u32[]{:S(2)}) collective-permute-start(bf16[128,768]{1,0:T(8,128)(2,1)S(1)} %get-tuple-element.72), channel_id=1, source_target_pairs={{0,4},{2,6},{4,0},{6,2},{1,5},{3,7},{5,1},{7,3},{8,12},{10,14},{12... | collective-permute-start | bytes 589832 | tf_op jit(solution)/shard_map/ppermute | solution.py:26
  91.2 18.5 %collective-permute-start.28 = (bf16[192,1536]{1,0:T(8,128)(2,1)S(1)}, bf16[192,1536]{1,0:T(8,128)(2,1)S(1)}, u32[]{:S(2)}, u32[]{:S(2)}) collective-permute-start(bf16[192,1536]{1,0:T(8,128)(2,1)S(1)} %get-tuple-element.64), channel_id=1, source_target_pairs={{0,8},{8,0},{16,24},{24,16},{1,9},{9,1},{17,25},{25,17},{2,10},{10... | collective-permute-start | bytes 1769480 | tf_op jit(solution)/shard_map/ppermute | solution.py:26
  92.5 13.0 %collective-permute-start.27 = (bf16[2,128,768]{2,1,0:T(8,128)(2,1)S(1)}, bf16[2,128,768]{2,1,0:T(8,128)(2,1)S(1)}, u32[]{:S(2)}, u32[]{:S(2)}) collective-permute-start(bf16[2,128,768]{2,1,0:T(8,128)(2,1)S(1)} %pad_maximum_fusion.3), channel_id=1, source_target_pairs={{0,2},{2,0},{4,6},{6,4},{1,3},{3,1},{5,7},{7,5},{8,10},{10,8},{12,... | collective-permute-start | bytes 1179656 | tf_op jit(solution)/shard_map/ppermute | solution.py:26
  101.7 11.2 %collective-permute-start.33 = (bf16[2,128,768]{2,1,0:T(8,128)(2,1)S(1)}, bf16[2,128,768]{2,1,0:T(8,128)(2,1)S(1)}, u32[]{:S(2)}, u32[]{:S(2)}) collective-permute-start(bf16[2,128,768]{2,1,0:T(8,128)(2,1)S(1)} %pad_maximum_fusion.4), channel_id=1, source_target_pairs={{0,4},{2,6},{4,0},{6,2},{1,5},{3,7},{5,1},{7,3},{8,12},{10,14},{12... | collective-permute-start | bytes 1179656 | tf_op jit(solution)/shard_map/ppermute | solution.py:26
  103.4 10.9 %collective-permute-start.34 = (bf16[2,128,768]{2,1,0:T(8,128)(2,1)S(1)}, bf16[2,128,768]{2,1,0:T(8,128)(2,1)S(1)}, u32[]{:S(2)}, u32[]{:S(2)}) collective-permute-start(bf16[2,128,768]{2,1,0:T(8,128)(2,1)S(1)} %pad_maximum_fusion.5), channel_id=1, source_target_pairs={{0,2},{2,0},{4,6},{6,4},{1,3},{3,1},{5,7},{7,5},{8,10},{10,8},{12,... | collective-permute-start | bytes 1179656 | tf_op jit(solution)/shard_map/ppermute | solution.py:26
  (13 other events, 231.0 us)
